TPU v7x, 32 devices: a whole 2x2x4 slice. The times are simulated.
32 devices in a mesh: tp: 16 (over z, y, x), dp: 2 (over core).
Axes of the slice: x: 2, y: 2, z: 4, core: 2. Of those that a mesh axis runs over, the one named last changes fastest.
Arguments:
- tokens: bfloat16 [64, 4096], P(None, 'dp'), may hold values from -6 to 6
- lengths: int32 [64], P('dp'), may hold values from 1 to 4096, 65536 in all
- norm_gain: float32 [2, 4096], P(None, 'dp'), may hold values from 0.1 to 1.9
- w_in: bfloat16 [2, 4096, 2048], P(None, 'dp', 'tp'), may hold values from -0.09375 to 0.09375
- log_step: float32 [2, 128], P(None, 'tp'), may hold values from -4.6 to -0.7
- eig_re: float32 [2, 128, 64], P(None, 'tp'), may hold values from -2 to -0.05
- eig_im: float32 [2, 128, 64], P(None, 'tp'), may hold values from 0 to 8
- in_mat: float32 [2, 2, 128, 64, 16], P(None, None, 'tp'), may hold values from -2.5 to 2.5
- output_matrices: float32 [2, 2, 128, 16, 64], P(None, None, 'tp'), may hold values from -1.25 to 1.25
- skip: float32 [2, 2048], P(None, 'tp'), may hold values from -4 to 4
- w_glu: bfloat16 [2, 2048, 4096], P(None, 'tp', 'dp'), may hold values from -0.375 to 0.375
- w_gate: bfloat16 [2, 2048, 4096], P(None, 'tp', 'dp'), may hold values from -0.125 to 0.125
- state: float32 [2, 2, 64, 8192], P(None, None, 'dp', 'tp'), may hold values from -6 to 6
Outputs:
- mixed: bfloat16 [64, 4096], P(None, 'dp')
- new_state: float32 [2, 2, 64, 8192], P(None, None, 'dp', 'tp')
Inputs may be any that keep to these rules, and one draw needn't show every extreme that they name: `lengths`: each sequence's number of past positions; the largest is exactly 4096 and all add up to 65536.
All inputs are finite; a program needn't handle non-finite values.
Results may differ from a plain program's by a relative error of at most 0.0095.
Values may be sent and summed in bfloat16 or wider, within the bound.
No kernel may reach another device: no remote copies, remote signals or barrier semaphores. Data moves between devices by JAX's collectives and lax.ppermute only.
A program may use at most 64 MiB of HBM per device.

v0:
```python
import functools
import math

import jax
import jax.numpy as jnp
from jax import lax
from jax.experimental import pallas as pl
from jax.experimental.pallas import tpu as pltpu
from jax.sharding import PartitionSpec as P


BLOCK_LEN = 256
LEN_MAX = 4096
NORM_EPS = 1e-06
F32 = jnp.float32
BF16 = jnp.bfloat16


def position_factor(lengths):
    blocks = (lengths // BLOCK_LEN).astype(F32)
    return 2.0 / (1.0 + blocks * (4.0 * BLOCK_LEN / LEN_MAX))


def exchange(value, axis, size, stride, count, k):
    pairs = []
    for i in range(size):
        digit = (i // stride) % count
        pairs.append((i, i + ((digit ^ k) - digit) * stride))
    return lax.ppermute(value, axis, pairs)


def params(mib=16):
    return pltpu.CompilerParams(vmem_limit_bytes=mib << 20)


VMEM = pl.BlockSpec(memory_space=pltpu.VMEM)
ANY = pl.BlockSpec(memory_space=pl.ANY)
HBM = pl.BlockSpec(memory_space=pltpu.HBM)


def struct(shape, dtype):
    return jax.ShapeDtypeStruct(shape, dtype)


def nt_dot(a, b):
    return lax.dot_general(a, b, (((1,), (1,)), ((), ())), preferred_element_type=F32)


def digits(inner):
    index = lax.axis_index("tp")
    return index % inner, index // inner


def corner():
    index = lax.axis_index("tp")
    return index % 4, (index // 4) % 2, index // 8


def placed_pieces(pieces, chunk):
    low, near, _ = corner()
    for k in range(4):
        for j in range(2):
            for far in range(2):
                at = ((2 * far + (near ^ j)) * 4 + (low ^ k)) * chunk
                yield pl.multiple_of(at, chunk), pieces[k][j, far]


def iota(shape, axis):
    return lax.broadcasted_iota(jnp.int32, shape, axis)


def exact_dot(a, b):
    return jnp.dot(a, b, precision=lax.Precision.HIGHEST, preferred_element_type=F32)


def prepare_kernel(count, *refs):
    lengths_ref, step_ref, re_ref, im_ref, in_ref, out_ref = refs[:6]
    stacks, (coeff_ref, m_ref, n_ref) = refs[6 : 6 + count], refs[6 + count : 9 + count]
    copies = [
        pltpu.make_async_copy(stacks[i].at[1], refs[9 + count + i], refs[-1].at[i])
        for i in range(count)
    ]
    for copy in copies:
        copy.start()
    layers, groups, states = re_ref.shape
    total, width = coeff_ref.shape[3], n_ref.shape[2]
    group = width // groups
    own = lengths_ref.shape[1]
    row = jnp.broadcast_to(position_factor(lengths_ref[...]), (own, own))
    factor = jnp.sum(
        jnp.where(iota((own, own), 0) == iota((own, own), 1), row, 0.0), axis=1, keepdims=True
    )
    spread = (iota((states, total), 1) % states == iota((states, total), 0)).astype(F32)
    spread_half = spread.astype(BF16)
    of_group = iota((groups, total), 1) // states == iota((groups, total), 0)
    keep = iota((width, total), 0) // group == iota((width, total), 1) // states

    def flat(value):
        return jnp.sum(
            jnp.where(of_group, exact_dot(value, spread), 0.0), axis=0, keepdims=True
        )

    for layer in range(layers):
        log_step = exact_dot(step_ref[layer : layer + 1, :], of_group.astype(F32))
        eig_re = flat(re_ref[layer])
        eig_im = flat(im_ref[layer])
        step_size = jnp.exp(log_step) * factor
        magnitude = jnp.exp(eig_re * step_size)
        turned = eig_im * step_size
        decay_re = magnitude * jnp.cos(turned)
        decay_im = magnitude * jnp.sin(turned)
        scale = 1.0 / (eig_re * eig_re + eig_im * eig_im)
        coeff_ref[layer, 0] = decay_re
        coeff_ref[layer, 1] = decay_im
        coeff_ref[layer, 2] = ((decay_re - 1.0) * eig_re + decay_im * eig_im) * scale
        coeff_ref[layer, 3] = (decay_im * eig_re - (decay_re - 1.0) * eig_im) * scale
        for part in range(2):
            for source, target in ((in_ref, m_ref), (out_ref, n_ref)):
                value = jnp.dot(
                    source[layer, part].astype(BF16), spread_half, preferred_element_type=F32
                )
                if part == 1 and target is n_ref:
                    value = -value
                target[layer, part] = jnp.where(keep, value, 0.0).astype(BF16)
    for copy in copies:
        copy.wait()


def prepare(own, lengths, log_step, eig_re, eig_im, in_rows, out_rows, stacks):
    layers, groups, states = eig_re.shape
    total, width = groups * states, in_rows.shape[2]
    outs = [
        struct((layers, 4, own, total), F32),
        struct((layers, 2, width, total), BF16),
        struct((layers, 2, width, total), BF16),
    ] + [pltpu.VMEM(a.shape[1:], a.dtype) for a in stacks]
    args = [lengths, log_step, eig_re, eig_im, in_rows, out_rows]
    specs = [VMEM] * len(args) + [HBM] * len(stacks)
    args += [pltpu.with_memory_space_constraint(a, pltpu.HBM) for a in stacks]
    made = pl.pallas_call(
        functools.partial(prepare_kernel, len(stacks)),
        in_specs=specs,
        out_specs=[VMEM] * len(outs),
        out_shape=outs,
        scratch_shapes=[pltpu.SemaphoreType.DMA((len(stacks),))],
        compiler_params=params(4),
        cost_estimate=pl.CostEstimate(flops=8 << 20, bytes_accessed=3 << 20, transcendentals=0),
        name="prepare",
    )(*args)
    return made[:3], made[3:]


def project_kernel(count, *refs):
    tokens_hbm, gain_hbm, weight_hbm = refs[:3]
    sources, (keep, send), targets = refs[3 : 3 + count], refs[3 + count : 5 + count], refs[5 + count : -4]
    tokens, gain, weight, sems = refs[-4:]
    pairs = [(tokens_hbm, tokens), (gain_hbm, gain), (weight_hbm.at[0], weight)]
    pairs += [(a.at[0] if len(a.shape) > len(b.shape) else a, b) for a, b in zip(sources, targets)]
    copies = [pltpu.make_async_copy(a, b, sems.at[i]) for i, (a, b) in enumerate(pairs)]
    for copy in copies:
        copy.start()
    own, width = keep.shape[0], weight.shape[1]
    chunk = tokens.shape[1] // 16
    copies[0].wait()
    copies[1].wait()
    current = tokens[...].astype(F32)
    squares = jnp.sum(current * current, axis=1, keepdims=True)
    scaled = (current * gain[0:1, :]).astype(BF16)
    copies[2].wait()
    term = jnp.dot(scaled, weight[...], preferred_element_type=F32)
    low, near, _ = corner()
    me = lax.axis_index("dp")
    for out, flip in ((keep, me), (send, 1 - me)):
        upper = flip == 1
        out[:, :width] = jnp.where(upper, term[own:], term[:own])
        out[:, width : width + 128] = jnp.broadcast_to(
            jnp.where(upper, squares[own:], squares[:own]), (own, 128)
        )
        start = pl.multiple_of(flip * own, own)
        for far in range(2):
            at = pl.multiple_of(((2 * far + near) * 4 + low) * chunk, chunk)
            base = width + 128 + far * chunk
            out[:, base : base + chunk] = tokens[pl.ds(start, own), pl.ds(at, chunk)].astype(F32)
    for copy in copies[3:]:
        copy.wait()


def project(dims, tokens, gain, weight, others, stacks):
    _, _, _, _, own, feats = dims
    width = weight.shape[2]
    shape = (own, width + 128 + 2 * feats // 16)
    args = [pltpu.with_memory_space_constraint(a, pltpu.HBM) for a in (tokens, gain, weight, *others, *stacks)]
    made = pl.pallas_call(
        functools.partial(project_kernel, len(others) + len(stacks)),
        in_specs=[HBM] * len(args),
        out_specs=[VMEM] * (2 + len(others) + len(stacks)),
        out_shape=[struct(shape, F32)] * 2 + [pltpu.VMEM(a.shape, a.dtype) for a in others]
        + [pltpu.VMEM(a.shape[1:], a.dtype) for a in stacks],
        scratch_shapes=[
            pltpu.VMEM(tokens.shape, BF16),
            pltpu.VMEM(gain.shape, F32),
            pltpu.VMEM(weight.shape[1:], BF16),
            pltpu.SemaphoreType.DMA((len(args),)),
        ],
        compiler_params=params(4),
        cost_estimate=pl.CostEstimate(flops=32 << 20, bytes_accessed=1 << 20, transcendentals=0),
        name="project",
    )(*args)
    return made[0], made[1], made[2 : 2 + len(others)], made[2 + len(others) :]


def recur_kernel(layer, dp, model, n_pieces, *refs):
    coeff_ref, m_ref, n_ref, skip_ref, state_ref = refs[:5]
    pieces = refs[5 : 5 + n_pieces]
    line, new_ref, sem = refs[-3:]
    own, feats = line.shape[1:]
    width = skip_ref.shape[1]
    chunk = feats // 16
    if layer == 0:
        readout_ref, state_out, before_ref = refs[-6:-3]
        partial_value = pieces[0][:, :width] + pieces[1][:, :width]
        squares = (pieces[0][:, width : width + 128] + pieces[1][:, width : width + 128])[:, :1]
        for far in range(2):
            for p in range(dp):
                base = width + 128 + far * chunk
                before_ref[far, :, p * chunk : (p + 1) * chunk] = pieces[p][
                    :, base : base + chunk
                ].astype(BF16)
    else:
        readout_ref, state_out = refs[-5:-3]
        gains = refs[5 + n_pieces : 5 + n_pieces + dp]
        weights = refs[5 + n_pieces + dp : 5 + n_pieces + 2 * dp]
        for at, piece in placed_pieces(pieces, chunk):
            for p in range(dp):
                line[p, :, pl.ds(at, chunk)] = piece[:, p * chunk : (p + 1) * chunk]
        squares = jnp.zeros((own, 1), F32)
        partial_value = None
        for p in range(dp):
            current = line[p].astype(F32)
            squares = squares + jnp.sum(current * current, axis=1, keepdims=True)
            scaled = (current * gains[p][layer : layer + 1, :]).astype(BF16)
            term = jnp.dot(scaled, weights[p][...], preferred_element_type=F32)
            partial_value = term if partial_value is None else partial_value + term
    driven = (partial_value * lax.rsqrt(squares / model + NORM_EPS)).astype(BF16)
    drive_re = jnp.dot(driven, m_ref[layer, 0], preferred_element_type=F32)
    drive_im = jnp.dot(driven, m_ref[layer, 1], preferred_element_type=F32)
    decay_re, decay_im = coeff_ref[layer, 0], coeff_ref[layer, 1]
    weight_re, weight_im = coeff_ref[layer, 2], coeff_ref[layer, 3]
    old_re, old_im = state_ref[layer, 0], state_ref[layer, 1]
    new_re = decay_re * old_re - decay_im * old_im + weight_re * drive_re - weight_im * drive_im
    new_im = decay_re * old_im + decay_im * old_re + weight_re * drive_im + weight_im * drive_re
    new_ref[0] = new_re
    new_ref[1] = new_im
    copy = pltpu.make_async_copy(new_ref, state_out.at[layer], sem)
    copy.start()
    value = nt_dot(new_re.astype(BF16), n_ref[layer, 0])
    value = value + nt_dot(new_im.astype(BF16), n_ref[layer, 1])
    value = value + skip_ref[layer : layer + 1, :] * driven.astype(F32)
    readout_ref[...] = jax.nn.gelu(value).astype(BF16)
    copy.wait()


def recur(layer, dims, consts, pieces, slabs, so_far):
    dp, _, _, model, own, feats = dims
    skip, state = consts[3:]
    args = [*consts, *pieces, *slabs]
    specs = [VMEM] * len(args)
    outs = [struct((own, skip.shape[1]), BF16), struct(state.shape, F32)]
    out_specs = [VMEM, ANY]
    alias = {}
    if layer == 0:
        outs.append(struct((2, own, dp * feats // 16), BF16))
        out_specs.append(VMEM)
    else:
        alias = {len(args): 1}
        args.append(so_far)
        specs.append(ANY)
    return pl.pallas_call(
        functools.partial(recur_kernel, layer, dp, model, len(pieces)),
        in_specs=specs,
        out_specs=out_specs,
        out_shape=outs,
        scratch_shapes=[
            pltpu.VMEM((dp, own, feats), BF16),
            pltpu.VMEM(state.shape[1:], F32),
            pltpu.SemaphoreType.DMA,
        ],
        input_output_aliases=alias,
        compiler_params=params(8),
        cost_estimate=pl.CostEstimate(flops=64 << 20, bytes_accessed=2 << 20, transcendentals=0),
    )(*args)


def product_kernel(chunk, readout_ref, *refs):
    weights, outs, spread = refs[:-5], refs[-5:-1], refs[-1]
    count = len(weights)
    low, _, _ = corner()
    readout = readout_ref[...]
    for w in range(count):
        value = jnp.dot(readout, weights[w][...], preferred_element_type=F32)
        for j in range(16):
            spread[w, j] = value[:, j * chunk : (j + 1) * chunk]
    for k in range(4):
        for h in range(4):
            for w in range(count):
                outs[k][h, :, w * chunk : (w + 1) * chunk] = spread[w, h * 4 + (low ^ k)].astype(
                    outs[k].dtype
                )


def call(kernel, args, outs, scratch=(), mib=4):
    return pl.pallas_call(
        kernel,
        in_specs=[VMEM] * len(args),
        out_specs=[VMEM] * len(outs),
        out_shape=outs,
        scratch_shapes=scratch,
        compiler_params=params(mib),
        cost_estimate=pl.CostEstimate(flops=1 << 22, bytes_accessed=1 << 20, transcendentals=0),
    )(*args)


def products(dims, readout, weights):
    _, _, _, _, own, feats = dims
    chunk = feats // 16
    shape = (4, own, len(weights) * chunk)
    return call(
        functools.partial(product_kernel, chunk),
        (readout, *weights),
        [struct(shape, F32)] + [struct(shape, BF16)] * 3,
        [pltpu.VMEM((len(weights), 16, own, chunk), F32)],
        8,
    )


def fold_low_kernel(own_ref, a_ref, b_ref, c_ref, keep, send):
    _, near, _ = corner()
    for far in range(2):
        for out, turn in ((keep, 0), (send, 1)):
            at = 2 * far + (near ^ turn)
            total = own_ref[at] + a_ref[at].astype(F32) + b_ref[at].astype(F32)
            out[far] = (total + c_ref[at].astype(F32)).astype(out.dtype)


def fold_near_kernel(own_ref, arrived_ref, send):
    send[...] = (own_ref[...] + arrived_ref[...].astype(F32)).astype(BF16)


def updated(own_ref, arrived_ref, before_ref):
    total = own_ref[...].astype(F32) + arrived_ref[...].astype(F32)
    half = total.shape[2] // 2
    linear, gate = total[:, :, :half], total[:, :, half:]
    return (before_ref[...].astype(F32) + linear * jax.nn.sigmoid(gate)).astype(BF16)


def update_kernel(own_ref, arrived_ref, before_ref, out):
    out[...] = updated(own_ref, arrived_ref, before_ref)


def last_update_kernel(own_ref, arrived_ref, before_ref, keep, send):
    value = updated(own_ref, arrived_ref, before_ref)
    half = value.shape[2] // 2
    keep[...] = value[:, :, :half]
    send[...] = value[:, :, half:]


def merge_kernel(own_ref, arrived_ref, out):
    rows = own_ref.shape[1]
    me = lax.axis_index("dp")
    out[:, pl.ds(pl.multiple_of(me * rows, rows), rows), :] = own_ref[...]
    out[:, pl.ds(pl.multiple_of((1 - me) * rows, rows), rows), :] = arrived_ref[...]


def settle_kernel(chunk, *refs):
    pieces, out, sem = refs[:4], refs[4], refs[5]
    copies = []
    for i, (at, _) in enumerate(placed_pieces(pieces, chunk)):
        source = pieces[i // 4].at[(i // 2) % 2, i % 2]
        copies.append(pltpu.make_async_copy(source, out.at[:, pl.ds(at, chunk)], sem.at[i]))
        copies[-1].start()
    for copy in copies:
        copy.wait()


def settle(pieces, feats):
    rows, chunk = pieces[0].shape[2:]
    return pl.pallas_call(
        functools.partial(settle_kernel, chunk),
        in_specs=[VMEM] * 4,
        out_specs=ANY,
        out_shape=struct((rows, feats), BF16),
        scratch_shapes=[pltpu.SemaphoreType.DMA((16,))],
        compiler_params=params(4),
        name="settle",
    )(*pieces)


def plain_prepare(lengths, log_step, eig_re, eig_im, in_mat, output_matrices):
    factor = position_factor(lengths)
    step_size = jnp.exp(log_step)[:, None, :, None] * factor[None, :, None, None]
    eig_re, eig_im = eig_re[:, None], eig_im[:, None]
    magnitude = jnp.exp(eig_re * step_size)
    turned = eig_im * step_size
    decay_re = magnitude * jnp.cos(turned)
    decay_im = magnitude * jnp.sin(turned)
    modulus = eig_re * eig_re + eig_im * eig_im
    weight_re = ((decay_re - 1.0) * eig_re + decay_im * eig_im) / modulus
    weight_im = (decay_im * eig_re - (decay_re - 1.0) * eig_im) / modulus
    return jnp.stack([decay_re, decay_im, weight_re, weight_im], axis=1), in_mat, output_matrices


def plain_order(pieces, inner, outer):
    low, high = digits(inner)
    rows = []
    for h in range(outer):
        for l in range(inner):
            row = jnp.stack(pieces)[low ^ l, high ^ h]
            rows.append(row)
    return jnp.stack(rows)


def plain_recur(layer, dims, pieces, gains, weights, coeff, m, n, skip, state, so_far):
    dp, inner, outer, model, own, feats = dims
    groups, states = coeff.shape[3:]
    if layer > 0:
        rows = plain_order(pieces, inner, outer)
        rows = rows.reshape(inner * outer, own, dp, feats // (inner * outer))
        pieces = [rows[:, :, p].transpose(1, 0, 2).reshape(own, feats) for p in range(dp)]
    else:
        start = lax.axis_index("dp") * own
        pieces = [lax.dynamic_slice_in_dim(p, start, own, axis=0) for p in pieces]
    squares, partial_value = 0.0, 0.0
    for p in range(dp):
        current = pieces[p].astype(F32)
        squares = squares + jnp.sum(current * current, axis=1, keepdims=True)
        scaled = (current * gains[p][layer]).astype(BF16)
        partial_value = partial_value + jnp.dot(
            scaled, weights[p][layer], preferred_element_type=F32
        )
    driven = (partial_value * lax.rsqrt(squares / model + NORM_EPS)).astype(BF16).astype(F32)
    driven = driven.reshape(own, groups, -1)
    exact = lax.Precision.HIGHEST
    drive_re = jnp.einsum("bgc,gpc->bgp", driven, m[layer, 0], precision=exact)
    drive_im = jnp.einsum("bgc,gpc->bgp", driven, m[layer, 1], precision=exact)
    decay_re, decay_im, weight_re, weight_im = [coeff[layer, c] for c in range(4)]
    old_re, old_im = [state[layer, c].reshape(own, groups, states) for c in range(2)]
    new_re = decay_re * old_re - decay_im * old_im + weight_re * drive_re - weight_im * drive_im
    new_im = decay_re * old_im + decay_im * old_re + weight_re * drive_im + weight_im * drive_re
    value = jnp.einsum("bgp,gcp->bgc", new_re, n[layer, 0], precision=exact)
    value = value - jnp.einsum("bgp,gcp->bgc", new_im, n[layer, 1], precision=exact)
    value = value + skip[layer].reshape(groups, -1) * driven
    readout = jax.nn.gelu(value).reshape(own, -1).astype(BF16)
    new = jnp.stack([new_re, new_im]).reshape(1, 2, own, groups * states)
    if layer > 0:
        return readout, jnp.concatenate([so_far, new])
    chunk = feats // (inner * outer)
    start = lax.axis_index("tp") * chunk
    cuts = [lax.dynamic_slice_in_dim(p, start, chunk, axis=1) for p in pieces]
    return readout, new, jnp.concatenate(cuts, axis=1)


def plain_products(layer, dims, readout, weights):
    _, inner, outer, _, own, _ = dims
    terms = []
    for w in weights:
        term = jnp.dot(readout, w[layer], preferred_element_type=F32)
        terms.append(term.reshape(own, outer, inner, -1))
    terms = jnp.concatenate(terms, axis=3).transpose(2, 1, 0, 3)
    low, _ = digits(inner)
    outs = [terms[low ^ k] for k in range(inner)]
    return [outs[0]] + [o.astype(BF16) for o in outs[1:]]


def plain_fold(value, arrived):
    for a in arrived:
        value = value + a.astype(F32)
    _, high = digits(len(arrived) + 1)
    outs = [value[high ^ k] for k in range(value.shape[0])]
    return [outs[0]] + [o.astype(BF16) for o in outs[1:]]


def plain_update(block, arrived, before):
    for a in arrived:
        block = block + a.astype(F32)
    half = block.shape[1] // 2
    gated = block[:, :half] * jax.nn.sigmoid(block[:, half:])
    return (before.astype(F32) + gated).astype(BF16)


def plain_settle(pieces, feats):
    rows = plain_order(pieces, len(pieces), pieces[0].shape[0])
    return rows.transpose(1, 0, 2).reshape(rows.shape[1], feats)


def plain_layers(dims, layers, pieces, slabs_of, pointwise):
    dp, inner, outer, _, own, feats = dims
    gain_slabs, in_slabs, out_slabs = slabs_of
    lengths, log_step, eig_re, eig_im, in_mat, output_matrices, skip, state = pointwise
    tp = inner * outer
    chunk = feats // tp

    def over_low(value, k):
        return exchange(value, "tp", tp, 1, inner, k)

    def over_high(value, k):
        return exchange(value, "tp", tp, inner, outer, k)

    coeff, m, n = plain_prepare(lengths, log_step, eig_re, eig_im, in_mat, output_matrices)
    new_state = None
    for layer in range(layers):
        made = plain_recur(
            layer, dims, pieces, gain_slabs, in_slabs, coeff, m, n, skip, state, new_state
        )
        readout, new_state = made[:2]
        if layer == 0:
            before = made[2]
        sends = plain_products(layer, dims, readout, out_slabs)
        arrived = [over_low(sends[k], k) for k in range(1, inner)]
        sends = plain_fold(sends[0], arrived)
        arrived = [over_high(sends[k], k) for k in range(1, outer)]
        shard = plain_update(sends[0], arrived, before)
        before = shard
        if layer + 1 == layers:
            cuts = [shard[:, k * chunk : (k + 1) * chunk] for k in range(dp)]
            here = [cuts[0]] + [exchange(cuts[k], "dp", dp, 1, dp, k) for k in range(1, dp)]
            order = lax.axis_index("dp") ^ jnp.arange(dp)
            shard = jnp.stack(here)[order].reshape(own * dp, chunk)
        column = jnp.stack([shard] + [over_high(shard, k) for k in range(1, outer)])
        pieces = [column] + [over_low(column, k) for k in range(1, inner)]
    return plain_settle(pieces, feats), new_state


def kernel_layers(dims, tokens, norm_gain, w_in, w_glu, w_gate, pointwise):
    dp, _, _, _, own, feats = dims
    lengths, log_step, eig_re, eig_im, in_mat, output_matrices, skip, state = pointwise
    layers = w_in.shape[0]
    chunk = feats // 16
    wide = 2 * dp * chunk

    def core_swap(value):
        return exchange(value, "dp", 2, 1, 2, 1)

    def over_low(value, k):
        return exchange(value, "tp", 16, 1, 4, k)

    def over_near(value):
        return exchange(value, "tp", 16, 4, 2, 1)

    def over_far(value):
        return exchange(value, "tp", 16, 8, 2, 1)

    width = skip.shape[1]
    others = (
        lengths[None, :],
        log_step,
        eig_re,
        eig_im,
        jnp.swapaxes(in_mat, 3, 4).reshape(layers, 2, width, -1),
        output_matrices.reshape(layers, 2, width, -1),
        skip,
        state,
    )
    keep, send, others, outward = project(
        dims, tokens, norm_gain, w_in, others, (w_glu, w_gate)
    )
    pieces = [keep, core_swap(send)]
    outward = [outward[0], core_swap(outward[0]), outward[1], core_swap(outward[1])]
    made, later = prepare(own, *others[:6], (w_in, w_glu, w_gate))
    consts = (*made, *others[6:])
    slabs = []
    new_state = None
    for layer in range(layers):
        made = recur(layer, dims, consts, pieces, slabs, new_state)
        readout, new_state = made[:2]
        if layer == 0:
            before = made[2]
        parts = products(dims, readout, outward)
        arrived = [over_low(parts[k], k) for k in range(1, 4)]
        if layer + 1 < layers:
            *later, gain, _ = lax.optimization_barrier((*later, norm_gain, parts[0]))
            slabs = [norm_gain, core_swap(gain), later[0], core_swap(later[0])]
            outward = [later[1], core_swap(later[1]), later[2], core_swap(later[2])]
        keep, send = call(
            fold_low_kernel,
            (parts[0], *arrived),
            [struct((2, own, wide), F32), struct((2, own, wide), BF16)],
        )
        (send,) = call(fold_near_kernel, (keep, over_near(send)), [struct((2, own, wide), BF16)])
        terms = (send, over_far(send), before)
        if layer + 1 < layers:
            (shard,) = call(update_kernel, terms, [struct((2, own, dp * chunk), BF16)])
            before = shard
        else:
            keep, send = call(last_update_kernel, terms, [struct((2, own, chunk), BF16)] * 2)
            (shard,) = call(
                merge_kernel, (keep, core_swap(send)), [struct((2, own * 2, chunk), BF16)]
            )
        column = jnp.stack([shard, over_near(shard)])
        pieces = [column] + [over_low(column, k) for k in range(1, 4)]
    return settle(pieces, feats), new_state


def make_body(tp, dp):
    inner = 1 << (int(math.log2(tp)) // 2)
    outer = tp // inner

    def body(
        tokens,
        lengths,
        norm_gain,
        w_in,
        log_step,
        eig_re,
        eig_im,
        in_mat,
        output_matrices,
        skip,
        w_glu,
        w_gate,
        state,
    ):
        layers = w_in.shape[0]
        seqs, feats = tokens.shape
        own = seqs // dp
        chunk = feats // tp
        dims = (dp, inner, outer, feats * dp, own, feats)
        pointwise = (lengths, log_step, eig_re, eig_im, in_mat, output_matrices, skip, state)
        regular = tp == 16 and dp == 2 and chunk % 128 == 0 and own % 16 == 0
        if regular and skip.shape[1] % 128 == 0:
            return kernel_layers(dims, tokens, norm_gain, w_in, w_glu, w_gate, pointwise)

        def slabs(value):
            return [value] + [exchange(value, "dp", dp, 1, dp, k) for k in range(1, dp)]

        slabs_of = (slabs(norm_gain), slabs(w_in), slabs(w_glu) + slabs(w_gate))
        return plain_layers(dims, layers, slabs(tokens), slabs_of, pointwise)

    return body


def solution(mesh):
    placed = (
        P(None, "dp"),
        P("dp"),
        P(None, "dp"),
        P(None, "dp", "tp"),
        P(None, "tp"),
        P(None, "tp", None),
        P(None, "tp", None),
        P(None, None, "tp", None, None),
        P(None, None, "tp", None, None),
        P(None, "tp"),
        P(None, "tp", "dp"),
        P(None, "tp", "dp"),
        P(None, None, "dp", "tp"),
    )
    return jax.shard_map(
        make_body(mesh.shape["tp"], mesh.shape["dp"]),
        mesh=mesh,
        in_specs=placed,
        out_specs=(P(None, "dp"), P(None, None, "dp", "tp")),
        check_vma=False,
    )
```

profile of v0, /device:TPU:0, one launch (start us, length us, event | category | flops | bytes accessed | tf_op | source)
XLA Modules:
  0.0 73.8 jit_solution(41675582063645325)
XLA Ops:
  0.6 1.9 %project.1 = (f32[32,512]{1,0:T(8,128)S(1)}, f32[32,512]{1,0:T(8,128)S(1)}, s32[1,32]{1,0:T(1,128)S(1)}, f32[2,8]{1,0:T(2,128)S(1)}, f32[2,8,64]{2,1,0:T(8,128)S...) custom-call(bf16[64,2048]{1,0:T(8,128)(2,1)} %refs_0_.1, ...), custom_call_target="tpu_custom_call" | custom-call | flops 33554432 | bytes 1048576 | tf_op jit(solution)/shard_map/project/pallas_call | solution.py:193
  2.5 0.6 collective-permute-start.1
  3.1 0.1 collective-permute-start.2
  3.2 0.4 collective-permute-start
  3.6 1.4 %prepare.1 = (f32[2,4,32,512]{3,2,1,0:T(8,128)S(1)}, bf16[2,2,128,512]{3,2,1,0:T(8,128)(2,1)S(1)}, bf16[2,2,128,512]{3,2,1,0:T(8,128)(2,1)S(1)}, bf16[2048,128]{...) custom-call(s32[1,32]{1,0:T(1,128)S(1)} %get-tuple-element.43.refs_0_, ...), custom_call_target="tpu_custom_call" | custom-call | flops 8388608 | bytes 3145728 | tf_op jit(solution)/shard_map/prepare/pallas_call | solution.py:140
  5.0 0.5 collective-permute-done.refs_6_
  5.5 0.9 %shard_map.140 = (bf16[32,128]{1,0:T(8,128)(2,1)S(1)}, f32[2,2,32,512]{3,2,1,0:T(8,128)}, bf16[2,32,256]{2,1,0:T(8,128)(2,1)S(1)}) custom-call(f32[2,4,32,512]{3,2,1,0:T(8,128)S(1)} %get-tuple-element.49.refs_0_, bf16[2,2,128,512]{3,2,1,0:T(8,128)(2,1)S(1)} %get-tuple-element.50.refs_1_, bf16[2,2,128,512]{3,2,1,0:T(8,128)(2,1)S(1)} %get-tuple-element.51.refs_2_, ...), custom_call_target="tpu_custom_call" | custom-call | flops 67108864 | bytes 2097152 | tf_op jit(solution)/shard_map/pallas_call | solution.py:278
  6.4 0.0 collective-permute-done.1.refs_1_
  6.4 0.0 collective-permute-done.2.refs_3_
  6.4 0.5 shard_map.141
  6.9 2.9 %collective-permute-start.3 = (bf16[4,32,512]{2,1,0:T(8,128)(2,1)S(1)}, bf16[4,32,512]{2,1,0:T(8,128)(2,1)S(1)}, u32[]{:S(2)}, u32[]{:S(2)}) collective-permute-start(bf16[4,32,512]{2,1,0:T(8,128)(2,1)S(1)} %get-tuple-element.60), channel_id=1, source_target_pairs={{0,2},{2,0},{4,6},{6,4},{8,10},{10,8},{12,14},{14,12},{16,18},{18,... | collective-permute-start | bytes 393224 | tf_op jit(solution)/shard_map/ppermute | solution.py:29
  9.8 1.5 %collective-permute-start.4 = (bf16[4,32,512]{2,1,0:T(8,128)(2,1)S(1)}, bf16[4,32,512]{2,1,0:T(8,128)(2,1)S(1)}, u32[]{:S(2)}, u32[]{:S(2)}) collective-permute-start(bf16[4,32,512]{2,1,0:T(8,128)(2,1)S(1)} %get-tuple-element.61), channel_id=1, source_target_pairs={{0,4},{2,6},{4,0},{6,2},{8,12},{10,14},{12,8},{14,10},{16,20},{18,... | collective-permute-start | bytes 393224 | tf_op jit(solution)/shard_map/ppermute | solution.py:29
  11.3 0.0 collective-permute-start.5
  11.4 0.0 collective-permute-start.13
  11.4 0.5 collective-permute-start.14
  11.9 1.9 %collective-permute-done.3.a_ref = bf16[4,32,512]{2,1,0:T(8,128)(2,1)S(1)} collective-permute-done((bf16[4,32,512]{2,1,0:T(8,128)(2,1)S(1)}, bf16[4,32,512]{2,1,0:T(8,128)(2,1)S(1)}, u32[]{:S(2)}, u32[]{:S(2)}) %collective-permute-start.3) | collective-permute-done | bytes 131104 | tf_op jit(solution)/shard_map/ppermute | solution.py:29
  13.8 0.0 collective-permute-start.15
  13.8 4.1 %collective-permute-done.4.b_ref = bf16[4,32,512]{2,1,0:T(8,128)(2,1)S(1)} collective-permute-done((bf16[4,32,512]{2,1,0:T(8,128)(2,1)S(1)}, bf16[4,32,512]{2,1,0:T(8,128)(2,1)S(1)}, u32[]{:S(2)}, u32[]{:S(2)}) %collective-permute-start.4) | collective-permute-done | bytes 131104 | tf_op jit(solution)/shard_map/ppermute | solution.py:29
  17.9 0.0 collective-permute-done.5.c_ref
  17.9 0.1 shard_map.142
  18.0 1.6 %collective-permute-start.6 = (bf16[2,32,512]{2,1,0:T(8,128)(2,1)S(1)}, bf16[2,32,512]{2,1,0:T(8,128)(2,1)S(1)}, u32[]{:S(2)}, u32[]{:S(2)}) collective-permute-start(bf16[2,32,512]{2,1,0:T(8,128)(2,1)S(1)} %get-tuple-element.64), channel_id=1, source_target_pairs={{0,8},{2,10},{4,12},{6,14},{8,0},{10,2},{12,4},{14,6},{16,24},{18,... | collective-permute-start | bytes 196616 | tf_op jit(solution)/shard_map/ppermute | solution.py:29
  19.6 2.7 %collective-permute-done.6.arrived_ref = bf16[2,32,512]{2,1,0:T(8,128)(2,1)S(1)} collective-permute-done((bf16[2,32,512]{2,1,0:T(8,128)(2,1)S(1)}, bf16[2,32,512]{2,1,0:T(8,128)(2,1)S(1)}, u32[]{:S(2)}, u32[]{:S(2)}) %collective-permute-start.6) | collective-permute-done | bytes 65568 | tf_op jit(solution)/shard_map/ppermute | solution.py:29
  22.3 2.7 %collective-permute-start.7 = (bf16[2,32,512]{2,1,0:T(8,128)(2,1)S(1)}, bf16[2,32,512]{2,1,0:T(8,128)(2,1)S(1)}, u32[]{:S(2)}, u32[]{:S(2)}) collective-permute-start(bf16[2,32,512]{2,1,0:T(8,128)(2,1)S(1)} %shard_map.143.own_ref), channel_id=1, source_target_pairs={{0,16},{2,18},{4,20},{6,22},{8,24},{10,26},{12,28},{14,30},{16,0},... | collective-permute-start | bytes 196616 | tf_op jit(solution)/shard_map/ppermute | solution.py:29
  25.0 2.6 %collective-permute-done.7.arrived_ref = bf16[2,32,512]{2,1,0:T(8,128)(2,1)S(1)} collective-permute-done((bf16[2,32,512]{2,1,0:T(8,128)(2,1)S(1)}, bf16[2,32,512]{2,1,0:T(8,128)(2,1)S(1)}, u32[]{:S(2)}, u32[]{:S(2)}) %collective-permute-start.7) | collective-permute-done | bytes 65568 | tf_op jit(solution)/shard_map/ppermute | solution.py:29
  27.6 1.6 %collective-permute-start.8 = (bf16[2,32,256]{2,1,0:T(8,128)(2,1)S(1)}, bf16[2,32,256]{2,1,0:T(8,128)(2,1)S(1)}, u32[]{:S(2)}, u32[]{:S(2)}) collective-permute-start(bf16[2,32,256]{2,1,0:T(8,128)(2,1)S(1)} %shard_map.144.before_ref), channel_id=1, source_target_pairs={{0,8},{2,10},{4,12},{6,14},{8,0},{10,2},{12,4},{14,6},{16,24},{18,... | collective-permute-start | bytes 98312 | tf_op jit(solution)/shard_map/ppermute | solution.py:29
  29.2 2.4 %collective-permute-done.8 = bf16[2,32,256]{2,1,0:T(8,128)(2,1)S(1)} collective-permute-done((bf16[2,32,256]{2,1,0:T(8,128)(2,1)S(1)}, bf16[2,32,256]{2,1,0:T(8,128)(2,1)S(1)}, u32[]{:S(2)}, u32[]{:S(2)}) %collective-permute-start.8) | collective-permute-done | bytes 32800 | tf_op jit(solution)/shard_map/ppermute | solution.py:29
  31.6 0.0 copy-start
  31.6 1.5 %collective-permute-start.11 = (bf16[2,2,32,256]{3,2,1,0:T(8,128)(2,1)S(1)}, bf16[2,2,32,256]{3,2,1,0:T(8,128)(2,1)S(1)}, u32[]{:S(2)}, u32[]{:S(2)}) collective-permute-start(bf16[2,2,32,256]{3,2,1,0:T(8,128)(2,1)S(1)} %pad_maximum_fusion.refs_5_), channel_id=1, source_target_pairs={{0,6},{2,4},{4,2},{6,0},{8,14},{10,12},{12,10},{14,8},{16,22},{18,... | collective-permute-start | bytes 196616 | tf_op jit(solution)/shard_map/ppermute | solution.py:29
  33.2 0.0 copy-done
  33.2 0.0 collective-permute-start.12
  33.2 1.2 %collective-permute-done.12.refs_10_ = f32[2,2048]{1,0:T(2,128)S(1)} collective-permute-done((f32[2,2048]{1,0:T(2,128)S(1)}, f32[2,2048]{1,0:T(2,128)S(1)}, u32[]{:S(2)}, u32[]{:S(2)}) %collective-permute-start.12) | collective-permute-done | bytes 16416 | tf_op jit(solution)/shard_map/ppermute | solution.py:29
  34.4 1.2 %collective-permute-start.10 = (bf16[2,2,32,256]{3,2,1,0:T(8,128)(2,1)S(1)}, bf16[2,2,32,256]{3,2,1,0:T(8,128)(2,1)S(1)}, u32[]{:S(2)}, u32[]{:S(2)}) collective-permute-start(bf16[2,2,32,256]{3,2,1,0:T(8,128)(2,1)S(1)} %pad_maximum_fusion.refs_5_), channel_id=1, source_target_pairs={{0,4},{2,6},{4,0},{6,2},{8,12},{10,14},{12,8},{14,10},{16,20},{18,... | collective-permute-start | bytes 196616 | tf_op jit(solution)/shard_map/ppermute | solution.py:29
  35.5 1.3 %collective-permute-done.11.refs_8_ = bf16[2,2,32,256]{3,2,1,0:T(8,128)(2,1)S(1)} collective-permute-done((bf16[2,2,32,256]{3,2,1,0:T(8,128)(2,1)S(1)}, bf16[2,2,32,256]{3,2,1,0:T(8,128)(2,1)S(1)}, u32[]{:S(2)}, u32[]{:S(2)}) %collective-permute-start.11) | collective-permute-done | bytes 65568 | tf_op jit(solution)/shard_map/ppermute | solution.py:29
  36.9 1.2 %collective-permute-start.9 = (bf16[2,2,32,256]{3,2,1,0:T(8,128)(2,1)S(1)}, bf16[2,2,32,256]{3,2,1,0:T(8,128)(2,1)S(1)}, u32[]{:S(2)}, u32[]{:S(2)}) collective-permute-start(bf16[2,2,32,256]{3,2,1,0:T(8,128)(2,1)S(1)} %pad_maximum_fusion.refs_5_), channel_id=1, source_target_pairs={{0,2},{2,0},{4,6},{6,4},{8,10},{10,8},{12,14},{14,12},{16,18},{18,... | collective-permute-start | bytes 196616 | tf_op jit(solution)/shard_map/ppermute | solution.py:29
  38.1 0.6 collective-permute-done.10.refs_7_
  38.6 2.5 %collective-permute-done.9.refs_6_ = bf16[2,2,32,256]{3,2,1,0:T(8,128)(2,1)S(1)} collective-permute-done((bf16[2,2,32,256]{3,2,1,0:T(8,128)(2,1)S(1)}, bf16[2,2,32,256]{3,2,1,0:T(8,128)(2,1)S(1)}, u32[]{:S(2)}, u32[]{:S(2)}) %collective-permute-start.9) | collective-permute-done | bytes 65568 | tf_op jit(solution)/shard_map/ppermute | solution.py:29
  41.1 0.0 collective-permute-done.13.refs_12_
  41.1 1.2 %shard_map.145 = (bf16[32,128]{1,0:T(8,128)(2,1)S(1)}, f32[2,2,32,512]{3,2,1,0:T(8,128)}) custom-call(f32[2,4,32,512]{3,2,1,0:T(8,128)S(1)} %get-tuple-element.49.refs_0_, bf16[2,2,128,512]{3,2,1,0:T(8,128)(2,1)S(1)} %get-tuple-element.50.refs_1_, bf16[2,2,128,512]{3,2,1,0:T(8,128)(2,1)S(1)} %get-tuple-element.51.refs_2_, ...), custom_call_target="tpu_custom_call", output_to_operand_aliasing={{1}: (13, {})} | custom-call | flops 67108864 | bytes 2097152 | tf_op jit(solution)/shard_map/pallas_call | solution.py:278
  42.3 0.0 collective-permute-done.14.refs_1_
  42.3 0.0 collective-permute-done.15.refs_3_
  42.3 0.5 shard_map.146
  42.8 1.3 %collective-permute-start.16 = (bf16[4,32,512]{2,1,0:T(8,128)(2,1)S(1)}, bf16[4,32,512]{2,1,0:T(8,128)(2,1)S(1)}, u32[]{:S(2)}, u32[]{:S(2)}) collective-permute-start(bf16[4,32,512]{2,1,0:T(8,128)(2,1)S(1)} %get-tuple-element.76), channel_id=1, source_target_pairs={{0,2},{2,0},{4,6},{6,4},{8,10},{10,8},{12,14},{14,12},{16,18},{18,... | collective-permute-start | bytes 393224 | tf_op jit(solution)/shard_map/ppermute | solution.py:29
  44.1 0.9 %collective-permute-start.17 = (bf16[4,32,512]{2,1,0:T(8,128)(2,1)S(1)}, bf16[4,32,512]{2,1,0:T(8,128)(2,1)S(1)}, u32[]{:S(2)}, u32[]{:S(2)}) collective-permute-start(bf16[4,32,512]{2,1,0:T(8,128)(2,1)S(1)} %get-tuple-element.77), channel_id=1, source_target_pairs={{0,4},{2,6},{4,0},{6,2},{8,12},{10,14},{12,8},{14,10},{16,20},{18,... | collective-permute-start | bytes 393224 | tf_op jit(solution)/shard_map/ppermute | solution.py:29
  44.9 1.4 %collective-permute-start.18 = (bf16[4,32,512]{2,1,0:T(8,128)(2,1)S(1)}, bf16[4,32,512]{2,1,0:T(8,128)(2,1)S(1)}, u32[]{:S(2)}, u32[]{:S(2)}) collective-permute-start(bf16[4,32,512]{2,1,0:T(8,128)(2,1)S(1)} %get-tuple-element.78), channel_id=1, source_target_pairs={{0,6},{2,4},{4,2},{6,0},{8,14},{10,12},{12,10},{14,8},{16,22},{18,... | collective-permute-start | bytes 393224 | tf_op jit(solution)/shard_map/ppermute | solution.py:29
  46.4 1.5 %collective-permute-done.16.a_ref = bf16[4,32,512]{2,1,0:T(8,128)(2,1)S(1)} collective-permute-done((bf16[4,32,512]{2,1,0:T(8,128)(2,1)S(1)}, bf16[4,32,512]{2,1,0:T(8,128)(2,1)S(1)}, u32[]{:S(2)}, u32[]{:S(2)}) %collective-permute-start.16) | collective-permute-done | bytes 131104 | tf_op jit(solution)/shard_map/ppermute | solution.py:29
  47.9 1.2 %collective-permute-done.17.b_ref = bf16[4,32,512]{2,1,0:T(8,128)(2,1)S(1)} collective-permute-done((bf16[4,32,512]{2,1,0:T(8,128)(2,1)S(1)}, bf16[4,32,512]{2,1,0:T(8,128)(2,1)S(1)}, u32[]{:S(2)}, u32[]{:S(2)}) %collective-permute-start.17) | collective-permute-done | bytes 131104 | tf_op jit(solution)/shard_map/ppermute | solution.py:29
  49.1 1.8 %collective-permute-done.18.c_ref = bf16[4,32,512]{2,1,0:T(8,128)(2,1)S(1)} collective-permute-done((bf16[4,32,512]{2,1,0:T(8,128)(2,1)S(1)}, bf16[4,32,512]{2,1,0:T(8,128)(2,1)S(1)}, u32[]{:S(2)}, u32[]{:S(2)}) %collective-permute-start.18) | collective-permute-done | bytes 131104 | tf_op jit(solution)/shard_map/ppermute | solution.py:29
  50.8 0.1 shard_map.147
  50.9 1.6 %collective-permute-start.19 = (bf16[2,32,512]{2,1,0:T(8,128)(2,1)S(1)}, bf16[2,32,512]{2,1,0:T(8,128)(2,1)S(1)}, u32[]{:S(2)}, u32[]{:S(2)}) collective-permute-start(bf16[2,32,512]{2,1,0:T(8,128)(2,1)S(1)} %get-tuple-element.80), channel_id=1, source_target_pairs={{0,8},{2,10},{4,12},{6,14},{8,0},{10,2},{12,4},{14,6},{16,24},{18,... | collective-permute-start | bytes 196616 | tf_op jit(solution)/shard_map/ppermute | solution.py:29
  52.5 3.2 %collective-permute-done.19.arrived_ref = bf16[2,32,512]{2,1,0:T(8,128)(2,1)S(1)} collective-permute-done((bf16[2,32,512]{2,1,0:T(8,128)(2,1)S(1)}, bf16[2,32,512]{2,1,0:T(8,128)(2,1)S(1)}, u32[]{:S(2)}, u32[]{:S(2)}) %collective-permute-start.19) | collective-permute-done | bytes 65568 | tf_op jit(solution)/shard_map/ppermute | solution.py:29
  55.7 2.6 %collective-permute-start.20 = (bf16[2,32,512]{2,1,0:T(8,128)(2,1)S(1)}, bf16[2,32,512]{2,1,0:T(8,128)(2,1)S(1)}, u32[]{:S(2)}, u32[]{:S(2)}) collective-permute-start(bf16[2,32,512]{2,1,0:T(8,128)(2,1)S(1)} %shard_map.148.own_ref), channel_id=1, source_target_pairs={{0,16},{2,18},{4,20},{6,22},{8,24},{10,26},{12,28},{14,30},{16,0},... | collective-permute-start | bytes 196616 | tf_op jit(solution)/shard_map/ppermute | solution.py:29
  58.3 2.7 %collective-permute-done.20.arrived_ref = bf16[2,32,512]{2,1,0:T(8,128)(2,1)S(1)} collective-permute-done((bf16[2,32,512]{2,1,0:T(8,128)(2,1)S(1)}, bf16[2,32,512]{2,1,0:T(8,128)(2,1)S(1)}, u32[]{:S(2)}, u32[]{:S(2)}) %collective-permute-start.20) | collective-permute-done | bytes 65568 | tf_op jit(solution)/shard_map/ppermute | solution.py:29
  61.0 0.1 collective-permute-start.21
  61.0 1.2 %collective-permute-done.21.arrived_ref = bf16[2,32,128]{2,1,0:T(8,128)(2,1)S(1)} collective-permute-done((bf16[2,32,128]{2,1,0:T(8,128)(2,1)S(1)}, bf16[2,32,128]{2,1,0:T(8,128)(2,1)S(1)}, u32[]{:S(2)}, u32[]{:S(2)}) %collective-permute-start.21) | collective-permute-done | bytes 16416 | tf_op jit(solution)/shard_map/ppermute | solution.py:29
  62.2 1.7 %collective-permute-start.22 = (bf16[2,64,128]{2,1,0:T(8,128)(2,1)S(1)}, bf16[2,64,128]{2,1,0:T(8,128)(2,1)S(1)}, u32[]{:S(2)}, u32[]{:S(2)}) collective-permute-start(bf16[2,64,128]{2,1,0:T(8,128)(2,1)S(1)} %shard_map.150), channel_id=1, source_target_pairs={{0,8},{2,10},{4,12},{6,14},{8,0},{10,2},{12,4},{14,6},{16,24},{18,... | collective-permute-start | bytes 98312 | tf_op jit(solution)/shard_map/ppermute | solution.py:29
  63.9 2.2 %collective-permute-done.22 = bf16[2,64,128]{2,1,0:T(8,128)(2,1)S(1)} collective-permute-done((bf16[2,64,128]{2,1,0:T(8,128)(2,1)S(1)}, bf16[2,64,128]{2,1,0:T(8,128)(2,1)S(1)}, u32[]{:S(2)}, u32[]{:S(2)}) %collective-permute-start.22) | collective-permute-done | bytes 32800 | tf_op jit(solution)/shard_map/ppermute | solution.py:29
  66.1 1.4 %collective-permute-start.25 = (bf16[2,2,64,128]{3,2,1,0:T(8,128)(2,1)S(1)}, bf16[2,2,64,128]{3,2,1,0:T(8,128)(2,1)S(1)}, u32[]{:S(2)}, u32[]{:S(2)}) collective-permute-start(bf16[2,2,64,128]{3,2,1,0:T(8,128)(2,1)S(1)} %pad_maximum_fusion.1.refs_0_), channel_id=1, source_target_pairs={{0,6},{2,4},{4,2},{6,0},{8,14},{10,12},{12,10},{14,8},{16,22},{18,... | collective-permute-start | bytes 196616 | tf_op jit(solution)/shard_map/ppermute | solution.py:29
  67.5 1.2 %collective-permute-start.24 = (bf16[2,2,64,128]{3,2,1,0:T(8,128)(2,1)S(1)}, bf16[2,2,64,128]{3,2,1,0:T(8,128)(2,1)S(1)}, u32[]{:S(2)}, u32[]{:S(2)}) collective-permute-start(bf16[2,2,64,128]{3,2,1,0:T(8,128)(2,1)S(1)} %pad_maximum_fusion.1.refs_0_), channel_id=1, source_target_pairs={{0,4},{2,6},{4,0},{6,2},{8,12},{10,14},{12,8},{14,10},{16,20},{18,... | collective-permute-start | bytes 196616 | tf_op jit(solution)/shard_map/ppermute | solution.py:29
  68.8 0.9 %collective-permute-start.23 = (bf16[2,2,64,128]{3,2,1,0:T(8,128)(2,1)S(1)}, bf16[2,2,64,128]{3,2,1,0:T(8,128)(2,1)S(1)}, u32[]{:S(2)}, u32[]{:S(2)}) collective-permute-start(bf16[2,2,64,128]{3,2,1,0:T(8,128)(2,1)S(1)} %pad_maximum_fusion.1.refs_0_), channel_id=1, source_target_pairs={{0,2},{2,0},{4,6},{6,4},{8,10},{10,8},{12,14},{14,12},{16,18},{18,... | collective-permute-start | bytes 196616 | tf_op jit(solution)/shard_map/ppermute | solution.py:29
  69.7 1.9 %collective-permute-done.25.refs_3_ = bf16[2,2,64,128]{3,2,1,0:T(8,128)(2,1)S(1)} collective-permute-done((bf16[2,2,64,128]{3,2,1,0:T(8,128)(2,1)S(1)}, bf16[2,2,64,128]{3,2,1,0:T(8,128)(2,1)S(1)}, u32[]{:S(2)}, u32[]{:S(2)}) %collective-permute-start.25) | collective-permute-done | bytes 65568 | tf_op jit(solution)/shard_map/ppermute | solution.py:29
  71.6 0.7 collective-permute-done.24.refs_2_
  72.2 0.8 %collective-permute-done.23.refs_1_ = bf16[2,2,64,128]{3,2,1,0:T(8,128)(2,1)S(1)} collective-permute-done((bf16[2,2,64,128]{3,2,1,0:T(8,128)(2,1)S(1)}, bf16[2,2,64,128]{3,2,1,0:T(8,128)(2,1)S(1)}, u32[]{:S(2)}, u32[]{:S(2)}) %collective-permute-start.23) | collective-permute-done | bytes 65568 | tf_op jit(solution)/shard_map/ppermute | solution.py:29
  73.0 0.8 %settle.1 = bf16[64,2048]{1,0:T(8,128)(2,1)} custom-call(bf16[2,2,64,128]{3,2,1,0:T(8,128)(2,1)S(1)} %pad_maximum_fusion.1.refs_0_, bf16[2,2,64,128]{3,2,1,0:T(8,128)(2,1)S(1)} %collective-permute-done.23.refs_1_, bf16[2,2,64,128]{3,2,1,0:T(8,128)(2,1)S(1)} %collective-permute-done.24.refs_2_, bf16[2,2,64,128]{3,2,1,0:T(8,128)(2,1)S(1)} %collective-permute-done.25.refs_3_), custom_call_target="tpu_custom_call" | custom-call | tf_op jit(solution)/shard_map/settle/pallas_call | solution.py:387
  (7 shorter events, 0.1 us)
Async XLA Ops:
  2.5 3.9 %collective-permute-start.1 = (bf16[128,2048]{1,0:T(8,128)(2,1)S(1)}, bf16[128,2048]{1,0:T(8,128)(2,1)S(1)}, u32[]{:S(2)}, u32[]{:S(2)}) collective-permute-start(bf16[128,2048]{1,0:T(8,128)(2,1)S(1)} %get-tuple-element.57.refs_0_), channel_id=1, source_target_pairs={{0,1},{1,0},{2,3},{3,2},{4,5},{5,4},{6,7},{7,6},{8,9},{9,8},{10,11... | collective-permute-start | bytes 1572872 | tf_op jit(solution)/shard_map/ppermute | solution.py:29
  3.1 3.3 %collective-permute-start.2 = (bf16[128,2048]{1,0:T(8,128)(2,1)S(1)}, bf16[128,2048]{1,0:T(8,128)(2,1)S(1)}, u32[]{:S(2)}, u32[]{:S(2)}) collective-permute-start(bf16[128,2048]{1,0:T(8,128)(2,1)S(1)} %get-tuple-element.58.refs_2_), channel_id=1, source_target_pairs={{0,1},{1,0},{2,3},{3,2},{4,5},{5,4},{6,7},{7,6},{8,9},{9,8},{10,11... | collective-permute-start | bytes 1572872 | tf_op jit(solution)/shard_map/ppermute | solution.py:29
  3.2 2.3 %collective-permute-start = (f32[32,512]{1,0:T(8,128)S(1)}, f32[32,512]{1,0:T(8,128)S(1)}, u32[]{:S(2)}, u32[]{:S(2)}) collective-permute-start(f32[32,512]{1,0:T(8,128)S(1)} %get-tuple-element.55), channel_id=1, source_target_pairs={{0,1},{1,0},{2,3},{3,2},{4,5},{5,4},{6,7},{7,6},{8,9},{9,8},{10,11... | collective-permute-start | bytes 196616 | tf_op jit(solution)/shard_map/ppermute | solution.py:29
  6.9 6.9 %collective-permute-start.3 = (bf16[4,32,512]{2,1,0:T(8,128)(2,1)S(1)}, bf16[4,32,512]{2,1,0:T(8,128)(2,1)S(1)}, u32[]{:S(2)}, u32[]{:S(2)}) collective-permute-start(bf16[4,32,512]{2,1,0:T(8,128)(2,1)S(1)} %get-tuple-element.60), channel_id=1, source_target_pairs={{0,2},{2,0},{4,6},{6,4},{8,10},{10,8},{12,14},{14,12},{16,18},{18,... | collective-permute-start | bytes 393224 | tf_op jit(solution)/shard_map/ppermute | solution.py:29
  9.8 8.1 %collective-permute-start.4 = (bf16[4,32,512]{2,1,0:T(8,128)(2,1)S(1)}, bf16[4,32,512]{2,1,0:T(8,128)(2,1)S(1)}, u32[]{:S(2)}, u32[]{:S(2)}) collective-permute-start(bf16[4,32,512]{2,1,0:T(8,128)(2,1)S(1)} %get-tuple-element.61), channel_id=1, source_target_pairs={{0,4},{2,6},{4,0},{6,2},{8,12},{10,14},{12,8},{14,10},{16,20},{18,... | collective-permute-start | bytes 393224 | tf_op jit(solution)/shard_map/ppermute | solution.py:29
  11.3 6.6 %collective-permute-start.5 = (bf16[4,32,512]{2,1,0:T(8,128)(2,1)S(1)}, bf16[4,32,512]{2,1,0:T(8,128)(2,1)S(1)}, u32[]{:S(2)}, u32[]{:S(2)}) collective-permute-start(bf16[4,32,512]{2,1,0:T(8,128)(2,1)S(1)} %get-tuple-element.62), channel_id=1, source_target_pairs={{0,6},{2,4},{4,2},{6,0},{8,14},{10,12},{12,10},{14,8},{16,22},{18,... | collective-permute-start | bytes 393224 | tf_op jit(solution)/shard_map/ppermute | solution.py:29
  11.4 29.8 %collective-permute-start.13 = (bf16[2048,128]{1,0:T(8,128)(2,1)S(1)}, bf16[2048,128]{1,0:T(8,128)(2,1)S(1)}, u32[]{:S(2)}, u32[]{:S(2)}) collective-permute-start(bf16[2048,128]{1,0:T(8,128)(2,1)S(1)} %get-tuple-element.70.refs_11_), channel_id=1, source_target_pairs={{0,1},{1,0},{2,3},{3,2},{4,5},{5,4},{6,7},{7,6},{8,9},{9,8},{10,11... | collective-permute-start | bytes 1572872 | tf_op jit(solution)/shard_map/ppermute | solution.py:29
  11.4 31.0 %collective-permute-start.14 = (bf16[128,2048]{1,0:T(8,128)(2,1)S(1)}, bf16[128,2048]{1,0:T(8,128)(2,1)S(1)}, u32[]{:S(2)}, u32[]{:S(2)}) collective-permute-start(bf16[128,2048]{1,0:T(8,128)(2,1)S(1)} %get-tuple-element.73.refs_0_), channel_id=1, source_target_pairs={{0,1},{1,0},{2,3},{3,2},{4,5},{5,4},{6,7},{7,6},{8,9},{9,8},{10,11... | collective-permute-start | bytes 1572872 | tf_op jit(solution)/shard_map/ppermute | solution.py:29
  13.8 28.6 %collective-permute-start.15 = (bf16[128,2048]{1,0:T(8,128)(2,1)S(1)}, bf16[128,2048]{1,0:T(8,128)(2,1)S(1)}, u32[]{:S(2)}, u32[]{:S(2)}) collective-permute-start(bf16[128,2048]{1,0:T(8,128)(2,1)S(1)} %get-tuple-element.74.refs_2_), channel_id=1, source_target_pairs={{0,1},{1,0},{2,3},{3,2},{4,5},{5,4},{6,7},{7,6},{8,9},{9,8},{10,11... | collective-permute-start | bytes 1572872 | tf_op jit(solution)/shard_map/ppermute | solution.py:29
  18.0 4.3 %collective-permute-start.6 = (bf16[2,32,512]{2,1,0:T(8,128)(2,1)S(1)}, bf16[2,32,512]{2,1,0:T(8,128)(2,1)S(1)}, u32[]{:S(2)}, u32[]{:S(2)}) collective-permute-start(bf16[2,32,512]{2,1,0:T(8,128)(2,1)S(1)} %get-tuple-element.64), channel_id=1, source_target_pairs={{0,8},{2,10},{4,12},{6,14},{8,0},{10,2},{12,4},{14,6},{16,24},{18,... | collective-permute-start | bytes 196616 | tf_op jit(solution)/shard_map/ppermute | solution.py:29
  22.3 5.3 %collective-permute-start.7 = (bf16[2,32,512]{2,1,0:T(8,128)(2,1)S(1)}, bf16[2,32,512]{2,1,0:T(8,128)(2,1)S(1)}, u32[]{:S(2)}, u32[]{:S(2)}) collective-permute-start(bf16[2,32,512]{2,1,0:T(8,128)(2,1)S(1)} %shard_map.143.own_ref), channel_id=1, source_target_pairs={{0,16},{2,18},{4,20},{6,22},{8,24},{10,26},{12,28},{14,30},{16,0},... | collective-permute-start | bytes 196616 | tf_op jit(solution)/shard_map/ppermute | solution.py:29
  27.6 4.0 %collective-permute-start.8 = (bf16[2,32,256]{2,1,0:T(8,128)(2,1)S(1)}, bf16[2,32,256]{2,1,0:T(8,128)(2,1)S(1)}, u32[]{:S(2)}, u32[]{:S(2)}) collective-permute-start(bf16[2,32,256]{2,1,0:T(8,128)(2,1)S(1)} %shard_map.144.before_ref), channel_id=1, source_target_pairs={{0,8},{2,10},{4,12},{6,14},{8,0},{10,2},{12,4},{14,6},{16,24},{18,... | collective-permute-start | bytes 98312 | tf_op jit(solution)/shard_map/ppermute | solution.py:29
  31.6 1.6 %copy-start = (f32[2,2048]{1,0:T(2,128)S(1)}, f32[2,2048]{1,0:T(2,128)}, u32[]{:S(2)}) copy-start(f32[2,2048]{1,0:T(2,128)} %refs_9_.3) | copy-start | bytes 49156
  31.6 5.2 %collective-permute-start.11 = (bf16[2,2,32,256]{3,2,1,0:T(8,128)(2,1)S(1)}, bf16[2,2,32,256]{3,2,1,0:T(8,128)(2,1)S(1)}, u32[]{:S(2)}, u32[]{:S(2)}) collective-permute-start(bf16[2,2,32,256]{3,2,1,0:T(8,128)(2,1)S(1)} %pad_maximum_fusion.refs_5_), channel_id=1, source_target_pairs={{0,6},{2,4},{4,2},{6,0},{8,14},{10,12},{12,10},{14,8},{16,22},{18,... | collective-permute-start | bytes 196616 | tf_op jit(solution)/shard_map/ppermute | solution.py:29
  33.2 1.2 %collective-permute-start.12 = (f32[2,2048]{1,0:T(2,128)S(1)}, f32[2,2048]{1,0:T(2,128)S(1)}, u32[]{:S(2)}, u32[]{:S(2)}) collective-permute-start(f32[2,2048]{1,0:T(2,128)S(1)} %copy-done), channel_id=1, source_target_pairs={{0,1},{1,0},{2,3},{3,2},{4,5},{5,4},{6,7},{7,6},{8,9},{9,8},{10,11... | collective-permute-start | bytes 49160 | tf_op jit(solution)/shard_map/ppermute | solution.py:29
  34.4 4.3 %collective-permute-start.10 = (bf16[2,2,32,256]{3,2,1,0:T(8,128)(2,1)S(1)}, bf16[2,2,32,256]{3,2,1,0:T(8,128)(2,1)S(1)}, u32[]{:S(2)}, u32[]{:S(2)}) collective-permute-start(bf16[2,2,32,256]{3,2,1,0:T(8,128)(2,1)S(1)} %pad_maximum_fusion.refs_5_), channel_id=1, source_target_pairs={{0,4},{2,6},{4,0},{6,2},{8,12},{10,14},{12,8},{14,10},{16,20},{18,... | collective-permute-start | bytes 196616 | tf_op jit(solution)/shard_map/ppermute | solution.py:29
  36.9 4.3 %collective-permute-start.9 = (bf16[2,2,32,256]{3,2,1,0:T(8,128)(2,1)S(1)}, bf16[2,2,32,256]{3,2,1,0:T(8,128)(2,1)S(1)}, u32[]{:S(2)}, u32[]{:S(2)}) collective-permute-start(bf16[2,2,32,256]{3,2,1,0:T(8,128)(2,1)S(1)} %pad_maximum_fusion.refs_5_), channel_id=1, source_target_pairs={{0,2},{2,0},{4,6},{6,4},{8,10},{10,8},{12,14},{14,12},{16,18},{18,... | collective-permute-start | bytes 196616 | tf_op jit(solution)/shard_map/ppermute | solution.py:29
  42.8 5.0 %collective-permute-start.16 = (bf16[4,32,512]{2,1,0:T(8,128)(2,1)S(1)}, bf16[4,32,512]{2,1,0:T(8,128)(2,1)S(1)}, u32[]{:S(2)}, u32[]{:S(2)}) collective-permute-start(bf16[4,32,512]{2,1,0:T(8,128)(2,1)S(1)} %get-tuple-element.76), channel_id=1, source_target_pairs={{0,2},{2,0},{4,6},{6,4},{8,10},{10,8},{12,14},{14,12},{16,18},{18,... | collective-permute-start | bytes 393224 | tf_op jit(solution)/shard_map/ppermute | solution.py:29
  44.1 5.0 %collective-permute-start.17 = (bf16[4,32,512]{2,1,0:T(8,128)(2,1)S(1)}, bf16[4,32,512]{2,1,0:T(8,128)(2,1)S(1)}, u32[]{:S(2)}, u32[]{:S(2)}) collective-permute-start(bf16[4,32,512]{2,1,0:T(8,128)(2,1)S(1)} %get-tuple-element.77), channel_id=1, source_target_pairs={{0,4},{2,6},{4,0},{6,2},{8,12},{10,14},{12,8},{14,10},{16,20},{18,... | collective-permute-start | bytes 393224 | tf_op jit(solution)/shard_map/ppermute | solution.py:29
  44.9 5.9 %collective-permute-start.18 = (bf16[4,32,512]{2,1,0:T(8,128)(2,1)S(1)}, bf16[4,32,512]{2,1,0:T(8,128)(2,1)S(1)}, u32[]{:S(2)}, u32[]{:S(2)}) collective-permute-start(bf16[4,32,512]{2,1,0:T(8,128)(2,1)S(1)} %get-tuple-element.78), channel_id=1, source_target_pairs={{0,6},{2,4},{4,2},{6,0},{8,14},{10,12},{12,10},{14,8},{16,22},{18,... | collective-permute-start | bytes 393224 | tf_op jit(solution)/shard_map/ppermute | solution.py:29
  50.9 4.8 %collective-permute-start.19 = (bf16[2,32,512]{2,1,0:T(8,128)(2,1)S(1)}, bf16[2,32,512]{2,1,0:T(8,128)(2,1)S(1)}, u32[]{:S(2)}, u32[]{:S(2)}) collective-permute-start(bf16[2,32,512]{2,1,0:T(8,128)(2,1)S(1)} %get-tuple-element.80), channel_id=1, source_target_pairs={{0,8},{2,10},{4,12},{6,14},{8,0},{10,2},{12,4},{14,6},{16,24},{18,... | collective-permute-start | bytes 196616 | tf_op jit(solution)/shard_map/ppermute | solution.py:29
  55.7 5.2 %collective-permute-start.20 = (bf16[2,32,512]{2,1,0:T(8,128)(2,1)S(1)}, bf16[2,32,512]{2,1,0:T(8,128)(2,1)S(1)}, u32[]{:S(2)}, u32[]{:S(2)}) collective-permute-start(bf16[2,32,512]{2,1,0:T(8,128)(2,1)S(1)} %shard_map.148.own_ref), channel_id=1, source_target_pairs={{0,16},{2,18},{4,20},{6,22},{8,24},{10,26},{12,28},{14,30},{16,0},... | collective-permute-start | bytes 196616 | tf_op jit(solution)/shard_map/ppermute | solution.py:29
  61.0 1.2 %collective-permute-start.21 = (bf16[2,32,128]{2,1,0:T(8,128)(2,1)S(1)}, bf16[2,32,128]{2,1,0:T(8,128)(2,1)S(1)}, u32[]{:S(2)}, u32[]{:S(2)}) collective-permute-start(bf16[2,32,128]{2,1,0:T(8,128)(2,1)S(1)} %get-tuple-element.82), channel_id=1, source_target_pairs={{0,1},{1,0},{2,3},{3,2},{4,5},{5,4},{6,7},{7,6},{8,9},{9,8},{10,11... | collective-permute-start | bytes 49160 | tf_op jit(solution)/shard_map/ppermute | solution.py:29
  62.2 3.9 %collective-permute-start.22 = (bf16[2,64,128]{2,1,0:T(8,128)(2,1)S(1)}, bf16[2,64,128]{2,1,0:T(8,128)(2,1)S(1)}, u32[]{:S(2)}, u32[]{:S(2)}) collective-permute-start(bf16[2,64,128]{2,1,0:T(8,128)(2,1)S(1)} %shard_map.150), channel_id=1, source_target_pairs={{0,8},{2,10},{4,12},{6,14},{8,0},{10,2},{12,4},{14,6},{16,24},{18,... | collective-permute-start | bytes 98312 | tf_op jit(solution)/shard_map/ppermute | solution.py:29
  66.1 5.4 %collective-permute-start.25 = (bf16[2,2,64,128]{3,2,1,0:T(8,128)(2,1)S(1)}, bf16[2,2,64,128]{3,2,1,0:T(8,128)(2,1)S(1)}, u32[]{:S(2)}, u32[]{:S(2)}) collective-permute-start(bf16[2,2,64,128]{3,2,1,0:T(8,128)(2,1)S(1)} %pad_maximum_fusion.1.refs_0_), channel_id=1, source_target_pairs={{0,6},{2,4},{4,2},{6,0},{8,14},{10,12},{12,10},{14,8},{16,22},{18,... | collective-permute-start | bytes 196616 | tf_op jit(solution)/shard_map/ppermute | solution.py:29
  67.5 4.7 %collective-permute-start.24 = (bf16[2,2,64,128]{3,2,1,0:T(8,128)(2,1)S(1)}, bf16[2,2,64,128]{3,2,1,0:T(8,128)(2,1)S(1)}, u32[]{:S(2)}, u32[]{:S(2)}) collective-permute-start(bf16[2,2,64,128]{3,2,1,0:T(8,128)(2,1)S(1)} %pad_maximum_fusion.1.refs_0_), channel_id=1, source_target_pairs={{0,4},{2,6},{4,0},{6,2},{8,12},{10,14},{12,8},{14,10},{16,20},{18,... | collective-permute-start | bytes 196616 | tf_op jit(solution)/shard_map/ppermute | solution.py:29
  68.8 4.3 %collective-permute-start.23 = (bf16[2,2,64,128]{3,2,1,0:T(8,128)(2,1)S(1)}, bf16[2,2,64,128]{3,2,1,0:T(8,128)(2,1)S(1)}, u32[]{:S(2)}, u32[]{:S(2)}) collective-permute-start(bf16[2,2,64,128]{3,2,1,0:T(8,128)(2,1)S(1)} %pad_maximum_fusion.1.refs_0_), channel_id=1, source_target_pairs={{0,2},{2,0},{4,6},{6,4},{8,10},{10,8},{12,14},{14,12},{16,18},{18,... | collective-permute-start | bytes 196616 | tf_op jit(solution)/shard_map/ppermute | solution.py:29
where the time goes:
time: 74 us; the launch traced here: 73.8 us
  waiting for transfers between devices  36.8 us (50%)
  starting transfers between devices  28.9 us (39%)
  Pallas kernels  7.37 us (10%)
  between operations  0.77 us (1%)
    ppermute x26, waiting for transfers between devices, exchange(): return lax.ppermute(value, axis, pairs)  36.8 us
    ppermute x26, starting transfers between devices, exchange(): return lax.ppermute(value, axis, pairs)  28.9 us
    pallas_call x2, Pallas kernels, recur(): pl.pallas_call(functools.partial(recur_kernel, layer, dp, model, len(piec...  2.08 us
    pallas_call x1, Pallas kernels, project(): pl.pallas_call(functools.partial(project_kernel, len(others) + len(stacks...  1.89 us
  transfers between devices with their start and end apart: 26, of which 20 were waited for; matrix products, arithmetic and copies ran while one was open for 0% of the time, Pallas kernels for 5%

commit v1 on v0

--- a/solution.py
+++ b/solution.py
@@ -49,6 +49,18 @@
 def digits(inner):
     index = lax.axis_index("tp")
     return index % inner, index // inner
+
+
+def call(kernel, args, outs, scratch=(), mib=4):
+    return pl.pallas_call(
+        kernel,
+        in_specs=[VMEM] * len(args),
+        out_specs=[VMEM] * len(outs),
+        out_shape=outs,
+        scratch_shapes=scratch,
+        compiler_params=params(mib),
+        cost_estimate=pl.CostEstimate(flops=1 << 22, bytes_accessed=1 << 20, transcendentals=0),
+    )(*args)
 
 
 def corner():
@@ -73,15 +85,9 @@
     return jnp.dot(a, b, precision=lax.Precision.HIGHEST, preferred_element_type=F32)
 
 
-def prepare_kernel(count, *refs):
-    lengths_ref, step_ref, re_ref, im_ref, in_ref, out_ref = refs[:6]
-    stacks, (coeff_ref, m_ref, n_ref) = refs[6 : 6 + count], refs[6 + count : 9 + count]
-    copies = [
-        pltpu.make_async_copy(stacks[i].at[1], refs[9 + count + i], refs[-1].at[i])
-        for i in range(count)
-    ]
-    for copy in copies:
-        copy.start()
+def prepare_kernel(
+    lengths_ref, step_ref, re_ref, im_ref, in_ref, out_ref, coeff_ref, m_ref, n_ref
+):
     layers, groups, states = re_ref.shape
     total, width = coeff_ref.shape[3], n_ref.shape[2]
     group = width // groups
@@ -122,32 +128,56 @@
                 if part == 1 and target is n_ref:
                     value = -value
                 target[layer, part] = jnp.where(keep, value, 0.0).astype(BF16)
-    for copy in copies:
-        copy.wait()
-
-
-def prepare(own, lengths, log_step, eig_re, eig_im, in_rows, out_rows, stacks):
+
+
+def prepare(own, lengths, log_step, eig_re, eig_im, in_rows, out_rows):
     layers, groups, states = eig_re.shape
     total, width = groups * states, in_rows.shape[2]
     outs = [
         struct((layers, 4, own, total), F32),
         struct((layers, 2, width, total), BF16),
         struct((layers, 2, width, total), BF16),
-    ] + [pltpu.VMEM(a.shape[1:], a.dtype) for a in stacks]
-    args = [lengths, log_step, eig_re, eig_im, in_rows, out_rows]
-    specs = [VMEM] * len(args) + [HBM] * len(stacks)
-    args += [pltpu.with_memory_space_constraint(a, pltpu.HBM) for a in stacks]
-    made = pl.pallas_call(
-        functools.partial(prepare_kernel, len(stacks)),
-        in_specs=specs,
-        out_specs=[VMEM] * len(outs),
+    ]
+    args = (lengths, log_step, eig_re, eig_im, in_rows, out_rows)
+    return call(prepare_kernel, args, outs)
+
+
+def pack_kernel(in_hbm, glu_hbm, gate_hbm, in_out, *refs):
+    packs, sem, sems = refs[:4], refs[4], refs[5]
+    chunk = packs[0].shape[1] // 8
+    low, _, _ = corner()
+    copies = [pltpu.make_async_copy(in_hbm.at[1], in_out, sem)]
+    for k in range(4):
+        for w, source in enumerate((glu_hbm, gate_hbm)):
+            for h in range(4):
+                at = pl.multiple_of((h * 4 + (low ^ k)) * chunk, chunk)
+                copies.append(
+                    pltpu.make_async_copy(
+                        source.at[1, :, pl.ds(at, chunk)],
+                        packs[k].at[:, (w * 4 + h) * chunk : (w * 4 + h + 1) * chunk],
+                        sems.at[k, w, h],
+                    )
+                )
+    for copy in copies:
+        copy.start()
+    for copy in copies:
+        copy.wait()
+
+
+def pack(w_in, w_glu, w_gate):
+    width, chunk = w_glu.shape[1], w_glu.shape[2] // 16
+    args = [pltpu.with_memory_space_constraint(a, pltpu.HBM) for a in (w_in, w_glu, w_gate)]
+    outs = [pltpu.VMEM(w_in.shape[1:], BF16)] + [pltpu.VMEM((width, 8 * chunk), BF16)] * 4
+    return pl.pallas_call(
+        pack_kernel,
+        in_specs=[HBM] * 3,
+        out_specs=[VMEM] * 5,
         out_shape=outs,
-        scratch_shapes=[pltpu.SemaphoreType.DMA((len(stacks),))],
+        scratch_shapes=[pltpu.SemaphoreType.DMA, pltpu.SemaphoreType.DMA((4, 2, 4))],
         compiler_params=params(4),
         cost_estimate=pl.CostEstimate(flops=8 << 20, bytes_accessed=3 << 20, transcendentals=0),
-        name="prepare",
+        name="pack",
     )(*args)
-    return made[:3], made[3:]
 
 
 def project_kernel(count, *refs):
@@ -308,18 +338,6 @@
                 )
 
 
-def call(kernel, args, outs, scratch=(), mib=4):
-    return pl.pallas_call(
-        kernel,
-        in_specs=[VMEM] * len(args),
-        out_specs=[VMEM] * len(outs),
-        out_shape=outs,
-        scratch_shapes=scratch,
-        compiler_params=params(mib),
-        cost_estimate=pl.CostEstimate(flops=1 << 22, bytes_accessed=1 << 20, transcendentals=0),
-    )(*args)
-
-
 def products(dims, readout, weights):
     _, _, _, _, own, feats = dims
     chunk = feats // 16
@@ -333,6 +351,34 @@
     )
 
 
+def gathered_kernel(chunk, *refs):
+    readouts, weights, (keep, send, spread) = refs[:4], refs[4:8], refs[8:]
+    _, near, _ = corner()
+    value = None
+    for k in range(4):
+        term = jnp.dot(readouts[k][...], weights[k][...], preferred_element_type=F32)
+        value = term if value is None else value + term
+    for j in range(8):
+        spread[j] = value[:, j * chunk : (j + 1) * chunk]
+    for far in range(2):
+        for w in range(2):
+            lanes = slice(w * chunk, (w + 1) * chunk)
+            at = w * 4 + 2 * far + near
+            keep[far, :, lanes] = spread[at]
+            send[far, :, lanes] = spread[w * 4 + 2 * far + (near ^ 1)].astype(BF16)
+
+
+def gathered_products(chunk, readouts, weights):
+    rows = readouts[0].shape[0]
+    return call(
+        functools.partial(gathered_kernel, chunk),
+        (*readouts, *weights),
+        [struct((2, rows, 2 * chunk), F32), struct((2, rows, 2 * chunk), BF16)],
+        [pltpu.VMEM((8, rows, chunk), F32)],
+        8,
+    )
+
+
 def fold_low_kernel(own_ref, a_ref, b_ref, c_ref, keep, send):
     _, near, _ = corner()
     for far in range(2):
@@ -357,17 +403,11 @@
     out[...] = updated(own_ref, arrived_ref, before_ref)
 
 
-def last_update_kernel(own_ref, arrived_ref, before_ref, keep, send):
-    value = updated(own_ref, arrived_ref, before_ref)
-    half = value.shape[2] // 2
-    keep[...] = value[:, :, :half]
-    send[...] = value[:, :, half:]
-
-
 def merge_kernel(own_ref, arrived_ref, out):
     rows = own_ref.shape[1]
     me = lax.axis_index("dp")
-    out[:, pl.ds(pl.multiple_of(me * rows, rows), rows), :] = own_ref[...]
+    half = out.shape[2]
+    out[:, pl.ds(pl.multiple_of(me * rows, rows), rows), :] = own_ref[:, :, :half]
     out[:, pl.ds(pl.multiple_of((1 - me) * rows, rows), rows), :] = arrived_ref[...]
 
 
@@ -565,38 +605,47 @@
     )
     pieces = [keep, core_swap(send)]
     outward = [outward[0], core_swap(outward[0]), outward[1], core_swap(outward[1])]
-    made, later = prepare(own, *others[:6], (w_in, w_glu, w_gate))
-    consts = (*made, *others[6:])
-    slabs = []
-    new_state = None
-    for layer in range(layers):
-        made = recur(layer, dims, consts, pieces, slabs, new_state)
-        readout, new_state = made[:2]
-        if layer == 0:
-            before = made[2]
-        parts = products(dims, readout, outward)
-        arrived = [over_low(parts[k], k) for k in range(1, 4)]
-        if layer + 1 < layers:
-            *later, gain, _ = lax.optimization_barrier((*later, norm_gain, parts[0]))
-            slabs = [norm_gain, core_swap(gain), later[0], core_swap(later[0])]
-            outward = [later[1], core_swap(later[1]), later[2], core_swap(later[2])]
-        keep, send = call(
-            fold_low_kernel,
-            (parts[0], *arrived),
-            [struct((2, own, wide), F32), struct((2, own, wide), BF16)],
-        )
-        (send,) = call(fold_near_kernel, (keep, over_near(send)), [struct((2, own, wide), BF16)])
-        terms = (send, over_far(send), before)
-        if layer + 1 < layers:
-            (shard,) = call(update_kernel, terms, [struct((2, own, dp * chunk), BF16)])
-            before = shard
-        else:
-            keep, send = call(last_update_kernel, terms, [struct((2, own, chunk), BF16)] * 2)
-            (shard,) = call(
-                merge_kernel, (keep, core_swap(send)), [struct((2, own * 2, chunk), BF16)]
-            )
-        column = jnp.stack([shard, over_near(shard)])
-        pieces = [column] + [over_low(column, k) for k in range(1, 4)]
+    consts = (*prepare(own, *others[:6]), *others[6:])
+
+    readout, new_state, before = recur(0, dims, consts, pieces, [], None)
+    parts = products(dims, readout, outward)
+    arrived = [over_low(parts[k], k) for k in range(1, 4)]
+    stacks = lax.optimization_barrier((w_in, w_glu, w_gate, norm_gain, parts[0]))
+    inward, *packs = pack(*stacks[:3])
+    gain = stacks[3]
+    slabs = [norm_gain, core_swap(gain), inward, core_swap(inward)]
+    keep, send = call(
+        fold_low_kernel,
+        (parts[0], *arrived),
+        [struct((2, own, wide), F32), struct((2, own, wide), BF16)],
+    )
+    arrived = over_near(send)
+    *packs, _ = lax.optimization_barrier((*packs, send))
+    weights = [packs[0]] + [over_low(packs[k], k) for k in range(1, 4)]
+    (send,) = call(fold_near_kernel, (keep, arrived), [struct((2, own, wide), BF16)])
+    terms = (send, over_far(send), before)
+    (shard,) = call(update_kernel, terms, [struct((2, own, dp * chunk), BF16)])
+    column = jnp.stack([shard, over_near(shard)])
+    pieces = [column] + [over_low(column, k) for k in range(1, 4)]
+    away, _ = lax.optimization_barrier((shard[:, :, chunk:], column))
+    away = core_swap(away)
+    (before,) = call(merge_kernel, (shard, away), [struct((2, own * dp, chunk), BF16)])
+
+    readout, new_state = recur(1, dims, consts, pieces, slabs, new_state)
+    readout = readout[None]
+    (rows,) = call(
+        merge_kernel, (readout, core_swap(readout)), [struct((1, own * dp, width), BF16)]
+    )
+    rows = rows[0]
+    readouts = [rows] + [over_low(rows, k) for k in range(1, 4)]
+    keep, send = gathered_products(chunk, readouts, weights)
+    (send,) = call(
+        fold_near_kernel, (keep, over_near(send)), [struct((2, own * dp, 2 * chunk), BF16)]
+    )
+    terms = (send, over_far(send), before)
+    (shard,) = call(update_kernel, terms, [struct((2, own * dp, chunk), BF16)])
+    column = jnp.stack([shard, over_near(shard)])
+    pieces = [column] + [over_low(column, k) for k in range(1, 4)]
     return settle(pieces, feats), new_state
 
 
@@ -625,7 +674,7 @@
         chunk = feats // tp
         dims = (dp, inner, outer, feats * dp, own, feats)
         pointwise = (lengths, log_step, eig_re, eig_im, in_mat, output_matrices, skip, state)
-        regular = tp == 16 and dp == 2 and chunk % 128 == 0 and own % 16 == 0
+        regular = tp == 16 and dp == 2 and layers == 2 and chunk % 128 == 0 and own % 16 == 0
         if regular and skip.shape[1] % 128 == 0:
             return kernel_layers(dims, tokens, norm_gain, w_in, w_glu, w_gate, pointwise)
 

time: 74 us -> 85.9 us (1.16)
  waiting for transfers between devices: 36.8 us -> 46.6 us
  Pallas kernels: 7.37 us -> 8.92 us
    ppermute x26 -> x28, waiting for transfers between devices: 36.8 us -> 46.6 us  [exchange(): return lax.ppermute(value, axis, pairs)]
    pallas_call x9 -> x10, Pallas kernels: 1.19 us -> 2.26 us  [call(): pl.pallas_call(kernel, in_specs=[VMEM] * len(args), out_specs=[VMEM] * le...]
    ppermute x26 -> x28, starting transfers between devices: 28.9 us -> 29.4 us  [exchange(): return lax.ppermute(value, axis, pairs)]
  transfers between devices with their start and end apart: 26 -> 28, of which waited for: 20 -> 20; matrix products, arithmetic and copies ran while one was open for 0% -> 0% of each run, Pallas kernels for 5% -> 6%
where the time goes in v1:
time: 85.9 us; the launch traced here: 85.7 us
  waiting for transfers between devices  46.6 us (54%)
  starting transfers between devices  29.4 us (34%)
  Pallas kernels  8.92 us (10%)
    ppermute x28, waiting for transfers between devices, exchange(): return lax.ppermute(value, axis, pairs)  46.6 us
    ppermute x28, starting transfers between devices, exchange(): return lax.ppermute(value, axis, pairs)  29.4 us
    pallas_call x10, Pallas kernels, call(): pl.pallas_call(kernel, in_specs=[VMEM] * len(args), out_specs=[VMEM] * le...  2.26 us
    pallas_call x2, Pallas kernels, recur(): pl.pallas_call(functools.partial(recur_kernel, layer, dp, model, len(piec...  2.09 us
    pallas_call x1, Pallas kernels, project(): pl.pallas_call(functools.partial(project_kernel, len(others) + len(stacks...  1.89 us
    pallas_call x1, Pallas kernels, pack(): pl.pallas_call(pack_kernel, in_specs=[HBM] * 3, out_specs=[VMEM] * 5, out...  1.86 us
  transfers between devices with their start and end apart: 28, of which 20 were waited for; matrix products, arithmetic and copies ran while one was open for 0% of the time, Pallas kernels for 6%

profile of v1, /device:TPU:0, one launch (start us, length us, event | category | flops | bytes accessed | tf_op | source)
XLA Modules:
  0.0 85.7 jit_solution(18274317586513845535)
XLA Ops:
  0.6 1.9 %project.1 = (f32[32,512]{1,0:T(8,128)S(1)}, f32[32,512]{1,0:T(8,128)S(1)}, s32[1,32]{1,0:T(1,128)S(1)}, f32[2,8]{1,0:T(2,128)S(1)}, f32[2,8,64]{2,1,0:T(8,128)S...) custom-call(bf16[64,2048]{1,0:T(8,128)(2,1)} %refs_0_.1, ...), custom_call_target="tpu_custom_call" | custom-call | flops 33554432 | bytes 1048576 | tf_op jit(solution)/shard_map/project/pallas_call | solution.py:223
  2.5 0.6 collective-permute-start.1
  3.1 0.1 collective-permute-start.2
  3.2 0.4 collective-permute-start
  3.6 1.3 %shard_map.140 = (f32[2,4,32,512]{3,2,1,0:T(8,128)S(1)}, bf16[2,2,128,512]{3,2,1,0:T(8,128)(2,1)S(1)}, bf16[2,2,128,512]{3,2,1,0:T(8,128)(2,1)S(1)}) custom-call(s32[1,32]{1,0:T(1,128)S(1)} %get-tuple-element.44.lengths_ref, f32[2,8]{1,0:T(2,128)S(1)} %get-tuple-element.45.step_ref, f32[2,8,64]{2,1,0:T(8,128)S(1)} %get-tuple-element.46.re_ref, ...), custom_call_target="tpu_custom_call" | custom-call | flops 4194304 | bytes 1048576 | tf_op jit(solution)/shard_map/pallas_call | solution.py:55
  4.9 0.6 collective-permute-done.refs_6_
  5.5 0.9 %shard_map.141 = (bf16[32,128]{1,0:T(8,128)(2,1)S(1)}, f32[2,2,32,512]{3,2,1,0:T(8,128)}, bf16[2,32,256]{2,1,0:T(8,128)(2,1)S(1)}) custom-call(f32[2,4,32,512]{3,2,1,0:T(8,128)S(1)} %get-tuple-element.50.refs_0_, bf16[2,2,128,512]{3,2,1,0:T(8,128)(2,1)S(1)} %get-tuple-element.51.refs_1_, bf16[2,2,128,512]{3,2,1,0:T(8,128)(2,1)S(1)} %get-tuple-element.52.refs_2_, ...), custom_call_target="tpu_custom_call" | custom-call | flops 67108864 | bytes 2097152 | tf_op jit(solution)/shard_map/pallas_call | solution.py:308
  6.4 0.0 collective-permute-done.1.refs_1_
  6.4 0.0 collective-permute-done.2.refs_3_
  6.4 0.5 shard_map.142
  6.9 2.9 %collective-permute-start.3 = (bf16[4,32,512]{2,1,0:T(8,128)(2,1)S(1)}, bf16[4,32,512]{2,1,0:T(8,128)(2,1)S(1)}, u32[]{:S(2)}, u32[]{:S(2)}) collective-permute-start(bf16[4,32,512]{2,1,0:T(8,128)(2,1)S(1)} %get-tuple-element.61), channel_id=1, source_target_pairs={{0,2},{2,0},{4,6},{6,4},{8,10},{10,8},{12,14},{14,12},{16,18},{18,... | collective-permute-start | bytes 393224 | tf_op jit(solution)/shard_map/ppermute | solution.py:29
  9.8 1.5 %collective-permute-start.4 = (bf16[4,32,512]{2,1,0:T(8,128)(2,1)S(1)}, bf16[4,32,512]{2,1,0:T(8,128)(2,1)S(1)}, u32[]{:S(2)}, u32[]{:S(2)}) collective-permute-start(bf16[4,32,512]{2,1,0:T(8,128)(2,1)S(1)} %get-tuple-element.62), channel_id=1, source_target_pairs={{0,4},{2,6},{4,0},{6,2},{8,12},{10,14},{12,8},{14,10},{16,20},{18,... | collective-permute-start | bytes 393224 | tf_op jit(solution)/shard_map/ppermute | solution.py:29
  11.3 0.0 collective-permute-start.5
  11.4 1.9 %pack.1 = (bf16[2048,128]{1,0:T(8,128)(2,1)S(1)}, bf16[128,1024]{1,0:T(8,128)(2,1)S(1)}, bf16[128,1024]{1,0:T(8,128)(2,1)S(1)}, bf16[128,1024]{1,0:T(8,128)(2,1)S(1)}, bf16[128,1024]{1,0:T(8,128)(2,1)S(1)}) custom-call(bf16[2,2048,128]{2,1,0:T(8,128)(2,1)} %in_hbm, bf16[2,128,2048]{2,1,0:T(8,128)(2,1)} %glu_hbm, bf16[2,128,2048]{2,1,0:T(8,128)(2,1)} %gate_hbm), custom_call_target="tpu_custom_call" | custom-call | flops 8388608 | bytes 3145728 | tf_op jit(solution)/shard_map/pack/pallas_call | solution.py:171
  13.2 0.1 collective-permute-start.13
  13.3 0.5 collective-permute-done.3.a_ref
  13.8 4.1 %collective-permute-done.4.b_ref = bf16[4,32,512]{2,1,0:T(8,128)(2,1)S(1)} collective-permute-done((bf16[4,32,512]{2,1,0:T(8,128)(2,1)S(1)}, bf16[4,32,512]{2,1,0:T(8,128)(2,1)S(1)}, u32[]{:S(2)}, u32[]{:S(2)}) %collective-permute-start.4) | collective-permute-done | bytes 131104 | tf_op jit(solution)/shard_map/ppermute | solution.py:29
  17.9 0.0 collective-permute-done.5.c_ref
  17.9 0.1 shard_map.143
  18.0 1.6 %collective-permute-start.6 = (bf16[2,32,512]{2,1,0:T(8,128)(2,1)S(1)}, bf16[2,32,512]{2,1,0:T(8,128)(2,1)S(1)}, u32[]{:S(2)}, u32[]{:S(2)}) collective-permute-start(bf16[2,32,512]{2,1,0:T(8,128)(2,1)S(1)} %get-tuple-element.65), channel_id=1, source_target_pairs={{0,8},{2,10},{4,12},{6,14},{8,0},{10,2},{12,4},{14,6},{16,24},{18,... | collective-permute-start | bytes 196616 | tf_op jit(solution)/shard_map/ppermute | solution.py:29
  19.6 2.7 %collective-permute-done.6.arrived_ref = bf16[2,32,512]{2,1,0:T(8,128)(2,1)S(1)} collective-permute-done((bf16[2,32,512]{2,1,0:T(8,128)(2,1)S(1)}, bf16[2,32,512]{2,1,0:T(8,128)(2,1)S(1)}, u32[]{:S(2)}, u32[]{:S(2)}) %collective-permute-start.6) | collective-permute-done | bytes 65568 | tf_op jit(solution)/shard_map/ppermute | solution.py:29
  22.3 2.7 %collective-permute-start.7 = (bf16[2,32,512]{2,1,0:T(8,128)(2,1)S(1)}, bf16[2,32,512]{2,1,0:T(8,128)(2,1)S(1)}, u32[]{:S(2)}, u32[]{:S(2)}) collective-permute-start(bf16[2,32,512]{2,1,0:T(8,128)(2,1)S(1)} %shard_map.144.own_ref), channel_id=1, source_target_pairs={{0,16},{2,18},{4,20},{6,22},{8,24},{10,26},{12,28},{14,30},{16,0},... | collective-permute-start | bytes 196616 | tf_op jit(solution)/shard_map/ppermute | solution.py:29
  25.0 2.6 %collective-permute-done.7.arrived_ref = bf16[2,32,512]{2,1,0:T(8,128)(2,1)S(1)} collective-permute-done((bf16[2,32,512]{2,1,0:T(8,128)(2,1)S(1)}, bf16[2,32,512]{2,1,0:T(8,128)(2,1)S(1)}, u32[]{:S(2)}, u32[]{:S(2)}) %collective-permute-start.7) | collective-permute-done | bytes 65568 | tf_op jit(solution)/shard_map/ppermute | solution.py:29
  27.6 1.6 %collective-permute-start.8 = (bf16[2,32,256]{2,1,0:T(8,128)(2,1)S(1)}, bf16[2,32,256]{2,1,0:T(8,128)(2,1)S(1)}, u32[]{:S(2)}, u32[]{:S(2)}) collective-permute-start(bf16[2,32,256]{2,1,0:T(8,128)(2,1)S(1)} %shard_map.145.own_ref), channel_id=1, source_target_pairs={{0,8},{2,10},{4,12},{6,14},{8,0},{10,2},{12,4},{14,6},{16,24},{18,... | collective-permute-start | bytes 98312 | tf_op jit(solution)/shard_map/ppermute | solution.py:29
  29.2 0.0 collective-permute-start.12
  29.2 1.2 %collective-permute-start.18 = (bf16[128,1024]{1,0:T(8,128)(2,1)S(1)}, bf16[128,1024]{1,0:T(8,128)(2,1)S(1)}, u32[]{:S(2)}, u32[]{:S(2)}) collective-permute-start(bf16[128,1024]{1,0:T(8,128)(2,1)S(1)} %get-tuple-element.79), channel_id=1, source_target_pairs={{0,2},{2,0},{4,6},{6,4},{8,10},{10,8},{12,14},{14,12},{16,18},{18,... | collective-permute-start | bytes 786440 | tf_op jit(solution)/shard_map/ppermute | solution.py:29
  30.5 0.8 collective-permute-start.19
  31.3 0.3 collective-permute-done.8
  31.6 1.5 %collective-permute-start.20 = (bf16[128,1024]{1,0:T(8,128)(2,1)S(1)}, bf16[128,1024]{1,0:T(8,128)(2,1)S(1)}, u32[]{:S(2)}, u32[]{:S(2)}) collective-permute-start(bf16[128,1024]{1,0:T(8,128)(2,1)S(1)} %get-tuple-element.81), channel_id=1, source_target_pairs={{0,6},{2,4},{4,2},{6,0},{8,14},{10,12},{12,10},{14,8},{16,22},{18,... | collective-permute-start | bytes 786440 | tf_op jit(solution)/shard_map/ppermute | solution.py:29
  33.1 0.0 collective-permute-done.12.refs_10_
  33.1 1.5 %collective-permute-start.11 = (bf16[2,2,32,256]{3,2,1,0:T(8,128)(2,1)S(1)}, bf16[2,2,32,256]{3,2,1,0:T(8,128)(2,1)S(1)}, u32[]{:S(2)}, u32[]{:S(2)}) collective-permute-start(bf16[2,2,32,256]{3,2,1,0:T(8,128)(2,1)S(1)} %pad_maximum_fusion.refs_5_), channel_id=1, source_target_pairs={{0,6},{2,4},{4,2},{6,0},{8,14},{10,12},{12,10},{14,8},{16,22},{18,... | collective-permute-start | bytes 196616 | tf_op jit(solution)/shard_map/ppermute | solution.py:29
  34.6 11.3 %collective-permute-done.11.refs_8_ = bf16[2,2,32,256]{3,2,1,0:T(8,128)(2,1)S(1)} collective-permute-done((bf16[2,2,32,256]{3,2,1,0:T(8,128)(2,1)S(1)}, bf16[2,2,32,256]{3,2,1,0:T(8,128)(2,1)S(1)}, u32[]{:S(2)}, u32[]{:S(2)}) %collective-permute-start.11) | collective-permute-done | bytes 65568 | tf_op jit(solution)/shard_map/ppermute | solution.py:29
  45.9 0.6 collective-permute-start.10
  46.5 3.7 %collective-permute-done.10.refs_7_ = bf16[2,2,32,256]{3,2,1,0:T(8,128)(2,1)S(1)} collective-permute-done((bf16[2,2,32,256]{3,2,1,0:T(8,128)(2,1)S(1)}, bf16[2,2,32,256]{3,2,1,0:T(8,128)(2,1)S(1)}, u32[]{:S(2)}, u32[]{:S(2)}) %collective-permute-start.10) | collective-permute-done | bytes 65568 | tf_op jit(solution)/shard_map/ppermute | solution.py:29
  50.2 0.6 collective-permute-start.9
  50.8 3.6 %collective-permute-done.9.refs_6_ = bf16[2,2,32,256]{3,2,1,0:T(8,128)(2,1)S(1)} collective-permute-done((bf16[2,2,32,256]{3,2,1,0:T(8,128)(2,1)S(1)}, bf16[2,2,32,256]{3,2,1,0:T(8,128)(2,1)S(1)}, u32[]{:S(2)}, u32[]{:S(2)}) %collective-permute-start.9) | collective-permute-done | bytes 65568 | tf_op jit(solution)/shard_map/ppermute | solution.py:29
  54.5 0.0 collective-permute-done.13.refs_12_
  54.5 1.2 %shard_map.146 = (bf16[32,128]{1,0:T(8,128)(2,1)S(1)}, f32[2,2,32,512]{3,2,1,0:T(8,128)}) custom-call(f32[2,4,32,512]{3,2,1,0:T(8,128)S(1)} %get-tuple-element.50.refs_0_, bf16[2,2,128,512]{3,2,1,0:T(8,128)(2,1)S(1)} %get-tuple-element.51.refs_1_, bf16[2,2,128,512]{3,2,1,0:T(8,128)(2,1)S(1)} %get-tuple-element.52.refs_2_, ...), custom_call_target="tpu_custom_call", output_to_operand_aliasing={{1}: (13, {})} | custom-call | flops 67108864 | bytes 2097152 | tf_op jit(solution)/shard_map/pallas_call | solution.py:308
  55.6 0.1 collective-permute-start.14
  55.7 1.2 %collective-permute-done.14.arrived_ref = bf16[1,32,128]{2,1,0:T(8,128)(2,1)S(1)} collective-permute-done((bf16[1,32,128]{2,1,0:T(8,128)(2,1)S(1)}, bf16[1,32,128]{2,1,0:T(8,128)(2,1)S(1)}, u32[]{:S(2)}, u32[]{:S(2)}) %collective-permute-start.14) | collective-permute-done | bytes 8224 | tf_op jit(solution)/shard_map/ppermute | solution.py:29
  56.9 1.3 %collective-permute-start.17 = (bf16[64,128]{1,0:T(8,128)(2,1)S(1)}, bf16[64,128]{1,0:T(8,128)(2,1)S(1)}, u32[]{:S(2)}, u32[]{:S(2)}) collective-permute-start(bf16[64,128]{1,0:T(8,128)(2,1)S(1)} %bitcast.13), channel_id=1, source_target_pairs={{0,6},{2,4},{4,2},{6,0},{8,14},{10,12},{12,10},{14,8},{16,22},{18,... | collective-permute-start | bytes 49160 | tf_op jit(solution)/shard_map/ppermute | solution.py:29
  58.2 0.8 collective-permute-start.16
  59.0 1.4 %collective-permute-start.15 = (bf16[64,128]{1,0:T(8,128)(2,1)S(1)}, bf16[64,128]{1,0:T(8,128)(2,1)S(1)}, u32[]{:S(2)}, u32[]{:S(2)}) collective-permute-start(bf16[64,128]{1,0:T(8,128)(2,1)S(1)} %bitcast.15), channel_id=1, source_target_pairs={{0,2},{2,0},{4,6},{6,4},{8,10},{10,8},{12,14},{14,12},{16,18},{18,... | collective-permute-start | bytes 49160 | tf_op jit(solution)/shard_map/ppermute | solution.py:29
  60.4 0.0 collective-permute-done.19.refs_6_
  60.4 0.0 collective-permute-done.20.refs_7_
  60.4 1.1 %collective-permute-done.17.refs_3_ = bf16[64,128]{1,0:T(8,128)(2,1)S(1)} collective-permute-done((bf16[64,128]{1,0:T(8,128)(2,1)S(1)}, bf16[64,128]{1,0:T(8,128)(2,1)S(1)}, u32[]{:S(2)}, u32[]{:S(2)}) %collective-permute-start.17) | collective-permute-done | bytes 16416 | tf_op jit(solution)/shard_map/ppermute | solution.py:29
  61.5 0.4 collective-permute-done.16.refs_2_
  61.9 0.8 collective-permute-done.15.refs_1_
  62.7 0.3 shard_map.148
  63.1 0.7 collective-permute-start.21
  63.7 3.6 %collective-permute-done.21.arrived_ref = bf16[2,64,256]{2,1,0:T(8,128)(2,1)S(1)} collective-permute-done((bf16[2,64,256]{2,1,0:T(8,128)(2,1)S(1)}, bf16[2,64,256]{2,1,0:T(8,128)(2,1)S(1)}, u32[]{:S(2)}, u32[]{:S(2)}) %collective-permute-start.21) | collective-permute-done | bytes 65568 | tf_op jit(solution)/shard_map/ppermute | solution.py:29
  67.4 3.8 %collective-permute-start.22 = (bf16[2,64,256]{2,1,0:T(8,128)(2,1)S(1)}, bf16[2,64,256]{2,1,0:T(8,128)(2,1)S(1)}, u32[]{:S(2)}, u32[]{:S(2)}) collective-permute-start(bf16[2,64,256]{2,1,0:T(8,128)(2,1)S(1)} %shard_map.149.own_ref), channel_id=1, source_target_pairs={{0,16},{2,18},{4,20},{6,22},{8,24},{10,26},{12,28},{14,30},{16,0},... | collective-permute-start | bytes 196616 | tf_op jit(solution)/shard_map/ppermute | solution.py:29
  71.2 0.0 collective-permute-start.23
  71.2 1.2 %collective-permute-done.23.arrived_ref = bf16[2,32,128]{2,1,0:T(8,128)(2,1)S(1)} collective-permute-done((bf16[2,32,128]{2,1,0:T(8,128)(2,1)S(1)}, bf16[2,32,128]{2,1,0:T(8,128)(2,1)S(1)}, u32[]{:S(2)}, u32[]{:S(2)}) %collective-permute-start.23) | collective-permute-done | bytes 16416 | tf_op jit(solution)/shard_map/ppermute | solution.py:29
  72.4 1.2 %collective-permute-done.22.arrived_ref = bf16[2,64,256]{2,1,0:T(8,128)(2,1)S(1)} collective-permute-done((bf16[2,64,256]{2,1,0:T(8,128)(2,1)S(1)}, bf16[2,64,256]{2,1,0:T(8,128)(2,1)S(1)}, u32[]{:S(2)}, u32[]{:S(2)}) %collective-permute-start.22) | collective-permute-done | bytes 65568 | tf_op jit(solution)/shard_map/ppermute | solution.py:29
  73.7 0.1 collective-permute-start.24
  73.8 3.9 %collective-permute-done.24 = bf16[2,64,128]{2,1,0:T(8,128)(2,1)S(1)} collective-permute-done((bf16[2,64,128]{2,1,0:T(8,128)(2,1)S(1)}, bf16[2,64,128]{2,1,0:T(8,128)(2,1)S(1)}, u32[]{:S(2)}, u32[]{:S(2)}) %collective-permute-start.24) | collective-permute-done | bytes 32800 | tf_op jit(solution)/shard_map/ppermute | solution.py:29
  77.7 1.5 %collective-permute-start.27 = (bf16[2,2,64,128]{3,2,1,0:T(8,128)(2,1)S(1)}, bf16[2,2,64,128]{3,2,1,0:T(8,128)(2,1)S(1)}, u32[]{:S(2)}, u32[]{:S(2)}) collective-permute-start(bf16[2,2,64,128]{3,2,1,0:T(8,128)(2,1)S(1)} %pad_maximum_fusion.1.refs_0_), channel_id=1, source_target_pairs={{0,6},{2,4},{4,2},{6,0},{8,14},{10,12},{12,10},{14,8},{16,22},{18,... | collective-permute-start | bytes 196616 | tf_op jit(solution)/shard_map/ppermute | solution.py:29
  79.2 1.4 %collective-permute-start.26 = (bf16[2,2,64,128]{3,2,1,0:T(8,128)(2,1)S(1)}, bf16[2,2,64,128]{3,2,1,0:T(8,128)(2,1)S(1)}, u32[]{:S(2)}, u32[]{:S(2)}) collective-permute-start(bf16[2,2,64,128]{3,2,1,0:T(8,128)(2,1)S(1)} %pad_maximum_fusion.1.refs_0_), channel_id=1, source_target_pairs={{0,4},{2,6},{4,0},{6,2},{8,12},{10,14},{12,8},{14,10},{16,20},{18,... | collective-permute-start | bytes 196616 | tf_op jit(solution)/shard_map/ppermute | solution.py:29
  80.6 0.6 collective-permute-start.25
  81.2 1.7 %collective-permute-done.27.refs_3_ = bf16[2,2,64,128]{3,2,1,0:T(8,128)(2,1)S(1)} collective-permute-done((bf16[2,2,64,128]{3,2,1,0:T(8,128)(2,1)S(1)}, bf16[2,2,64,128]{3,2,1,0:T(8,128)(2,1)S(1)}, u32[]{:S(2)}, u32[]{:S(2)}) %collective-permute-start.27) | collective-permute-done | bytes 65568 | tf_op jit(solution)/shard_map/ppermute | solution.py:29
  82.9 0.7 collective-permute-done.26.refs_2_
  83.6 1.3 %collective-permute-done.25.refs_1_ = bf16[2,2,64,128]{3,2,1,0:T(8,128)(2,1)S(1)} collective-permute-done((bf16[2,2,64,128]{3,2,1,0:T(8,128)(2,1)S(1)}, bf16[2,2,64,128]{3,2,1,0:T(8,128)(2,1)S(1)}, u32[]{:S(2)}, u32[]{:S(2)}) %collective-permute-start.25) | collective-permute-done | bytes 65568 | tf_op jit(solution)/shard_map/ppermute | solution.py:29
  84.9 0.8 settle.1
  (12 shorter events, 0.1 us)
Async XLA Ops:
  2.5 3.9 %collective-permute-start.1 = (bf16[128,2048]{1,0:T(8,128)(2,1)S(1)}, bf16[128,2048]{1,0:T(8,128)(2,1)S(1)}, u32[]{:S(2)}, u32[]{:S(2)}) collective-permute-start(bf16[128,2048]{1,0:T(8,128)(2,1)S(1)} %get-tuple-element.58.refs_0_), channel_id=1, source_target_pairs={{0,1},{1,0},{2,3},{3,2},{4,5},{5,4},{6,7},{7,6},{8,9},{9,8},{10,11... | collective-permute-start | bytes 1572872 | tf_op jit(solution)/shard_map/ppermute | solution.py:29
  3.1 3.3 %collective-permute-start.2 = (bf16[128,2048]{1,0:T(8,128)(2,1)S(1)}, bf16[128,2048]{1,0:T(8,128)(2,1)S(1)}, u32[]{:S(2)}, u32[]{:S(2)}) collective-permute-start(bf16[128,2048]{1,0:T(8,128)(2,1)S(1)} %get-tuple-element.59.refs_2_), channel_id=1, source_target_pairs={{0,1},{1,0},{2,3},{3,2},{4,5},{5,4},{6,7},{7,6},{8,9},{9,8},{10,11... | collective-permute-start | bytes 1572872 | tf_op jit(solution)/shard_map/ppermute | solution.py:29
  3.2 2.3 %collective-permute-start = (f32[32,512]{1,0:T(8,128)S(1)}, f32[32,512]{1,0:T(8,128)S(1)}, u32[]{:S(2)}, u32[]{:S(2)}) collective-permute-start(f32[32,512]{1,0:T(8,128)S(1)} %get-tuple-element.56), channel_id=1, source_target_pairs={{0,1},{1,0},{2,3},{3,2},{4,5},{5,4},{6,7},{7,6},{8,9},{9,8},{10,11... | collective-permute-start | bytes 196616 | tf_op jit(solution)/shard_map/ppermute | solution.py:29
  6.9 6.9 %collective-permute-start.3 = (bf16[4,32,512]{2,1,0:T(8,128)(2,1)S(1)}, bf16[4,32,512]{2,1,0:T(8,128)(2,1)S(1)}, u32[]{:S(2)}, u32[]{:S(2)}) collective-permute-start(bf16[4,32,512]{2,1,0:T(8,128)(2,1)S(1)} %get-tuple-element.61), channel_id=1, source_target_pairs={{0,2},{2,0},{4,6},{6,4},{8,10},{10,8},{12,14},{14,12},{16,18},{18,... | collective-permute-start | bytes 393224 | tf_op jit(solution)/shard_map/ppermute | solution.py:29
  9.8 8.1 %collective-permute-start.4 = (bf16[4,32,512]{2,1,0:T(8,128)(2,1)S(1)}, bf16[4,32,512]{2,1,0:T(8,128)(2,1)S(1)}, u32[]{:S(2)}, u32[]{:S(2)}) collective-permute-start(bf16[4,32,512]{2,1,0:T(8,128)(2,1)S(1)} %get-tuple-element.62), channel_id=1, source_target_pairs={{0,4},{2,6},{4,0},{6,2},{8,12},{10,14},{12,8},{14,10},{16,20},{18,... | collective-permute-start | bytes 393224 | tf_op jit(solution)/shard_map/ppermute | solution.py:29
  11.3 6.6 %collective-permute-start.5 = (bf16[4,32,512]{2,1,0:T(8,128)(2,1)S(1)}, bf16[4,32,512]{2,1,0:T(8,128)(2,1)S(1)}, u32[]{:S(2)}, u32[]{:S(2)}) collective-permute-start(bf16[4,32,512]{2,1,0:T(8,128)(2,1)S(1)} %get-tuple-element.63), channel_id=1, source_target_pairs={{0,6},{2,4},{4,2},{6,0},{8,14},{10,12},{12,10},{14,8},{16,22},{18,... | collective-permute-start | bytes 393224 | tf_op jit(solution)/shard_map/ppermute | solution.py:29
  13.2 41.2 %collective-permute-start.13 = (bf16[2048,128]{1,0:T(8,128)(2,1)S(1)}, bf16[2048,128]{1,0:T(8,128)(2,1)S(1)}, u32[]{:S(2)}, u32[]{:S(2)}) collective-permute-start(bf16[2048,128]{1,0:T(8,128)(2,1)S(1)} %get-tuple-element.71.refs_11_), channel_id=1, source_target_pairs={{0,1},{1,0},{2,3},{3,2},{4,5},{5,4},{6,7},{7,6},{8,9},{9,8},{10,11... | collective-permute-start | bytes 1572872 | tf_op jit(solution)/shard_map/ppermute | solution.py:29
  18.0 4.3 %collective-permute-start.6 = (bf16[2,32,512]{2,1,0:T(8,128)(2,1)S(1)}, bf16[2,32,512]{2,1,0:T(8,128)(2,1)S(1)}, u32[]{:S(2)}, u32[]{:S(2)}) collective-permute-start(bf16[2,32,512]{2,1,0:T(8,128)(2,1)S(1)} %get-tuple-element.65), channel_id=1, source_target_pairs={{0,8},{2,10},{4,12},{6,14},{8,0},{10,2},{12,4},{14,6},{16,24},{18,... | collective-permute-start | bytes 196616 | tf_op jit(solution)/shard_map/ppermute | solution.py:29
  22.3 5.3 %collective-permute-start.7 = (bf16[2,32,512]{2,1,0:T(8,128)(2,1)S(1)}, bf16[2,32,512]{2,1,0:T(8,128)(2,1)S(1)}, u32[]{:S(2)}, u32[]{:S(2)}) collective-permute-start(bf16[2,32,512]{2,1,0:T(8,128)(2,1)S(1)} %shard_map.144.own_ref), channel_id=1, source_target_pairs={{0,16},{2,18},{4,20},{6,22},{8,24},{10,26},{12,28},{14,30},{16,0},... | collective-permute-start | bytes 196616 | tf_op jit(solution)/shard_map/ppermute | solution.py:29
  27.6 1.6 %copy-start = (f32[2,2048]{1,0:T(2,128)S(1)}, f32[2,2048]{1,0:T(2,128)}, u32[]{:S(2)}) copy-start(f32[2,2048]{1,0:T(2,128)} %refs_9_.3) | copy-start | bytes 49156
  27.6 4.0 %collective-permute-start.8 = (bf16[2,32,256]{2,1,0:T(8,128)(2,1)S(1)}, bf16[2,32,256]{2,1,0:T(8,128)(2,1)S(1)}, u32[]{:S(2)}, u32[]{:S(2)}) collective-permute-start(bf16[2,32,256]{2,1,0:T(8,128)(2,1)S(1)} %shard_map.145.own_ref), channel_id=1, source_target_pairs={{0,8},{2,10},{4,12},{6,14},{8,0},{10,2},{12,4},{14,6},{16,24},{18,... | collective-permute-start | bytes 98312 | tf_op jit(solution)/shard_map/ppermute | solution.py:29
  29.2 3.9 %collective-permute-start.12 = (f32[2,2048]{1,0:T(2,128)S(1)}, f32[2,2048]{1,0:T(2,128)S(1)}, u32[]{:S(2)}, u32[]{:S(2)}) collective-permute-start(f32[2,2048]{1,0:T(2,128)S(1)} %copy-done), channel_id=1, source_target_pairs={{0,1},{1,0},{2,3},{3,2},{4,5},{5,4},{6,7},{7,6},{8,9},{9,8},{10,11... | collective-permute-start | bytes 49160 | tf_op jit(solution)/shard_map/ppermute | solution.py:29
  29.2 29.8 %collective-permute-start.18 = (bf16[128,1024]{1,0:T(8,128)(2,1)S(1)}, bf16[128,1024]{1,0:T(8,128)(2,1)S(1)}, u32[]{:S(2)}, u32[]{:S(2)}) collective-permute-start(bf16[128,1024]{1,0:T(8,128)(2,1)S(1)} %get-tuple-element.79), channel_id=1, source_target_pairs={{0,2},{2,0},{4,6},{6,4},{8,10},{10,8},{12,14},{14,12},{16,18},{18,... | collective-permute-start | bytes 786440 | tf_op jit(solution)/shard_map/ppermute | solution.py:29
  30.5 29.9 %collective-permute-start.19 = (bf16[128,1024]{1,0:T(8,128)(2,1)S(1)}, bf16[128,1024]{1,0:T(8,128)(2,1)S(1)}, u32[]{:S(2)}, u32[]{:S(2)}) collective-permute-start(bf16[128,1024]{1,0:T(8,128)(2,1)S(1)} %get-tuple-element.80), channel_id=1, source_target_pairs={{0,4},{2,6},{4,0},{6,2},{8,12},{10,14},{12,8},{14,10},{16,20},{18,... | collective-permute-start | bytes 786440 | tf_op jit(solution)/shard_map/ppermute | solution.py:29
  31.6 28.8 %collective-permute-start.20 = (bf16[128,1024]{1,0:T(8,128)(2,1)S(1)}, bf16[128,1024]{1,0:T(8,128)(2,1)S(1)}, u32[]{:S(2)}, u32[]{:S(2)}) collective-permute-start(bf16[128,1024]{1,0:T(8,128)(2,1)S(1)} %get-tuple-element.81), channel_id=1, source_target_pairs={{0,6},{2,4},{4,2},{6,0},{8,14},{10,12},{12,10},{14,8},{16,22},{18,... | collective-permute-start | bytes 786440 | tf_op jit(solution)/shard_map/ppermute | solution.py:29
  33.1 12.8 %collective-permute-start.11 = (bf16[2,2,32,256]{3,2,1,0:T(8,128)(2,1)S(1)}, bf16[2,2,32,256]{3,2,1,0:T(8,128)(2,1)S(1)}, u32[]{:S(2)}, u32[]{:S(2)}) collective-permute-start(bf16[2,2,32,256]{3,2,1,0:T(8,128)(2,1)S(1)} %pad_maximum_fusion.refs_5_), channel_id=1, source_target_pairs={{0,6},{2,4},{4,2},{6,0},{8,14},{10,12},{12,10},{14,8},{16,22},{18,... | collective-permute-start | bytes 196616 | tf_op jit(solution)/shard_map/ppermute | solution.py:29
  45.9 4.3 %collective-permute-start.10 = (bf16[2,2,32,256]{3,2,1,0:T(8,128)(2,1)S(1)}, bf16[2,2,32,256]{3,2,1,0:T(8,128)(2,1)S(1)}, u32[]{:S(2)}, u32[]{:S(2)}) collective-permute-start(bf16[2,2,32,256]{3,2,1,0:T(8,128)(2,1)S(1)} %pad_maximum_fusion.refs_5_), channel_id=1, source_target_pairs={{0,4},{2,6},{4,0},{6,2},{8,12},{10,14},{12,8},{14,10},{16,20},{18,... | collective-permute-start | bytes 196616 | tf_op jit(solution)/shard_map/ppermute | solution.py:29
  50.2 4.3 %collective-permute-start.9 = (bf16[2,2,32,256]{3,2,1,0:T(8,128)(2,1)S(1)}, bf16[2,2,32,256]{3,2,1,0:T(8,128)(2,1)S(1)}, u32[]{:S(2)}, u32[]{:S(2)}) collective-permute-start(bf16[2,2,32,256]{3,2,1,0:T(8,128)(2,1)S(1)} %pad_maximum_fusion.refs_5_), channel_id=1, source_target_pairs={{0,2},{2,0},{4,6},{6,4},{8,10},{10,8},{12,14},{14,12},{16,18},{18,... | collective-permute-start | bytes 196616 | tf_op jit(solution)/shard_map/ppermute | solution.py:29
  55.6 1.2 %collective-permute-start.14 = (bf16[1,32,128]{2,1,0:T(8,128)(2,1)S(1)}, bf16[1,32,128]{2,1,0:T(8,128)(2,1)S(1)}, u32[]{:S(2)}, u32[]{:S(2)}) collective-permute-start(bf16[1,32,128]{2,1,0:T(8,128)(2,1)S(1)} %bitcast.17), channel_id=1, source_target_pairs={{0,1},{1,0},{2,3},{3,2},{4,5},{5,4},{6,7},{7,6},{8,9},{9,8},{10,11... | collective-permute-start | bytes 24584 | tf_op jit(solution)/shard_map/ppermute | solution.py:29
  56.9 4.6 %collective-permute-start.17 = (bf16[64,128]{1,0:T(8,128)(2,1)S(1)}, bf16[64,128]{1,0:T(8,128)(2,1)S(1)}, u32[]{:S(2)}, u32[]{:S(2)}) collective-permute-start(bf16[64,128]{1,0:T(8,128)(2,1)S(1)} %bitcast.13), channel_id=1, source_target_pairs={{0,6},{2,4},{4,2},{6,0},{8,14},{10,12},{12,10},{14,8},{16,22},{18,... | collective-permute-start | bytes 49160 | tf_op jit(solution)/shard_map/ppermute | solution.py:29
  58.2 3.7 %collective-permute-start.16 = (bf16[64,128]{1,0:T(8,128)(2,1)S(1)}, bf16[64,128]{1,0:T(8,128)(2,1)S(1)}, u32[]{:S(2)}, u32[]{:S(2)}) collective-permute-start(bf16[64,128]{1,0:T(8,128)(2,1)S(1)} %bitcast.14), channel_id=1, source_target_pairs={{0,4},{2,6},{4,0},{6,2},{8,12},{10,14},{12,8},{14,10},{16,20},{18,... | collective-permute-start | bytes 49160 | tf_op jit(solution)/shard_map/ppermute | solution.py:29
  59.0 3.7 %collective-permute-start.15 = (bf16[64,128]{1,0:T(8,128)(2,1)S(1)}, bf16[64,128]{1,0:T(8,128)(2,1)S(1)}, u32[]{:S(2)}, u32[]{:S(2)}) collective-permute-start(bf16[64,128]{1,0:T(8,128)(2,1)S(1)} %bitcast.15), channel_id=1, source_target_pairs={{0,2},{2,0},{4,6},{6,4},{8,10},{10,8},{12,14},{14,12},{16,18},{18,... | collective-permute-start | bytes 49160 | tf_op jit(solution)/shard_map/ppermute | solution.py:29
  63.1 4.3 %collective-permute-start.21 = (bf16[2,64,256]{2,1,0:T(8,128)(2,1)S(1)}, bf16[2,64,256]{2,1,0:T(8,128)(2,1)S(1)}, u32[]{:S(2)}, u32[]{:S(2)}) collective-permute-start(bf16[2,64,256]{2,1,0:T(8,128)(2,1)S(1)} %get-tuple-element.83), channel_id=1, source_target_pairs={{0,8},{2,10},{4,12},{6,14},{8,0},{10,2},{12,4},{14,6},{16,24},{18,... | collective-permute-start | bytes 196616 | tf_op jit(solution)/shard_map/ppermute | solution.py:29
  67.4 6.3 %collective-permute-start.22 = (bf16[2,64,256]{2,1,0:T(8,128)(2,1)S(1)}, bf16[2,64,256]{2,1,0:T(8,128)(2,1)S(1)}, u32[]{:S(2)}, u32[]{:S(2)}) collective-permute-start(bf16[2,64,256]{2,1,0:T(8,128)(2,1)S(1)} %shard_map.149.own_ref), channel_id=1, source_target_pairs={{0,16},{2,18},{4,20},{6,22},{8,24},{10,26},{12,28},{14,30},{16,0},... | collective-permute-start | bytes 196616 | tf_op jit(solution)/shard_map/ppermute | solution.py:29
  71.2 1.2 %collective-permute-start.23 = (bf16[2,32,128]{2,1,0:T(8,128)(2,1)S(1)}, bf16[2,32,128]{2,1,0:T(8,128)(2,1)S(1)}, u32[]{:S(2)}, u32[]{:S(2)}) collective-permute-start(bf16[2,32,128]{2,1,0:T(8,128)(2,1)S(1)} %slice.4), channel_id=1, source_target_pairs={{0,1},{1,0},{2,3},{3,2},{4,5},{5,4},{6,7},{7,6},{8,9},{9,8},{10,11... | collective-permute-start | bytes 49160 | tf_op jit(solution)/shard_map/ppermute | solution.py:29
  73.7 4.0 %collective-permute-start.24 = (bf16[2,64,128]{2,1,0:T(8,128)(2,1)S(1)}, bf16[2,64,128]{2,1,0:T(8,128)(2,1)S(1)}, u32[]{:S(2)}, u32[]{:S(2)}) collective-permute-start(bf16[2,64,128]{2,1,0:T(8,128)(2,1)S(1)} %shard_map.151), channel_id=1, source_target_pairs={{0,8},{2,10},{4,12},{6,14},{8,0},{10,2},{12,4},{14,6},{16,24},{18,... | collective-permute-start | bytes 98312 | tf_op jit(solution)/shard_map/ppermute | solution.py:29
  77.7 5.2 %collective-permute-start.27 = (bf16[2,2,64,128]{3,2,1,0:T(8,128)(2,1)S(1)}, bf16[2,2,64,128]{3,2,1,0:T(8,128)(2,1)S(1)}, u32[]{:S(2)}, u32[]{:S(2)}) collective-permute-start(bf16[2,2,64,128]{3,2,1,0:T(8,128)(2,1)S(1)} %pad_maximum_fusion.1.refs_0_), channel_id=1, source_target_pairs={{0,6},{2,4},{4,2},{6,0},{8,14},{10,12},{12,10},{14,8},{16,22},{18,... | collective-permute-start | bytes 196616 | tf_op jit(solution)/shard_map/ppermute | solution.py:29
  79.2 4.4 %collective-permute-start.26 = (bf16[2,2,64,128]{3,2,1,0:T(8,128)(2,1)S(1)}, bf16[2,2,64,128]{3,2,1,0:T(8,128)(2,1)S(1)}, u32[]{:S(2)}, u32[]{:S(2)}) collective-permute-start(bf16[2,2,64,128]{3,2,1,0:T(8,128)(2,1)S(1)} %pad_maximum_fusion.1.refs_0_), channel_id=1, source_target_pairs={{0,4},{2,6},{4,0},{6,2},{8,12},{10,14},{12,8},{14,10},{16,20},{18,... | collective-permute-start | bytes 196616 | tf_op jit(solution)/shard_map/ppermute | solution.py:29
  80.6 4.3 %collective-permute-start.25 = (bf16[2,2,64,128]{3,2,1,0:T(8,128)(2,1)S(1)}, bf16[2,2,64,128]{3,2,1,0:T(8,128)(2,1)S(1)}, u32[]{:S(2)}, u32[]{:S(2)}) collective-permute-start(bf16[2,2,64,128]{3,2,1,0:T(8,128)(2,1)S(1)} %pad_maximum_fusion.1.refs_0_), channel_id=1, source_target_pairs={{0,2},{2,0},{4,6},{6,4},{8,10},{10,8},{12,14},{14,12},{16,18},{18,... | collective-permute-start | bytes 196616 | tf_op jit(solution)/shard_map/ppermute | solution.py:29

commit v2 on v1

--- a/solution.py
+++ b/solution.py
@@ -68,13 +68,14 @@
     return index % 4, (index // 4) % 2, index // 8
 
 
-def placed_pieces(pieces, chunk):
+def placed_sources(pieces, chunk):
     low, near, _ = corner()
-    for k in range(4):
-        for j in range(2):
-            for far in range(2):
-                at = ((2 * far + (near ^ j)) * 4 + (low ^ k)) * chunk
-                yield pl.multiple_of(at, chunk), pieces[k][j, far]
+    for k, piece in enumerate(pieces):
+        if piece is not None:
+            for j in range(2):
+                for far in range(2):
+                    at = ((2 * far + (near ^ j)) * 4 + (low ^ k)) * chunk
+                    yield pl.multiple_of(at, chunk), k, piece.at[j, far]
 
 
 def iota(shape, axis):
@@ -86,10 +87,10 @@
 
 
 def prepare_kernel(
-    lengths_ref, step_ref, re_ref, im_ref, in_ref, out_ref, coeff_ref, m_ref, n_ref
+    layer, lengths_ref, step_ref, re_ref, im_ref, in_ref, out_ref, coeff_ref, m_ref, n_ref
 ):
-    layers, groups, states = re_ref.shape
-    total, width = coeff_ref.shape[3], n_ref.shape[2]
+    _, groups, states = re_ref.shape
+    total, width = coeff_ref.shape[2], n_ref.shape[1]
     group = width // groups
     own = lengths_ref.shape[1]
     row = jnp.broadcast_to(position_factor(lengths_ref[...]), (own, own))
@@ -106,40 +107,39 @@
             jnp.where(of_group, exact_dot(value, spread), 0.0), axis=0, keepdims=True
         )
 
-    for layer in range(layers):
-        log_step = exact_dot(step_ref[layer : layer + 1, :], of_group.astype(F32))
-        eig_re = flat(re_ref[layer])
-        eig_im = flat(im_ref[layer])
-        step_size = jnp.exp(log_step) * factor
-        magnitude = jnp.exp(eig_re * step_size)
-        turned = eig_im * step_size
-        decay_re = magnitude * jnp.cos(turned)
-        decay_im = magnitude * jnp.sin(turned)
-        scale = 1.0 / (eig_re * eig_re + eig_im * eig_im)
-        coeff_ref[layer, 0] = decay_re
-        coeff_ref[layer, 1] = decay_im
-        coeff_ref[layer, 2] = ((decay_re - 1.0) * eig_re + decay_im * eig_im) * scale
-        coeff_ref[layer, 3] = (decay_im * eig_re - (decay_re - 1.0) * eig_im) * scale
-        for part in range(2):
-            for source, target in ((in_ref, m_ref), (out_ref, n_ref)):
-                value = jnp.dot(
-                    source[layer, part].astype(BF16), spread_half, preferred_element_type=F32
-                )
-                if part == 1 and target is n_ref:
-                    value = -value
-                target[layer, part] = jnp.where(keep, value, 0.0).astype(BF16)
-
-
-def prepare(own, lengths, log_step, eig_re, eig_im, in_rows, out_rows):
-    layers, groups, states = eig_re.shape
+    log_step = exact_dot(step_ref[layer : layer + 1, :], of_group.astype(F32))
+    eig_re = flat(re_ref[layer])
+    eig_im = flat(im_ref[layer])
+    step_size = jnp.exp(log_step) * factor
+    magnitude = jnp.exp(eig_re * step_size)
+    turned = eig_im * step_size
+    decay_re = magnitude * jnp.cos(turned)
+    decay_im = magnitude * jnp.sin(turned)
+    scale = 1.0 / (eig_re * eig_re + eig_im * eig_im)
+    coeff_ref[0] = decay_re
+    coeff_ref[1] = decay_im
+    coeff_ref[2] = ((decay_re - 1.0) * eig_re + decay_im * eig_im) * scale
+    coeff_ref[3] = (decay_im * eig_re - (decay_re - 1.0) * eig_im) * scale
+    for part in range(2):
+        for source, target in ((in_ref, m_ref), (out_ref, n_ref)):
+            value = jnp.dot(
+                source[layer, part].astype(BF16), spread_half, preferred_element_type=F32
+            )
+            if part == 1 and target is n_ref:
+                value = -value
+            target[part] = jnp.where(keep, value, 0.0).astype(BF16)
+
+
+def prepare(layer, own, lengths, log_step, eig_re, eig_im, in_rows, out_rows):
+    _, groups, states = eig_re.shape
     total, width = groups * states, in_rows.shape[2]
     outs = [
-        struct((layers, 4, own, total), F32),
-        struct((layers, 2, width, total), BF16),
-        struct((layers, 2, width, total), BF16),
+        struct((4, own, total), F32),
+        struct((2, width, total), BF16),
+        struct((2, width, total), BF16),
     ]
     args = (lengths, log_step, eig_re, eig_im, in_rows, out_rows)
-    return call(prepare_kernel, args, outs)
+    return call(functools.partial(prepare_kernel, layer), args, outs)
 
 
 def pack_kernel(in_hbm, glu_hbm, gate_hbm, in_out, *refs):
@@ -239,15 +239,45 @@
     return made[0], made[1], made[2 : 2 + len(others)], made[2 + len(others) :]
 
 
-def recur_kernel(layer, dp, model, n_pieces, *refs):
+def piece_kernel(k, dp, layer, piece, *refs):
+    gains, weights, (partial_out, squares_out) = refs[:dp], refs[dp : 2 * dp], refs[2 * dp :]
+    own, chunk = piece.shape[2], piece.shape[3] // dp
+    low, near, _ = corner()
+    squares = jnp.zeros((own, 1), F32)
+    partial_value = jnp.zeros(partial_out.shape, F32)
+    for j in range(2):
+        for far in range(2):
+            at = ((2 * far + (near ^ j)) * 4 + (low ^ k)) * chunk
+            at = pl.multiple_of(at, chunk)
+            for p in range(dp):
+                current = piece[j, far, :, p * chunk : (p + 1) * chunk].astype(F32)
+                squares = squares + jnp.sum(current * current, axis=1, keepdims=True)
+                gain = gains[p][layer : layer + 1, pl.ds(at, chunk)]
+                scaled = (current * gain).astype(BF16)
+                partial_value = partial_value + jnp.dot(
+                    scaled, weights[p][pl.ds(at, chunk), :], preferred_element_type=F32
+                )
+    partial_out[...] = partial_value
+    squares_out[...] = jnp.broadcast_to(squares, squares_out.shape)
+
+
+def project_piece(k, layer, piece, gains, weights):
+    own = piece.shape[2]
+    dp = len(gains)
+    width = weights[0].shape[1]
+    return call(
+        functools.partial(piece_kernel, k, dp, layer),
+        (piece, *gains, *weights),
+        [struct((own, width), F32), struct((own, 128), F32)],
+    )
+
+
+def recur_kernel(layer, dp, model, *refs):
     coeff_ref, m_ref, n_ref, skip_ref, state_ref = refs[:5]
-    pieces = refs[5 : 5 + n_pieces]
-    line, new_ref, sem = refs[-3:]
-    own, feats = line.shape[1:]
     width = skip_ref.shape[1]
-    chunk = feats // 16
     if layer == 0:
-        readout_ref, state_out, before_ref = refs[-6:-3]
+        pieces, (readout_ref, new_ref, before_ref) = refs[5:7], refs[7:]
+        chunk = before_ref.shape[2] // dp
         partial_value = pieces[0][:, :width] + pieces[1][:, :width]
         squares = (pieces[0][:, width : width + 128] + pieces[1][:, width : width + 128])[:, :1]
         for far in range(2):
@@ -257,68 +287,57 @@
                     :, base : base + chunk
                 ].astype(BF16)
     else:
-        readout_ref, state_out = refs[-5:-3]
-        gains = refs[5 + n_pieces : 5 + n_pieces + dp]
-        weights = refs[5 + n_pieces + dp : 5 + n_pieces + 2 * dp]
-        for at, piece in placed_pieces(pieces, chunk):
-            for p in range(dp):
-                line[p, :, pl.ds(at, chunk)] = piece[:, p * chunk : (p + 1) * chunk]
-        squares = jnp.zeros((own, 1), F32)
-        partial_value = None
-        for p in range(dp):
-            current = line[p].astype(F32)
-            squares = squares + jnp.sum(current * current, axis=1, keepdims=True)
-            scaled = (current * gains[p][layer : layer + 1, :]).astype(BF16)
-            term = jnp.dot(scaled, weights[p][...], preferred_element_type=F32)
-            partial_value = term if partial_value is None else partial_value + term
+        terms, (readout_ref, new_ref) = refs[5:13], refs[13:]
+        partial_value = terms[0][...] + terms[2][...] + terms[4][...] + terms[6][...]
+        squares = terms[1][...] + terms[3][...] + terms[5][...] + terms[7][...]
+        squares = squares[:, :1]
     driven = (partial_value * lax.rsqrt(squares / model + NORM_EPS)).astype(BF16)
-    drive_re = jnp.dot(driven, m_ref[layer, 0], preferred_element_type=F32)
-    drive_im = jnp.dot(driven, m_ref[layer, 1], preferred_element_type=F32)
-    decay_re, decay_im = coeff_ref[layer, 0], coeff_ref[layer, 1]
-    weight_re, weight_im = coeff_ref[layer, 2], coeff_ref[layer, 3]
+    drive_re = jnp.dot(driven, m_ref[0], preferred_element_type=F32)
+    drive_im = jnp.dot(driven, m_ref[1], preferred_element_type=F32)
+    decay_re, decay_im = coeff_ref[0], coeff_ref[1]
+    weight_re, weight_im = coeff_ref[2], coeff_ref[3]
     old_re, old_im = state_ref[layer, 0], state_ref[layer, 1]
     new_re = decay_re * old_re - decay_im * old_im + weight_re * drive_re - weight_im * drive_im
     new_im = decay_re * old_im + decay_im * old_re + weight_re * drive_im + weight_im * drive_re
     new_ref[0] = new_re
     new_ref[1] = new_im
-    copy = pltpu.make_async_copy(new_ref, state_out.at[layer], sem)
-    copy.start()
-    value = nt_dot(new_re.astype(BF16), n_ref[layer, 0])
-    value = value + nt_dot(new_im.astype(BF16), n_ref[layer, 1])
+    value = nt_dot(new_re.astype(BF16), n_ref[0])
+    value = value + nt_dot(new_im.astype(BF16), n_ref[1])
     value = value + skip_ref[layer : layer + 1, :] * driven.astype(F32)
     readout_ref[...] = jax.nn.gelu(value).astype(BF16)
-    copy.wait()
-
-
-def recur(layer, dims, consts, pieces, slabs, so_far):
+
+
+def recur(layer, dims, consts, terms):
     dp, _, _, model, own, feats = dims
     skip, state = consts[3:]
-    args = [*consts, *pieces, *slabs]
-    specs = [VMEM] * len(args)
-    outs = [struct((own, skip.shape[1]), BF16), struct(state.shape, F32)]
-    out_specs = [VMEM, ANY]
-    alias = {}
+    outs = [struct((own, skip.shape[1]), BF16), pltpu.VMEM(state.shape[1:], F32)]
     if layer == 0:
         outs.append(struct((2, own, dp * feats // 16), BF16))
-        out_specs.append(VMEM)
-    else:
-        alias = {len(args): 1}
-        args.append(so_far)
-        specs.append(ANY)
+    return call(functools.partial(recur_kernel, layer, dp, model), (*consts, *terms), outs, mib=8)
+
+
+def store_kernel(first, second, out, sems):
+    copies = [
+        pltpu.make_async_copy(ref, out.at[layer], sems.at[layer])
+        for layer, ref in enumerate((first, second))
+    ]
+    for copy in copies:
+        copy.start()
+    for copy in copies:
+        copy.wait()
+
+
+def store(states):
     return pl.pallas_call(
-        functools.partial(recur_kernel, layer, dp, model, len(pieces)),
-        in_specs=specs,
-        out_specs=out_specs,
-        out_shape=outs,
-        scratch_shapes=[
-            pltpu.VMEM((dp, own, feats), BF16),
-            pltpu.VMEM(state.shape[1:], F32),
-            pltpu.SemaphoreType.DMA,
-        ],
-        input_output_aliases=alias,
-        compiler_params=params(8),
-        cost_estimate=pl.CostEstimate(flops=64 << 20, bytes_accessed=2 << 20, transcendentals=0),
-    )(*args)
+        store_kernel,
+        in_specs=[VMEM] * 2,
+        out_specs=ANY,
+        out_shape=struct((2,) + states[0].shape, F32),
+        scratch_shapes=[pltpu.SemaphoreType.DMA((2,))],
+        compiler_params=params(4),
+        cost_estimate=pl.CostEstimate(flops=1 << 20, bytes_accessed=1 << 19, transcendentals=0),
+        name="store",
+    )(*states)
 
 
 def product_kernel(chunk, readout_ref, *refs):
@@ -411,28 +430,41 @@
     out[:, pl.ds(pl.multiple_of((1 - me) * rows, rows), rows), :] = arrived_ref[...]
 
 
-def settle_kernel(chunk, *refs):
-    pieces, out, sem = refs[:4], refs[4], refs[5]
+def settle_kernel(which, chunk, *refs):
+    pieces, out, sem = refs[: len(which)], refs[-2], refs[-1]
+    slots = [None] * 4
+    for k, piece in zip(which, pieces):
+        slots[k] = piece
     copies = []
-    for i, (at, _) in enumerate(placed_pieces(pieces, chunk)):
-        source = pieces[i // 4].at[(i // 2) % 2, i % 2]
-        copies.append(pltpu.make_async_copy(source, out.at[:, pl.ds(at, chunk)], sem.at[i]))
+    for at, k, source in placed_sources(slots, chunk):
+        copies.append(
+            pltpu.make_async_copy(source, out.at[:, pl.ds(at, chunk)], sem.at[len(copies)])
+        )
         copies[-1].start()
     for copy in copies:
         copy.wait()
 
 
-def settle(pieces, feats):
+def settle(which, pieces, feats, so_far=None):
     rows, chunk = pieces[0].shape[2:]
+    args = [pieces[k] for k in which]
+    specs = [VMEM] * len(args)
+    alias = {}
+    if so_far is not None:
+        alias = {len(args): 0}
+        args.append(so_far)
+        specs.append(ANY)
     return pl.pallas_call(
-        functools.partial(settle_kernel, chunk),
-        in_specs=[VMEM] * 4,
+        functools.partial(settle_kernel, which, chunk),
+        in_specs=specs,
         out_specs=ANY,
         out_shape=struct((rows, feats), BF16),
-        scratch_shapes=[pltpu.SemaphoreType.DMA((16,))],
+        scratch_shapes=[pltpu.SemaphoreType.DMA((4 * len(which),))],
+        input_output_aliases=alias,
         compiler_params=params(4),
+        cost_estimate=pl.CostEstimate(flops=1 << 20, bytes_accessed=1 << 18, transcendentals=0),
         name="settle",
-    )(*pieces)
+    )(*args)
 
 
 def plain_prepare(lengths, log_step, eig_re, eig_im, in_mat, output_matrices):
@@ -605,14 +637,16 @@
     )
     pieces = [keep, core_swap(send)]
     outward = [outward[0], core_swap(outward[0]), outward[1], core_swap(outward[1])]
-    consts = (*prepare(own, *others[:6]), *others[6:])
-
-    readout, new_state, before = recur(0, dims, consts, pieces, [], None)
+    consts = (*prepare(0, own, *others[:6]), *others[6:])
+
+    readout, new_first, before = recur(0, dims, consts, pieces)
     parts = products(dims, readout, outward)
     arrived = [over_low(parts[k], k) for k in range(1, 4)]
     stacks = lax.optimization_barrier((w_in, w_glu, w_gate, norm_gain, parts[0]))
     inward, *packs = pack(*stacks[:3])
     gain = stacks[3]
+    *others, _ = lax.optimization_barrier((*others, parts[0]))
+    later_consts = (*prepare(1, own, *others[:6]), *others[6:])
     slabs = [norm_gain, core_swap(gain), inward, core_swap(inward)]
     keep, send = call(
         fold_low_kernel,
@@ -631,7 +665,10 @@
     away = core_swap(away)
     (before,) = call(merge_kernel, (shard, away), [struct((2, own * dp, chunk), BF16)])
 
-    readout, new_state = recur(1, dims, consts, pieces, slabs, new_state)
+    terms = []
+    for k in (0, 3, 2, 1):
+        terms += project_piece(k, 1, pieces[k], slabs[:2], slabs[2:])
+    readout, new_second = recur(1, dims, later_consts, terms)
     readout = readout[None]
     (rows,) = call(
         merge_kernel, (readout, core_swap(readout)), [struct((1, own * dp, width), BF16)]
@@ -639,14 +676,15 @@
     rows = rows[0]
     readouts = [rows] + [over_low(rows, k) for k in range(1, 4)]
     keep, send = gathered_products(chunk, readouts, weights)
-    (send,) = call(
-        fold_near_kernel, (keep, over_near(send)), [struct((2, own * dp, 2 * chunk), BF16)]
-    )
+    arrived = over_near(send)
+    (send,) = call(fold_near_kernel, (keep, arrived), [struct((2, own * dp, 2 * chunk), BF16)])
+    new_state = store([new_first, new_second])
     terms = (send, over_far(send), before)
     (shard,) = call(update_kernel, terms, [struct((2, own * dp, chunk), BF16)])
     column = jnp.stack([shard, over_near(shard)])
     pieces = [column] + [over_low(column, k) for k in range(1, 4)]
-    return settle(pieces, feats), new_state
+    mixed = settle((0, 3), pieces, feats)
+    return settle((1, 2), pieces, feats, mixed), new_state
 
 
 def make_body(tp, dp):

time: 85.9 us -> 81.2 us (0.945)
  waiting for transfers between devices: 46.6 us -> 41 us
  Pallas kernels: 8.92 us -> 9.93 us
    ppermute x28, waiting for transfers between devices: 46.6 us -> 41 us  [exchange(): return lax.ppermute(value, axis, pairs)]
    pallas_call x10 -> x17, Pallas kernels: 2.26 us -> 4.02 us  [call(): pl.pallas_call(kernel, in_specs=[VMEM] * len(args), out_specs=[VMEM] * le...]
  transfers between devices with their start and end apart: 28 -> 28, of which waited for: 20 -> 19; matrix products, arithmetic and copies ran while one was open for 0% -> 0% of each run, Pallas kernels for 6% -> 6%
where the time goes in v2:
time: 81.2 us; the launch traced here: 81 us
  waiting for transfers between devices  41 us (50%)
  starting transfers between devices  29.3 us (36%)
  Pallas kernels  9.93 us (12%)
    ppermute x28, waiting for transfers between devices, exchange(): return lax.ppermute(value, axis, pairs)  41 us
    ppermute x28, starting transfers between devices, exchange(): return lax.ppermute(value, axis, pairs)  29.3 us
    pallas_call x17, Pallas kernels, call(): pl.pallas_call(kernel, in_specs=[VMEM] * len(args), out_specs=[VMEM] * le...  4.02 us
    pallas_call x1, Pallas kernels, project(): pl.pallas_call(functools.partial(project_kernel, len(others) + len(stacks...  1.89 us
    pallas_call x1, Pallas kernels, pack(): pl.pallas_call(pack_kernel, in_specs=[HBM] * 3, out_specs=[VMEM] * 5, out...  1.88 us
  transfers between devices with their start and end apart: 28, of which 19 were waited for; matrix products, arithmetic and copies ran while one was open for 0% of the time, Pallas kernels for 6%

profile of v2, /device:TPU:0, one launch (start us, length us, event | category | flops | bytes accessed | tf_op | source)
XLA Modules:
  0.0 81.0 jit_solution(8893887953901968406)
XLA Ops:
  0.6 1.9 %project.1 = (f32[32,512]{1,0:T(8,128)S(1)}, f32[32,512]{1,0:T(8,128)S(1)}, s32[1,32]{1,0:T(1,128)S(1)}, f32[2,8]{1,0:T(2,128)S(1)}, f32[2,8,64]{2,1,0:T(8,128)S...) custom-call(bf16[64,2048]{1,0:T(8,128)(2,1)} %refs_0_.5, ...), custom_call_target="tpu_custom_call" | custom-call | flops 33554432 | bytes 1048576 | tf_op jit(solution)/shard_map/project/pallas_call | solution.py:223
  2.5 0.6 collective-permute-start.1
  3.1 0.1 collective-permute-start.2
  3.2 0.4 collective-permute-start
  3.6 0.7 shard_map.140
  4.3 1.2 %collective-permute-done.refs_6_ = f32[32,512]{1,0:T(8,128)S(1)} collective-permute-done((f32[32,512]{1,0:T(8,128)S(1)}, f32[32,512]{1,0:T(8,128)S(1)}, u32[]{:S(2)}, u32[]{:S(2)}) %collective-permute-start) | collective-permute-done | bytes 65568 | tf_op jit(solution)/shard_map/ppermute | solution.py:29
  5.5 0.4 shard_map.141
  5.9 0.0 collective-permute-done.2.refs_3_
  5.9 0.5 shard_map.142
  6.4 1.9 %pack.1 = (bf16[2048,128]{1,0:T(8,128)(2,1)S(1)}, bf16[128,1024]{1,0:T(8,128)(2,1)S(1)}, bf16[128,1024]{1,0:T(8,128)(2,1)S(1)}, bf16[128,1024]{1,0:T(8,128)(2,1)S(1)}, bf16[128,1024]{1,0:T(8,128)(2,1)S(1)}) custom-call(bf16[2,2048,128]{2,1,0:T(8,128)(2,1)} %in_hbm, bf16[2,128,2048]{2,1,0:T(8,128)(2,1)} %glu_hbm, bf16[2,128,2048]{2,1,0:T(8,128)(2,1)} %gate_hbm), custom_call_target="tpu_custom_call" | custom-call | flops 8388608 | bytes 3145728 | tf_op jit(solution)/shard_map/pack/pallas_call | solution.py:171
  8.3 0.4 collective-permute-start.10
  8.7 2.6 %collective-permute-start.3 = (bf16[4,32,512]{2,1,0:T(8,128)(2,1)S(1)}, bf16[4,32,512]{2,1,0:T(8,128)(2,1)S(1)}, u32[]{:S(2)}, u32[]{:S(2)}) collective-permute-start(bf16[4,32,512]{2,1,0:T(8,128)(2,1)S(1)} %get-tuple-element.91), channel_id=1, source_target_pairs={{0,2},{2,0},{4,6},{6,4},{8,10},{10,8},{12,14},{14,12},{16,18},{18,... | collective-permute-start | bytes 393224 | tf_op jit(solution)/shard_map/ppermute | solution.py:29
  11.3 1.5 %collective-permute-start.4 = (bf16[4,32,512]{2,1,0:T(8,128)(2,1)S(1)}, bf16[4,32,512]{2,1,0:T(8,128)(2,1)S(1)}, u32[]{:S(2)}, u32[]{:S(2)}) collective-permute-start(bf16[4,32,512]{2,1,0:T(8,128)(2,1)S(1)} %get-tuple-element.92), channel_id=1, source_target_pairs={{0,4},{2,6},{4,0},{6,2},{8,12},{10,14},{12,8},{14,10},{16,20},{18,... | collective-permute-start | bytes 393224 | tf_op jit(solution)/shard_map/ppermute | solution.py:29
  12.9 2.7 %collective-permute-done.3.a_ref = bf16[4,32,512]{2,1,0:T(8,128)(2,1)S(1)} collective-permute-done((bf16[4,32,512]{2,1,0:T(8,128)(2,1)S(1)}, bf16[4,32,512]{2,1,0:T(8,128)(2,1)S(1)}, u32[]{:S(2)}, u32[]{:S(2)}) %collective-permute-start.3) | collective-permute-done | bytes 131104 | tf_op jit(solution)/shard_map/ppermute | solution.py:29
  15.5 4.1 %collective-permute-done.4.b_ref = bf16[4,32,512]{2,1,0:T(8,128)(2,1)S(1)} collective-permute-done((bf16[4,32,512]{2,1,0:T(8,128)(2,1)S(1)}, bf16[4,32,512]{2,1,0:T(8,128)(2,1)S(1)}, u32[]{:S(2)}, u32[]{:S(2)}) %collective-permute-start.4) | collective-permute-done | bytes 131104 | tf_op jit(solution)/shard_map/ppermute | solution.py:29
  19.6 0.1 shard_map.144
  19.7 1.6 %collective-permute-start.6 = (bf16[2,32,512]{2,1,0:T(8,128)(2,1)S(1)}, bf16[2,32,512]{2,1,0:T(8,128)(2,1)S(1)}, u32[]{:S(2)}, u32[]{:S(2)}) collective-permute-start(bf16[2,32,512]{2,1,0:T(8,128)(2,1)S(1)} %get-tuple-element.95), channel_id=1, source_target_pairs={{0,8},{2,10},{4,12},{6,14},{8,0},{10,2},{12,4},{14,6},{16,24},{18,... | collective-permute-start | bytes 196616 | tf_op jit(solution)/shard_map/ppermute | solution.py:29
  21.4 2.7 %collective-permute-done.6.arrived_ref = bf16[2,32,512]{2,1,0:T(8,128)(2,1)S(1)} collective-permute-done((bf16[2,32,512]{2,1,0:T(8,128)(2,1)S(1)}, bf16[2,32,512]{2,1,0:T(8,128)(2,1)S(1)}, u32[]{:S(2)}, u32[]{:S(2)}) %collective-permute-start.6) | collective-permute-done | bytes 65568 | tf_op jit(solution)/shard_map/ppermute | solution.py:29
  24.1 2.7 %collective-permute-start.7 = (bf16[2,32,512]{2,1,0:T(8,128)(2,1)S(1)}, bf16[2,32,512]{2,1,0:T(8,128)(2,1)S(1)}, u32[]{:S(2)}, u32[]{:S(2)}) collective-permute-start(bf16[2,32,512]{2,1,0:T(8,128)(2,1)S(1)} %shard_map.145.own_ref), channel_id=1, source_target_pairs={{0,16},{2,18},{4,20},{6,22},{8,24},{10,26},{12,28},{14,30},{16,0},... | collective-permute-start | bytes 196616 | tf_op jit(solution)/shard_map/ppermute | solution.py:29
  26.7 2.6 %collective-permute-done.7.arrived_ref = bf16[2,32,512]{2,1,0:T(8,128)(2,1)S(1)} collective-permute-done((bf16[2,32,512]{2,1,0:T(8,128)(2,1)S(1)}, bf16[2,32,512]{2,1,0:T(8,128)(2,1)S(1)}, u32[]{:S(2)}, u32[]{:S(2)}) %collective-permute-start.7) | collective-permute-done | bytes 65568 | tf_op jit(solution)/shard_map/ppermute | solution.py:29
  29.4 1.6 %collective-permute-start.8 = (bf16[2,32,256]{2,1,0:T(8,128)(2,1)S(1)}, bf16[2,32,256]{2,1,0:T(8,128)(2,1)S(1)}, u32[]{:S(2)}, u32[]{:S(2)}) collective-permute-start(bf16[2,32,256]{2,1,0:T(8,128)(2,1)S(1)} %shard_map.146.own_ref), channel_id=1, source_target_pairs={{0,8},{2,10},{4,12},{6,14},{8,0},{10,2},{12,4},{14,6},{16,24},{18,... | collective-permute-start | bytes 98312 | tf_op jit(solution)/shard_map/ppermute | solution.py:29
  31.0 1.2 %collective-permute-start.18 = (bf16[128,1024]{1,0:T(8,128)(2,1)S(1)}, bf16[128,1024]{1,0:T(8,128)(2,1)S(1)}, u32[]{:S(2)}, u32[]{:S(2)}) collective-permute-start(bf16[128,1024]{1,0:T(8,128)(2,1)S(1)} %get-tuple-element.116), channel_id=1, source_target_pairs={{0,2},{2,0},{4,6},{6,4},{8,10},{10,8},{12,14},{14,12},{16,18},{18,... | collective-permute-start | bytes 786440 | tf_op jit(solution)/shard_map/ppermute | solution.py:29
  32.2 0.8 %collective-permute-start.19 = (bf16[128,1024]{1,0:T(8,128)(2,1)S(1)}, bf16[128,1024]{1,0:T(8,128)(2,1)S(1)}, u32[]{:S(2)}, u32[]{:S(2)}) collective-permute-start(bf16[128,1024]{1,0:T(8,128)(2,1)S(1)} %get-tuple-element.117), channel_id=1, source_target_pairs={{0,4},{2,6},{4,0},{6,2},{8,12},{10,14},{12,8},{14,10},{16,20},{18,... | collective-permute-start | bytes 786440 | tf_op jit(solution)/shard_map/ppermute | solution.py:29
  33.0 0.3 collective-permute-done.8
  33.4 1.5 %collective-permute-start.20 = (bf16[128,1024]{1,0:T(8,128)(2,1)S(1)}, bf16[128,1024]{1,0:T(8,128)(2,1)S(1)}, u32[]{:S(2)}, u32[]{:S(2)}) collective-permute-start(bf16[128,1024]{1,0:T(8,128)(2,1)S(1)} %get-tuple-element.118), channel_id=1, source_target_pairs={{0,6},{2,4},{4,2},{6,0},{8,14},{10,12},{12,10},{14,8},{16,22},{18,... | collective-permute-start | bytes 786440 | tf_op jit(solution)/shard_map/ppermute | solution.py:29
  34.9 1.5 %collective-permute-start.11 = (bf16[2,2,32,256]{3,2,1,0:T(8,128)(2,1)S(1)}, bf16[2,2,32,256]{3,2,1,0:T(8,128)(2,1)S(1)}, u32[]{:S(2)}, u32[]{:S(2)}) collective-permute-start(bf16[2,2,32,256]{3,2,1,0:T(8,128)(2,1)S(1)} %pad_maximum_fusion.piece), channel_id=1, source_target_pairs={{0,6},{2,4},{4,2},{6,0},{8,14},{10,12},{12,10},{14,8},{16,22},{18,... | collective-permute-start | bytes 196616 | tf_op jit(solution)/shard_map/ppermute | solution.py:29
  36.4 9.1 %collective-permute-done.11.piece = bf16[2,2,32,256]{3,2,1,0:T(8,128)(2,1)S(1)} collective-permute-done((bf16[2,2,32,256]{3,2,1,0:T(8,128)(2,1)S(1)}, bf16[2,2,32,256]{3,2,1,0:T(8,128)(2,1)S(1)}, u32[]{:S(2)}, u32[]{:S(2)}) %collective-permute-start.11) | collective-permute-done | bytes 65568 | tf_op jit(solution)/shard_map/ppermute | solution.py:29
  45.4 0.5 collective-permute-start.12
  45.9 0.0 collective-permute-done.10.refs_3_
  45.9 1.2 %collective-permute-start.13 = (bf16[2,2,32,256]{3,2,1,0:T(8,128)(2,1)S(1)}, bf16[2,2,32,256]{3,2,1,0:T(8,128)(2,1)S(1)}, u32[]{:S(2)}, u32[]{:S(2)}) collective-permute-start(bf16[2,2,32,256]{3,2,1,0:T(8,128)(2,1)S(1)} %pad_maximum_fusion.piece), channel_id=1, source_target_pairs={{0,2},{2,0},{4,6},{6,4},{8,10},{10,8},{12,14},{14,12},{16,18},{18,... | collective-permute-start | bytes 196616 | tf_op jit(solution)/shard_map/ppermute | solution.py:29
  47.2 0.7 shard_map.143
  47.9 0.2 shard_map.147
  48.1 0.2 shard_map.148
  48.3 1.4 %collective-permute-done.12.piece = bf16[2,2,32,256]{3,2,1,0:T(8,128)(2,1)S(1)} collective-permute-done((bf16[2,2,32,256]{3,2,1,0:T(8,128)(2,1)S(1)}, bf16[2,2,32,256]{3,2,1,0:T(8,128)(2,1)S(1)}, u32[]{:S(2)}, u32[]{:S(2)}) %collective-permute-start.12) | collective-permute-done | bytes 65568 | tf_op jit(solution)/shard_map/ppermute | solution.py:29
  49.7 0.2 shard_map.149
  49.9 0.3 collective-permute-done.13.piece
  50.2 0.2 shard_map.150
  50.4 0.4 shard_map.151
  50.8 0.1 collective-permute-start.14
  50.9 1.2 %collective-permute-done.14.arrived_ref = bf16[1,32,128]{2,1,0:T(8,128)(2,1)S(1)} collective-permute-done((bf16[1,32,128]{2,1,0:T(8,128)(2,1)S(1)}, bf16[1,32,128]{2,1,0:T(8,128)(2,1)S(1)}, u32[]{:S(2)}, u32[]{:S(2)}) %collective-permute-start.14) | collective-permute-done | bytes 8224 | tf_op jit(solution)/shard_map/ppermute | solution.py:29
  52.1 1.2 %collective-permute-start.15 = (bf16[64,128]{1,0:T(8,128)(2,1)S(1)}, bf16[64,128]{1,0:T(8,128)(2,1)S(1)}, u32[]{:S(2)}, u32[]{:S(2)}) collective-permute-start(bf16[64,128]{1,0:T(8,128)(2,1)S(1)} %bitcast.13), channel_id=1, source_target_pairs={{0,2},{2,0},{4,6},{6,4},{8,10},{10,8},{12,14},{14,12},{16,18},{18,... | collective-permute-start | bytes 49160 | tf_op jit(solution)/shard_map/ppermute | solution.py:29
  53.3 0.8 %collective-permute-start.16 = (bf16[64,128]{1,0:T(8,128)(2,1)S(1)}, bf16[64,128]{1,0:T(8,128)(2,1)S(1)}, u32[]{:S(2)}, u32[]{:S(2)}) collective-permute-start(bf16[64,128]{1,0:T(8,128)(2,1)S(1)} %bitcast.14), channel_id=1, source_target_pairs={{0,4},{2,6},{4,0},{6,2},{8,12},{10,14},{12,8},{14,10},{16,20},{18,... | collective-permute-start | bytes 49160 | tf_op jit(solution)/shard_map/ppermute | solution.py:29
  54.1 0.0 collective-permute-done.18.refs_5_
  54.1 1.4 %collective-permute-start.17 = (bf16[64,128]{1,0:T(8,128)(2,1)S(1)}, bf16[64,128]{1,0:T(8,128)(2,1)S(1)}, u32[]{:S(2)}, u32[]{:S(2)}) collective-permute-start(bf16[64,128]{1,0:T(8,128)(2,1)S(1)} %bitcast.15), channel_id=1, source_target_pairs={{0,6},{2,4},{4,2},{6,0},{8,14},{10,12},{12,10},{14,8},{16,22},{18,... | collective-permute-start | bytes 49160 | tf_op jit(solution)/shard_map/ppermute | solution.py:29
  55.6 0.0 collective-permute-done.19.refs_6_
  55.6 0.2 collective-permute-done.15.refs_1_
  55.8 1.2 %collective-permute-done.16.refs_2_ = bf16[64,128]{1,0:T(8,128)(2,1)S(1)} collective-permute-done((bf16[64,128]{1,0:T(8,128)(2,1)S(1)}, bf16[64,128]{1,0:T(8,128)(2,1)S(1)}, u32[]{:S(2)}, u32[]{:S(2)}) %collective-permute-start.16) | collective-permute-done | bytes 16416 | tf_op jit(solution)/shard_map/ppermute | solution.py:29
  57.0 1.7 %collective-permute-done.17.refs_3_ = bf16[64,128]{1,0:T(8,128)(2,1)S(1)} collective-permute-done((bf16[64,128]{1,0:T(8,128)(2,1)S(1)}, bf16[64,128]{1,0:T(8,128)(2,1)S(1)}, u32[]{:S(2)}, u32[]{:S(2)}) %collective-permute-start.17) | collective-permute-done | bytes 16416 | tf_op jit(solution)/shard_map/ppermute | solution.py:29
  58.8 0.3 shard_map.153
  59.1 0.6 collective-permute-start.21
  59.7 3.8 %collective-permute-done.21.arrived_ref = bf16[2,64,256]{2,1,0:T(8,128)(2,1)S(1)} collective-permute-done((bf16[2,64,256]{2,1,0:T(8,128)(2,1)S(1)}, bf16[2,64,256]{2,1,0:T(8,128)(2,1)S(1)}, u32[]{:S(2)}, u32[]{:S(2)}) %collective-permute-start.21) | collective-permute-done | bytes 65568 | tf_op jit(solution)/shard_map/ppermute | solution.py:29
  63.5 3.3 %collective-permute-start.22 = (bf16[2,64,256]{2,1,0:T(8,128)(2,1)S(1)}, bf16[2,64,256]{2,1,0:T(8,128)(2,1)S(1)}, u32[]{:S(2)}, u32[]{:S(2)}) collective-permute-start(bf16[2,64,256]{2,1,0:T(8,128)(2,1)S(1)} %shard_map.154.own_ref), channel_id=1, source_target_pairs={{0,16},{2,18},{4,20},{6,22},{8,24},{10,26},{12,28},{14,30},{16,0},... | collective-permute-start | bytes 196616 | tf_op jit(solution)/shard_map/ppermute | solution.py:29
  66.8 1.2 %collective-permute-done.23.arrived_ref = bf16[2,32,128]{2,1,0:T(8,128)(2,1)S(1)} collective-permute-done((bf16[2,32,128]{2,1,0:T(8,128)(2,1)S(1)}, bf16[2,32,128]{2,1,0:T(8,128)(2,1)S(1)}, u32[]{:S(2)}, u32[]{:S(2)}) %collective-permute-start.23) | collective-permute-done | bytes 16416 | tf_op jit(solution)/shard_map/ppermute | solution.py:29
  67.9 1.4 %collective-permute-done.22.arrived_ref = bf16[2,64,256]{2,1,0:T(8,128)(2,1)S(1)} collective-permute-done((bf16[2,64,256]{2,1,0:T(8,128)(2,1)S(1)}, bf16[2,64,256]{2,1,0:T(8,128)(2,1)S(1)}, u32[]{:S(2)}, u32[]{:S(2)}) %collective-permute-start.22) | collective-permute-done | bytes 65568 | tf_op jit(solution)/shard_map/ppermute | solution.py:29
  69.4 0.1 collective-permute-start.24
  69.4 3.9 %collective-permute-done.24 = bf16[2,64,128]{2,1,0:T(8,128)(2,1)S(1)} collective-permute-done((bf16[2,64,128]{2,1,0:T(8,128)(2,1)S(1)}, bf16[2,64,128]{2,1,0:T(8,128)(2,1)S(1)}, u32[]{:S(2)}, u32[]{:S(2)}) %collective-permute-start.24) | collective-permute-done | bytes 32800 | tf_op jit(solution)/shard_map/ppermute | solution.py:29
  73.4 1.5 %collective-permute-start.27 = (bf16[2,2,64,128]{3,2,1,0:T(8,128)(2,1)S(1)}, bf16[2,2,64,128]{3,2,1,0:T(8,128)(2,1)S(1)}, u32[]{:S(2)}, u32[]{:S(2)}) collective-permute-start(bf16[2,2,64,128]{3,2,1,0:T(8,128)(2,1)S(1)} %pad_maximum_fusion.1.refs_0_), channel_id=1, source_target_pairs={{0,6},{2,4},{4,2},{6,0},{8,14},{10,12},{12,10},{14,8},{16,22},{18,... | collective-permute-start | bytes 196616 | tf_op jit(solution)/shard_map/ppermute | solution.py:29
  74.9 1.2 %collective-permute-start.25 = (bf16[2,2,64,128]{3,2,1,0:T(8,128)(2,1)S(1)}, bf16[2,2,64,128]{3,2,1,0:T(8,128)(2,1)S(1)}, u32[]{:S(2)}, u32[]{:S(2)}) collective-permute-start(bf16[2,2,64,128]{3,2,1,0:T(8,128)(2,1)S(1)} %pad_maximum_fusion.1.refs_0_), channel_id=1, source_target_pairs={{0,2},{2,0},{4,6},{6,4},{8,10},{10,8},{12,14},{14,12},{16,18},{18,... | collective-permute-start | bytes 196616 | tf_op jit(solution)/shard_map/ppermute | solution.py:29
  76.1 0.8 %collective-permute-start.26 = (bf16[2,2,64,128]{3,2,1,0:T(8,128)(2,1)S(1)}, bf16[2,2,64,128]{3,2,1,0:T(8,128)(2,1)S(1)}, u32[]{:S(2)}, u32[]{:S(2)}) collective-permute-start(bf16[2,2,64,128]{3,2,1,0:T(8,128)(2,1)S(1)} %pad_maximum_fusion.1.refs_0_), channel_id=1, source_target_pairs={{0,4},{2,6},{4,0},{6,2},{8,12},{10,14},{12,8},{14,10},{16,20},{18,... | collective-permute-start | bytes 196616 | tf_op jit(solution)/shard_map/ppermute | solution.py:29
  76.9 0.7 store.1
  77.6 1.0 %collective-permute-done.27.refs_1_ = bf16[2,2,64,128]{3,2,1,0:T(8,128)(2,1)S(1)} collective-permute-done((bf16[2,2,64,128]{3,2,1,0:T(8,128)(2,1)S(1)}, bf16[2,2,64,128]{3,2,1,0:T(8,128)(2,1)S(1)}, u32[]{:S(2)}, u32[]{:S(2)}) %collective-permute-start.27) | collective-permute-done | bytes 65568 | tf_op jit(solution)/shard_map/ppermute | solution.py:29
  78.6 0.7 settle.2.refs_2_
  79.3 1.0 %collective-permute-done.26.refs_1_ = bf16[2,2,64,128]{3,2,1,0:T(8,128)(2,1)S(1)} collective-permute-done((bf16[2,2,64,128]{3,2,1,0:T(8,128)(2,1)S(1)}, bf16[2,2,64,128]{3,2,1,0:T(8,128)(2,1)S(1)}, u32[]{:S(2)}, u32[]{:S(2)}) %collective-permute-start.26) | collective-permute-done | bytes 65568 | tf_op jit(solution)/shard_map/ppermute | solution.py:29
  80.3 0.7 settle.3
  (19 shorter events, 0.1 us)
Async XLA Ops:
  2.5 3.4 %collective-permute-start.1 = (bf16[128,2048]{1,0:T(8,128)(2,1)S(1)}, bf16[128,2048]{1,0:T(8,128)(2,1)S(1)}, u32[]{:S(2)}, u32[]{:S(2)}) collective-permute-start(bf16[128,2048]{1,0:T(8,128)(2,1)S(1)} %get-tuple-element.77.refs_0_), channel_id=1, source_target_pairs={{0,1},{1,0},{2,3},{3,2},{4,5},{5,4},{6,7},{7,6},{8,9},{9,8},{10,11... | collective-permute-start | bytes 1572872 | tf_op jit(solution)/shard_map/ppermute | solution.py:29
  3.1 2.8 %collective-permute-start.2 = (bf16[128,2048]{1,0:T(8,128)(2,1)S(1)}, bf16[128,2048]{1,0:T(8,128)(2,1)S(1)}, u32[]{:S(2)}, u32[]{:S(2)}) collective-permute-start(bf16[128,2048]{1,0:T(8,128)(2,1)S(1)} %get-tuple-element.78.refs_2_), channel_id=1, source_target_pairs={{0,1},{1,0},{2,3},{3,2},{4,5},{5,4},{6,7},{7,6},{8,9},{9,8},{10,11... | collective-permute-start | bytes 1572872 | tf_op jit(solution)/shard_map/ppermute | solution.py:29
  3.2 2.3 %collective-permute-start = (f32[32,512]{1,0:T(8,128)S(1)}, f32[32,512]{1,0:T(8,128)S(1)}, u32[]{:S(2)}, u32[]{:S(2)}) collective-permute-start(f32[32,512]{1,0:T(8,128)S(1)} %get-tuple-element.75), channel_id=1, source_target_pairs={{0,1},{1,0},{2,3},{3,2},{4,5},{5,4},{6,7},{7,6},{8,9},{9,8},{10,11... | collective-permute-start | bytes 196616 | tf_op jit(solution)/shard_map/ppermute | solution.py:29
  8.3 37.6 %collective-permute-start.10 = (bf16[2048,128]{1,0:T(8,128)(2,1)S(1)}, bf16[2048,128]{1,0:T(8,128)(2,1)S(1)}, u32[]{:S(2)}, u32[]{:S(2)}) collective-permute-start(bf16[2048,128]{1,0:T(8,128)(2,1)S(1)} %get-tuple-element.101.refs_2_), channel_id=1, source_target_pairs={{0,1},{1,0},{2,3},{3,2},{4,5},{5,4},{6,7},{7,6},{8,9},{9,8},{10,11... | collective-permute-start | bytes 1572872 | tf_op jit(solution)/shard_map/ppermute | solution.py:29
  8.7 6.8 %collective-permute-start.3 = (bf16[4,32,512]{2,1,0:T(8,128)(2,1)S(1)}, bf16[4,32,512]{2,1,0:T(8,128)(2,1)S(1)}, u32[]{:S(2)}, u32[]{:S(2)}) collective-permute-start(bf16[4,32,512]{2,1,0:T(8,128)(2,1)S(1)} %get-tuple-element.91), channel_id=1, source_target_pairs={{0,2},{2,0},{4,6},{6,4},{8,10},{10,8},{12,14},{14,12},{16,18},{18,... | collective-permute-start | bytes 393224 | tf_op jit(solution)/shard_map/ppermute | solution.py:29
  11.3 8.3 %collective-permute-start.4 = (bf16[4,32,512]{2,1,0:T(8,128)(2,1)S(1)}, bf16[4,32,512]{2,1,0:T(8,128)(2,1)S(1)}, u32[]{:S(2)}, u32[]{:S(2)}) collective-permute-start(bf16[4,32,512]{2,1,0:T(8,128)(2,1)S(1)} %get-tuple-element.92), channel_id=1, source_target_pairs={{0,4},{2,6},{4,0},{6,2},{8,12},{10,14},{12,8},{14,10},{16,20},{18,... | collective-permute-start | bytes 393224 | tf_op jit(solution)/shard_map/ppermute | solution.py:29
  12.9 6.8 %collective-permute-start.5 = (bf16[4,32,512]{2,1,0:T(8,128)(2,1)S(1)}, bf16[4,32,512]{2,1,0:T(8,128)(2,1)S(1)}, u32[]{:S(2)}, u32[]{:S(2)}) collective-permute-start(bf16[4,32,512]{2,1,0:T(8,128)(2,1)S(1)} %get-tuple-element.93), channel_id=1, source_target_pairs={{0,6},{2,4},{4,2},{6,0},{8,14},{10,12},{12,10},{14,8},{16,22},{18,... | collective-permute-start | bytes 393224 | tf_op jit(solution)/shard_map/ppermute | solution.py:29
  19.7 4.3 %collective-permute-start.6 = (bf16[2,32,512]{2,1,0:T(8,128)(2,1)S(1)}, bf16[2,32,512]{2,1,0:T(8,128)(2,1)S(1)}, u32[]{:S(2)}, u32[]{:S(2)}) collective-permute-start(bf16[2,32,512]{2,1,0:T(8,128)(2,1)S(1)} %get-tuple-element.95), channel_id=1, source_target_pairs={{0,8},{2,10},{4,12},{6,14},{8,0},{10,2},{12,4},{14,6},{16,24},{18,... | collective-permute-start | bytes 196616 | tf_op jit(solution)/shard_map/ppermute | solution.py:29
  24.1 5.3 %collective-permute-start.7 = (bf16[2,32,512]{2,1,0:T(8,128)(2,1)S(1)}, bf16[2,32,512]{2,1,0:T(8,128)(2,1)S(1)}, u32[]{:S(2)}, u32[]{:S(2)}) collective-permute-start(bf16[2,32,512]{2,1,0:T(8,128)(2,1)S(1)} %shard_map.145.own_ref), channel_id=1, source_target_pairs={{0,16},{2,18},{4,20},{6,22},{8,24},{10,26},{12,28},{14,30},{16,0},... | collective-permute-start | bytes 196616 | tf_op jit(solution)/shard_map/ppermute | solution.py:29
  29.3 2.9 %copy-start = (f32[2,2048]{1,0:T(2,128)S(1)}, f32[2,2048]{1,0:T(2,128)}, u32[]{:S(2)}) copy-start(f32[2,2048]{1,0:T(2,128)} %refs_0_.9) | copy-start | bytes 49156
  29.4 4.0 %collective-permute-start.8 = (bf16[2,32,256]{2,1,0:T(8,128)(2,1)S(1)}, bf16[2,32,256]{2,1,0:T(8,128)(2,1)S(1)}, u32[]{:S(2)}, u32[]{:S(2)}) collective-permute-start(bf16[2,32,256]{2,1,0:T(8,128)(2,1)S(1)} %shard_map.146.own_ref), channel_id=1, source_target_pairs={{0,8},{2,10},{4,12},{6,14},{8,0},{10,2},{12,4},{14,6},{16,24},{18,... | collective-permute-start | bytes 98312 | tf_op jit(solution)/shard_map/ppermute | solution.py:29
  31.0 23.2 %collective-permute-start.18 = (bf16[128,1024]{1,0:T(8,128)(2,1)S(1)}, bf16[128,1024]{1,0:T(8,128)(2,1)S(1)}, u32[]{:S(2)}, u32[]{:S(2)}) collective-permute-start(bf16[128,1024]{1,0:T(8,128)(2,1)S(1)} %get-tuple-element.116), channel_id=1, source_target_pairs={{0,2},{2,0},{4,6},{6,4},{8,10},{10,8},{12,14},{14,12},{16,18},{18,... | collective-permute-start | bytes 786440 | tf_op jit(solution)/shard_map/ppermute | solution.py:29
  32.2 2.6 %collective-permute-start.9 = (f32[2,2048]{1,0:T(2,128)S(1)}, f32[2,2048]{1,0:T(2,128)S(1)}, u32[]{:S(2)}, u32[]{:S(2)}) collective-permute-start(f32[2,2048]{1,0:T(2,128)S(1)} %copy-done), channel_id=1, source_target_pairs={{0,1},{1,0},{2,3},{3,2},{4,5},{5,4},{6,7},{7,6},{8,9},{9,8},{10,11... | collective-permute-start | bytes 49160 | tf_op jit(solution)/shard_map/ppermute | solution.py:29
  32.2 23.4 %collective-permute-start.19 = (bf16[128,1024]{1,0:T(8,128)(2,1)S(1)}, bf16[128,1024]{1,0:T(8,128)(2,1)S(1)}, u32[]{:S(2)}, u32[]{:S(2)}) collective-permute-start(bf16[128,1024]{1,0:T(8,128)(2,1)S(1)} %get-tuple-element.117), channel_id=1, source_target_pairs={{0,4},{2,6},{4,0},{6,2},{8,12},{10,14},{12,8},{14,10},{16,20},{18,... | collective-permute-start | bytes 786440 | tf_op jit(solution)/shard_map/ppermute | solution.py:29
  33.4 22.2 %collective-permute-start.20 = (bf16[128,1024]{1,0:T(8,128)(2,1)S(1)}, bf16[128,1024]{1,0:T(8,128)(2,1)S(1)}, u32[]{:S(2)}, u32[]{:S(2)}) collective-permute-start(bf16[128,1024]{1,0:T(8,128)(2,1)S(1)} %get-tuple-element.118), channel_id=1, source_target_pairs={{0,6},{2,4},{4,2},{6,0},{8,14},{10,12},{12,10},{14,8},{16,22},{18,... | collective-permute-start | bytes 786440 | tf_op jit(solution)/shard_map/ppermute | solution.py:29
  34.9 10.6 %collective-permute-start.11 = (bf16[2,2,32,256]{3,2,1,0:T(8,128)(2,1)S(1)}, bf16[2,2,32,256]{3,2,1,0:T(8,128)(2,1)S(1)}, u32[]{:S(2)}, u32[]{:S(2)}) collective-permute-start(bf16[2,2,32,256]{3,2,1,0:T(8,128)(2,1)S(1)} %pad_maximum_fusion.piece), channel_id=1, source_target_pairs={{0,6},{2,4},{4,2},{6,0},{8,14},{10,12},{12,10},{14,8},{16,22},{18,... | collective-permute-start | bytes 196616 | tf_op jit(solution)/shard_map/ppermute | solution.py:29
  45.4 4.3 %collective-permute-start.12 = (bf16[2,2,32,256]{3,2,1,0:T(8,128)(2,1)S(1)}, bf16[2,2,32,256]{3,2,1,0:T(8,128)(2,1)S(1)}, u32[]{:S(2)}, u32[]{:S(2)}) collective-permute-start(bf16[2,2,32,256]{3,2,1,0:T(8,128)(2,1)S(1)} %pad_maximum_fusion.piece), channel_id=1, source_target_pairs={{0,4},{2,6},{4,0},{6,2},{8,12},{10,14},{12,8},{14,10},{16,20},{18,... | collective-permute-start | bytes 196616 | tf_op jit(solution)/shard_map/ppermute | solution.py:29
  45.9 4.3 %collective-permute-start.13 = (bf16[2,2,32,256]{3,2,1,0:T(8,128)(2,1)S(1)}, bf16[2,2,32,256]{3,2,1,0:T(8,128)(2,1)S(1)}, u32[]{:S(2)}, u32[]{:S(2)}) collective-permute-start(bf16[2,2,32,256]{3,2,1,0:T(8,128)(2,1)S(1)} %pad_maximum_fusion.piece), channel_id=1, source_target_pairs={{0,2},{2,0},{4,6},{6,4},{8,10},{10,8},{12,14},{14,12},{16,18},{18,... | collective-permute-start | bytes 196616 | tf_op jit(solution)/shard_map/ppermute | solution.py:29
  50.8 1.2 %collective-permute-start.14 = (bf16[1,32,128]{2,1,0:T(8,128)(2,1)S(1)}, bf16[1,32,128]{2,1,0:T(8,128)(2,1)S(1)}, u32[]{:S(2)}, u32[]{:S(2)}) collective-permute-start(bf16[1,32,128]{2,1,0:T(8,128)(2,1)S(1)} %bitcast.17), channel_id=1, source_target_pairs={{0,1},{1,0},{2,3},{3,2},{4,5},{5,4},{6,7},{7,6},{8,9},{9,8},{10,11... | collective-permute-start | bytes 24584 | tf_op jit(solution)/shard_map/ppermute | solution.py:29
  52.1 3.7 %collective-permute-start.15 = (bf16[64,128]{1,0:T(8,128)(2,1)S(1)}, bf16[64,128]{1,0:T(8,128)(2,1)S(1)}, u32[]{:S(2)}, u32[]{:S(2)}) collective-permute-start(bf16[64,128]{1,0:T(8,128)(2,1)S(1)} %bitcast.13), channel_id=1, source_target_pairs={{0,2},{2,0},{4,6},{6,4},{8,10},{10,8},{12,14},{14,12},{16,18},{18,... | collective-permute-start | bytes 49160 | tf_op jit(solution)/shard_map/ppermute | solution.py:29
  53.3 3.7 %collective-permute-start.16 = (bf16[64,128]{1,0:T(8,128)(2,1)S(1)}, bf16[64,128]{1,0:T(8,128)(2,1)S(1)}, u32[]{:S(2)}, u32[]{:S(2)}) collective-permute-start(bf16[64,128]{1,0:T(8,128)(2,1)S(1)} %bitcast.14), channel_id=1, source_target_pairs={{0,4},{2,6},{4,0},{6,2},{8,12},{10,14},{12,8},{14,10},{16,20},{18,... | collective-permute-start | bytes 49160 | tf_op jit(solution)/shard_map/ppermute | solution.py:29
  54.1 4.6 %collective-permute-start.17 = (bf16[64,128]{1,0:T(8,128)(2,1)S(1)}, bf16[64,128]{1,0:T(8,128)(2,1)S(1)}, u32[]{:S(2)}, u32[]{:S(2)}) collective-permute-start(bf16[64,128]{1,0:T(8,128)(2,1)S(1)} %bitcast.15), channel_id=1, source_target_pairs={{0,6},{2,4},{4,2},{6,0},{8,14},{10,12},{12,10},{14,8},{16,22},{18,... | collective-permute-start | bytes 49160 | tf_op jit(solution)/shard_map/ppermute | solution.py:29
  59.1 4.3 %collective-permute-start.21 = (bf16[2,64,256]{2,1,0:T(8,128)(2,1)S(1)}, bf16[2,64,256]{2,1,0:T(8,128)(2,1)S(1)}, u32[]{:S(2)}, u32[]{:S(2)}) collective-permute-start(bf16[2,64,256]{2,1,0:T(8,128)(2,1)S(1)} %get-tuple-element.120), channel_id=1, source_target_pairs={{0,8},{2,10},{4,12},{6,14},{8,0},{10,2},{12,4},{14,6},{16,24},{18,... | collective-permute-start | bytes 196616 | tf_op jit(solution)/shard_map/ppermute | solution.py:29
  63.5 5.9 %collective-permute-start.22 = (bf16[2,64,256]{2,1,0:T(8,128)(2,1)S(1)}, bf16[2,64,256]{2,1,0:T(8,128)(2,1)S(1)}, u32[]{:S(2)}, u32[]{:S(2)}) collective-permute-start(bf16[2,64,256]{2,1,0:T(8,128)(2,1)S(1)} %shard_map.154.own_ref), channel_id=1, source_target_pairs={{0,16},{2,18},{4,20},{6,22},{8,24},{10,26},{12,28},{14,30},{16,0},... | collective-permute-start | bytes 196616 | tf_op jit(solution)/shard_map/ppermute | solution.py:29
  66.7 1.2 %collective-permute-start.23 = (bf16[2,32,128]{2,1,0:T(8,128)(2,1)S(1)}, bf16[2,32,128]{2,1,0:T(8,128)(2,1)S(1)}, u32[]{:S(2)}, u32[]{:S(2)}) collective-permute-start(bf16[2,32,128]{2,1,0:T(8,128)(2,1)S(1)} %slice.4), channel_id=1, source_target_pairs={{0,1},{1,0},{2,3},{3,2},{4,5},{5,4},{6,7},{7,6},{8,9},{9,8},{10,11... | collective-permute-start | bytes 49160 | tf_op jit(solution)/shard_map/ppermute | solution.py:29
  69.4 4.0 %collective-permute-start.24 = (bf16[2,64,128]{2,1,0:T(8,128)(2,1)S(1)}, bf16[2,64,128]{2,1,0:T(8,128)(2,1)S(1)}, u32[]{:S(2)}, u32[]{:S(2)}) collective-permute-start(bf16[2,64,128]{2,1,0:T(8,128)(2,1)S(1)} %shard_map.156), channel_id=1, source_target_pairs={{0,8},{2,10},{4,12},{6,14},{8,0},{10,2},{12,4},{14,6},{16,24},{18,... | collective-permute-start | bytes 98312 | tf_op jit(solution)/shard_map/ppermute | solution.py:29
  73.4 5.2 %collective-permute-start.27 = (bf16[2,2,64,128]{3,2,1,0:T(8,128)(2,1)S(1)}, bf16[2,2,64,128]{3,2,1,0:T(8,128)(2,1)S(1)}, u32[]{:S(2)}, u32[]{:S(2)}) collective-permute-start(bf16[2,2,64,128]{3,2,1,0:T(8,128)(2,1)S(1)} %pad_maximum_fusion.1.refs_0_), channel_id=1, source_target_pairs={{0,6},{2,4},{4,2},{6,0},{8,14},{10,12},{12,10},{14,8},{16,22},{18,... | collective-permute-start | bytes 196616 | tf_op jit(solution)/shard_map/ppermute | solution.py:29
  74.9 4.4 %collective-permute-start.25 = (bf16[2,2,64,128]{3,2,1,0:T(8,128)(2,1)S(1)}, bf16[2,2,64,128]{3,2,1,0:T(8,128)(2,1)S(1)}, u32[]{:S(2)}, u32[]{:S(2)}) collective-permute-start(bf16[2,2,64,128]{3,2,1,0:T(8,128)(2,1)S(1)} %pad_maximum_fusion.1.refs_0_), channel_id=1, source_target_pairs={{0,2},{2,0},{4,6},{6,4},{8,10},{10,8},{12,14},{14,12},{16,18},{18,... | collective-permute-start | bytes 196616 | tf_op jit(solution)/shard_map/ppermute | solution.py:29
  76.1 4.3 %collective-permute-start.26 = (bf16[2,2,64,128]{3,2,1,0:T(8,128)(2,1)S(1)}, bf16[2,2,64,128]{3,2,1,0:T(8,128)(2,1)S(1)}, u32[]{:S(2)}, u32[]{:S(2)}) collective-permute-start(bf16[2,2,64,128]{3,2,1,0:T(8,128)(2,1)S(1)} %pad_maximum_fusion.1.refs_0_), channel_id=1, source_target_pairs={{0,4},{2,6},{4,0},{6,2},{8,12},{10,14},{12,8},{14,10},{16,20},{18,... | collective-permute-start | bytes 196616 | tf_op jit(solution)/shard_map/ppermute | solution.py:29

commit v3 on v2

--- a/solution.py
+++ b/solution.py
@@ -340,32 +340,42 @@
     )(*states)
 
 
-def product_kernel(chunk, readout_ref, *refs):
-    weights, outs, spread = refs[:-5], refs[-5:-1], refs[-1]
-    count = len(weights)
-    low, _, _ = corner()
-    readout = readout_ref[...]
-    for w in range(count):
-        value = jnp.dot(readout, weights[w][...], preferred_element_type=F32)
+def half_kernel(chunk, readout_ref, *refs):
+    weights, spread = refs[:-1], refs[-1]
+    for w, ref in enumerate(weights):
+        value = jnp.dot(readout_ref[...], ref[...], preferred_element_type=F32)
         for j in range(16):
             spread[w, j] = value[:, j * chunk : (j + 1) * chunk]
+
+
+def product_kernel(chunk, readout_ref, mine, *refs):
+    weights, outs, theirs = refs[:2], refs[2:6], refs[6]
+    low, _, _ = corner()
+    half_kernel(chunk, readout_ref, *weights, theirs)
     for k in range(4):
         for h in range(4):
-            for w in range(count):
-                outs[k][h, :, w * chunk : (w + 1) * chunk] = spread[w, h * 4 + (low ^ k)].astype(
-                    outs[k].dtype
-                )
+            for w in range(4):
+                source = (mine, theirs)[w % 2]
+                outs[k][h, :, w * chunk : (w + 1) * chunk] = source[
+                    w // 2, h * 4 + (low ^ k)
+                ].astype(outs[k].dtype)
 
 
 def products(dims, readout, weights):
     _, _, _, _, own, feats = dims
     chunk = feats // 16
     shape = (4, own, len(weights) * chunk)
+    half = (2, 16, own, chunk)
+    (mine,) = call(
+        functools.partial(half_kernel, chunk),
+        (readout, weights[0], weights[2]),
+        [struct(half, F32)],
+    )
     return call(
         functools.partial(product_kernel, chunk),
-        (readout, *weights),
+        (readout, mine, weights[1], weights[3]),
         [struct(shape, F32)] + [struct(shape, BF16)] * 3,
-        [pltpu.VMEM((len(weights), 16, own, chunk), F32)],
+        [pltpu.VMEM(half, F32)],
         8,
     )
 
@@ -630,14 +640,13 @@
         jnp.swapaxes(in_mat, 3, 4).reshape(layers, 2, width, -1),
         output_matrices.reshape(layers, 2, width, -1),
         skip,
-        state,
     )
     keep, send, others, outward = project(
         dims, tokens, norm_gain, w_in, others, (w_glu, w_gate)
     )
     pieces = [keep, core_swap(send)]
     outward = [outward[0], core_swap(outward[0]), outward[1], core_swap(outward[1])]
-    consts = (*prepare(0, own, *others[:6]), *others[6:])
+    consts = (*prepare(0, own, *others[:6]), *others[6:], state)
 
     readout, new_first, before = recur(0, dims, consts, pieces)
     parts = products(dims, readout, outward)
@@ -646,7 +655,7 @@
     inward, *packs = pack(*stacks[:3])
     gain = stacks[3]
     *others, _ = lax.optimization_barrier((*others, parts[0]))
-    later_consts = (*prepare(1, own, *others[:6]), *others[6:])
+    later_consts = (*prepare(1, own, *others[:6]), *others[6:], state)
     slabs = [norm_gain, core_swap(gain), inward, core_swap(inward)]
     keep, send = call(
         fold_low_kernel,

time: 81.2 us -> 81.3 us (level)
    pallas_call x17 -> x18, Pallas kernels: 4.02 us -> 4.11 us  [call(): pl.pallas_call(kernel, in_specs=[VMEM] * len(args), out_specs=[VMEM] * le...]
where the time goes in v3:
time: 81.3 us; the launch traced here: 81.1 us
  waiting for transfers between devices  40.9 us (50%)
  starting transfers between devices  29.4 us (36%)
  Pallas kernels  9.93 us (12%)
    ppermute x28, waiting for transfers between devices, exchange(): return lax.ppermute(value, axis, pairs)  40.9 us
    ppermute x28, starting transfers between devices, exchange(): return lax.ppermute(value, axis, pairs)  29.4 us
    pallas_call x18, Pallas kernels, call(): pl.pallas_call(kernel, in_specs=[VMEM] * len(args), out_specs=[VMEM] * le...  4.11 us
    pallas_call x1, Pallas kernels, pack(): pl.pallas_call(pack_kernel, in_specs=[HBM] * 3, out_specs=[VMEM] * 5, out...  1.88 us
    pallas_call x1, Pallas kernels, project(): pl.pallas_call(functools.partial(project_kernel, len(others) + len(stacks...  1.8 us
  transfers between devices with their start and end apart: 28, of which 19 were waited for; matrix products, arithmetic and copies ran while one was open for 0% of the time, Pallas kernels for 6%

profile of v3, /device:TPU:0, one launch (start us, length us, event | category | flops | bytes accessed | tf_op | source)
XLA Modules:
  0.0 81.1 jit_solution(6250004616467767018)
XLA Ops:
  0.6 1.8 %project.1 = (f32[32,512]{1,0:T(8,128)S(1)}, f32[32,512]{1,0:T(8,128)S(1)}, s32[1,32]{1,0:T(1,128)S(1)}, f32[2,8]{1,0:T(2,128)S(1)}, f32[2,8,64]{2,1,0:T(8,128)S...) custom-call(bf16[64,2048]{1,0:T(8,128)(2,1)} %refs_0_.5, ...), custom_call_target="tpu_custom_call" | custom-call | flops 33554432 | bytes 1048576 | tf_op jit(solution)/shard_map/project/pallas_call | solution.py:223
  2.4 0.6 collective-permute-start.1
  3.0 0.1 collective-permute-start.2
  3.1 0.4 collective-permute-start
  3.5 0.7 shard_map.140
  4.2 1.2 %collective-permute-done.refs_6_ = f32[32,512]{1,0:T(8,128)S(1)} collective-permute-done((f32[32,512]{1,0:T(8,128)S(1)}, f32[32,512]{1,0:T(8,128)S(1)}, u32[]{:S(2)}, u32[]{:S(2)}) %collective-permute-start) | collective-permute-done | bytes 65568 | tf_op jit(solution)/shard_map/ppermute | solution.py:29
  5.4 0.4 shard_map.141
  5.8 0.3 shard_map.142.mine
  6.1 0.0 collective-permute-done.1.refs_0_
  6.1 0.0 collective-permute-done.2.refs_1_
  6.1 0.3 shard_map.143
  6.4 1.9 %pack.1 = (bf16[2048,128]{1,0:T(8,128)(2,1)S(1)}, bf16[128,1024]{1,0:T(8,128)(2,1)S(1)}, bf16[128,1024]{1,0:T(8,128)(2,1)S(1)}, bf16[128,1024]{1,0:T(8,128)(2,1)S(1)}, bf16[128,1024]{1,0:T(8,128)(2,1)S(1)}) custom-call(bf16[2,2048,128]{2,1,0:T(8,128)(2,1)} %in_hbm, bf16[2,128,2048]{2,1,0:T(8,128)(2,1)} %glu_hbm, bf16[2,128,2048]{2,1,0:T(8,128)(2,1)} %gate_hbm), custom_call_target="tpu_custom_call" | custom-call | flops 8388608 | bytes 3145728 | tf_op jit(solution)/shard_map/pack/pallas_call | solution.py:171
  8.3 0.4 collective-permute-start.10
  8.7 2.6 %collective-permute-start.3 = (bf16[4,32,512]{2,1,0:T(8,128)(2,1)S(1)}, bf16[4,32,512]{2,1,0:T(8,128)(2,1)S(1)}, u32[]{:S(2)}, u32[]{:S(2)}) collective-permute-start(bf16[4,32,512]{2,1,0:T(8,128)(2,1)S(1)} %get-tuple-element.87), channel_id=1, source_target_pairs={{0,2},{2,0},{4,6},{6,4},{8,10},{10,8},{12,14},{14,12},{16,18},{18,... | collective-permute-start | bytes 393224 | tf_op jit(solution)/shard_map/ppermute | solution.py:29
  11.4 1.5 %collective-permute-start.4 = (bf16[4,32,512]{2,1,0:T(8,128)(2,1)S(1)}, bf16[4,32,512]{2,1,0:T(8,128)(2,1)S(1)}, u32[]{:S(2)}, u32[]{:S(2)}) collective-permute-start(bf16[4,32,512]{2,1,0:T(8,128)(2,1)S(1)} %get-tuple-element.88), channel_id=1, source_target_pairs={{0,4},{2,6},{4,0},{6,2},{8,12},{10,14},{12,8},{14,10},{16,20},{18,... | collective-permute-start | bytes 393224 | tf_op jit(solution)/shard_map/ppermute | solution.py:29
  12.9 2.7 %collective-permute-done.3.a_ref = bf16[4,32,512]{2,1,0:T(8,128)(2,1)S(1)} collective-permute-done((bf16[4,32,512]{2,1,0:T(8,128)(2,1)S(1)}, bf16[4,32,512]{2,1,0:T(8,128)(2,1)S(1)}, u32[]{:S(2)}, u32[]{:S(2)}) %collective-permute-start.3) | collective-permute-done | bytes 131104 | tf_op jit(solution)/shard_map/ppermute | solution.py:29
  15.6 4.1 %collective-permute-done.4.b_ref = bf16[4,32,512]{2,1,0:T(8,128)(2,1)S(1)} collective-permute-done((bf16[4,32,512]{2,1,0:T(8,128)(2,1)S(1)}, bf16[4,32,512]{2,1,0:T(8,128)(2,1)S(1)}, u32[]{:S(2)}, u32[]{:S(2)}) %collective-permute-start.4) | collective-permute-done | bytes 131104 | tf_op jit(solution)/shard_map/ppermute | solution.py:29
  19.7 0.0 collective-permute-done.5.c_ref
  19.7 0.1 shard_map.145
  19.7 1.6 %collective-permute-start.6 = (bf16[2,32,512]{2,1,0:T(8,128)(2,1)S(1)}, bf16[2,32,512]{2,1,0:T(8,128)(2,1)S(1)}, u32[]{:S(2)}, u32[]{:S(2)}) collective-permute-start(bf16[2,32,512]{2,1,0:T(8,128)(2,1)S(1)} %get-tuple-element.91), channel_id=1, source_target_pairs={{0,8},{2,10},{4,12},{6,14},{8,0},{10,2},{12,4},{14,6},{16,24},{18,... | collective-permute-start | bytes 196616 | tf_op jit(solution)/shard_map/ppermute | solution.py:29
  21.4 2.7 %collective-permute-done.6.arrived_ref = bf16[2,32,512]{2,1,0:T(8,128)(2,1)S(1)} collective-permute-done((bf16[2,32,512]{2,1,0:T(8,128)(2,1)S(1)}, bf16[2,32,512]{2,1,0:T(8,128)(2,1)S(1)}, u32[]{:S(2)}, u32[]{:S(2)}) %collective-permute-start.6) | collective-permute-done | bytes 65568 | tf_op jit(solution)/shard_map/ppermute | solution.py:29
  24.1 2.6 %collective-permute-start.7 = (bf16[2,32,512]{2,1,0:T(8,128)(2,1)S(1)}, bf16[2,32,512]{2,1,0:T(8,128)(2,1)S(1)}, u32[]{:S(2)}, u32[]{:S(2)}) collective-permute-start(bf16[2,32,512]{2,1,0:T(8,128)(2,1)S(1)} %shard_map.146.own_ref), channel_id=1, source_target_pairs={{0,16},{2,18},{4,20},{6,22},{8,24},{10,26},{12,28},{14,30},{16,0},... | collective-permute-start | bytes 196616 | tf_op jit(solution)/shard_map/ppermute | solution.py:29
  26.7 2.6 %collective-permute-done.7.arrived_ref = bf16[2,32,512]{2,1,0:T(8,128)(2,1)S(1)} collective-permute-done((bf16[2,32,512]{2,1,0:T(8,128)(2,1)S(1)}, bf16[2,32,512]{2,1,0:T(8,128)(2,1)S(1)}, u32[]{:S(2)}, u32[]{:S(2)}) %collective-permute-start.7) | collective-permute-done | bytes 65568 | tf_op jit(solution)/shard_map/ppermute | solution.py:29
  29.4 1.6 %collective-permute-start.8 = (bf16[2,32,256]{2,1,0:T(8,128)(2,1)S(1)}, bf16[2,32,256]{2,1,0:T(8,128)(2,1)S(1)}, u32[]{:S(2)}, u32[]{:S(2)}) collective-permute-start(bf16[2,32,256]{2,1,0:T(8,128)(2,1)S(1)} %shard_map.147.own_ref), channel_id=1, source_target_pairs={{0,8},{2,10},{4,12},{6,14},{8,0},{10,2},{12,4},{14,6},{16,24},{18,... | collective-permute-start | bytes 98312 | tf_op jit(solution)/shard_map/ppermute | solution.py:29
  31.0 1.2 %collective-permute-start.18 = (bf16[128,1024]{1,0:T(8,128)(2,1)S(1)}, bf16[128,1024]{1,0:T(8,128)(2,1)S(1)}, u32[]{:S(2)}, u32[]{:S(2)}) collective-permute-start(bf16[128,1024]{1,0:T(8,128)(2,1)S(1)} %get-tuple-element.112), channel_id=1, source_target_pairs={{0,2},{2,0},{4,6},{6,4},{8,10},{10,8},{12,14},{14,12},{16,18},{18,... | collective-permute-start | bytes 786440 | tf_op jit(solution)/shard_map/ppermute | solution.py:29
  32.2 0.8 %collective-permute-start.19 = (bf16[128,1024]{1,0:T(8,128)(2,1)S(1)}, bf16[128,1024]{1,0:T(8,128)(2,1)S(1)}, u32[]{:S(2)}, u32[]{:S(2)}) collective-permute-start(bf16[128,1024]{1,0:T(8,128)(2,1)S(1)} %get-tuple-element.113), channel_id=1, source_target_pairs={{0,4},{2,6},{4,0},{6,2},{8,12},{10,14},{12,8},{14,10},{16,20},{18,... | collective-permute-start | bytes 786440 | tf_op jit(solution)/shard_map/ppermute | solution.py:29
  33.1 0.3 collective-permute-done.8
  33.4 1.5 %collective-permute-start.20 = (bf16[128,1024]{1,0:T(8,128)(2,1)S(1)}, bf16[128,1024]{1,0:T(8,128)(2,1)S(1)}, u32[]{:S(2)}, u32[]{:S(2)}) collective-permute-start(bf16[128,1024]{1,0:T(8,128)(2,1)S(1)} %get-tuple-element.114), channel_id=1, source_target_pairs={{0,6},{2,4},{4,2},{6,0},{8,14},{10,12},{12,10},{14,8},{16,22},{18,... | collective-permute-start | bytes 786440 | tf_op jit(solution)/shard_map/ppermute | solution.py:29
  34.9 1.5 %collective-permute-start.11 = (bf16[2,2,32,256]{3,2,1,0:T(8,128)(2,1)S(1)}, bf16[2,2,32,256]{3,2,1,0:T(8,128)(2,1)S(1)}, u32[]{:S(2)}, u32[]{:S(2)}) collective-permute-start(bf16[2,2,32,256]{3,2,1,0:T(8,128)(2,1)S(1)} %pad_maximum_fusion.piece), channel_id=1, source_target_pairs={{0,6},{2,4},{4,2},{6,0},{8,14},{10,12},{12,10},{14,8},{16,22},{18,... | collective-permute-start | bytes 196616 | tf_op jit(solution)/shard_map/ppermute | solution.py:29
  36.4 9.1 %collective-permute-done.11.piece = bf16[2,2,32,256]{3,2,1,0:T(8,128)(2,1)S(1)} collective-permute-done((bf16[2,2,32,256]{3,2,1,0:T(8,128)(2,1)S(1)}, bf16[2,2,32,256]{3,2,1,0:T(8,128)(2,1)S(1)}, u32[]{:S(2)}, u32[]{:S(2)}) %collective-permute-start.11) | collective-permute-done | bytes 65568 | tf_op jit(solution)/shard_map/ppermute | solution.py:29
  45.5 0.5 collective-permute-start.12
  46.0 1.2 %collective-permute-start.13 = (bf16[2,2,32,256]{3,2,1,0:T(8,128)(2,1)S(1)}, bf16[2,2,32,256]{3,2,1,0:T(8,128)(2,1)S(1)}, u32[]{:S(2)}, u32[]{:S(2)}) collective-permute-start(bf16[2,2,32,256]{3,2,1,0:T(8,128)(2,1)S(1)} %pad_maximum_fusion.piece), channel_id=1, source_target_pairs={{0,2},{2,0},{4,6},{6,4},{8,10},{10,8},{12,14},{14,12},{16,18},{18,... | collective-permute-start | bytes 196616 | tf_op jit(solution)/shard_map/ppermute | solution.py:29
  47.2 0.7 shard_map.144
  47.9 0.2 shard_map.148
  48.1 0.2 shard_map.149
  48.3 1.4 %collective-permute-done.12.piece = bf16[2,2,32,256]{3,2,1,0:T(8,128)(2,1)S(1)} collective-permute-done((bf16[2,2,32,256]{3,2,1,0:T(8,128)(2,1)S(1)}, bf16[2,2,32,256]{3,2,1,0:T(8,128)(2,1)S(1)}, u32[]{:S(2)}, u32[]{:S(2)}) %collective-permute-start.12) | collective-permute-done | bytes 65568 | tf_op jit(solution)/shard_map/ppermute | solution.py:29
  49.7 0.2 shard_map.150
  49.9 0.3 collective-permute-done.13.piece
  50.2 0.2 shard_map.151
  50.4 0.4 shard_map.152
  50.9 0.1 collective-permute-start.14
  50.9 1.2 %collective-permute-done.14.arrived_ref = bf16[1,32,128]{2,1,0:T(8,128)(2,1)S(1)} collective-permute-done((bf16[1,32,128]{2,1,0:T(8,128)(2,1)S(1)}, bf16[1,32,128]{2,1,0:T(8,128)(2,1)S(1)}, u32[]{:S(2)}, u32[]{:S(2)}) %collective-permute-start.14) | collective-permute-done | bytes 8224 | tf_op jit(solution)/shard_map/ppermute | solution.py:29
  52.1 1.2 %collective-permute-start.15 = (bf16[64,128]{1,0:T(8,128)(2,1)S(1)}, bf16[64,128]{1,0:T(8,128)(2,1)S(1)}, u32[]{:S(2)}, u32[]{:S(2)}) collective-permute-start(bf16[64,128]{1,0:T(8,128)(2,1)S(1)} %bitcast.13), channel_id=1, source_target_pairs={{0,2},{2,0},{4,6},{6,4},{8,10},{10,8},{12,14},{14,12},{16,18},{18,... | collective-permute-start | bytes 49160 | tf_op jit(solution)/shard_map/ppermute | solution.py:29
  53.3 0.8 %collective-permute-start.16 = (bf16[64,128]{1,0:T(8,128)(2,1)S(1)}, bf16[64,128]{1,0:T(8,128)(2,1)S(1)}, u32[]{:S(2)}, u32[]{:S(2)}) collective-permute-start(bf16[64,128]{1,0:T(8,128)(2,1)S(1)} %bitcast.14), channel_id=1, source_target_pairs={{0,4},{2,6},{4,0},{6,2},{8,12},{10,14},{12,8},{14,10},{16,20},{18,... | collective-permute-start | bytes 49160 | tf_op jit(solution)/shard_map/ppermute | solution.py:29
  54.2 1.4 %collective-permute-start.17 = (bf16[64,128]{1,0:T(8,128)(2,1)S(1)}, bf16[64,128]{1,0:T(8,128)(2,1)S(1)}, u32[]{:S(2)}, u32[]{:S(2)}) collective-permute-start(bf16[64,128]{1,0:T(8,128)(2,1)S(1)} %bitcast.15), channel_id=1, source_target_pairs={{0,6},{2,4},{4,2},{6,0},{8,14},{10,12},{12,10},{14,8},{16,22},{18,... | collective-permute-start | bytes 49160 | tf_op jit(solution)/shard_map/ppermute | solution.py:29
  55.6 0.2 collective-permute-done.15.refs_1_
  55.8 1.2 %collective-permute-done.16.refs_2_ = bf16[64,128]{1,0:T(8,128)(2,1)S(1)} collective-permute-done((bf16[64,128]{1,0:T(8,128)(2,1)S(1)}, bf16[64,128]{1,0:T(8,128)(2,1)S(1)}, u32[]{:S(2)}, u32[]{:S(2)}) %collective-permute-start.16) | collective-permute-done | bytes 16416 | tf_op jit(solution)/shard_map/ppermute | solution.py:29
  57.1 1.7 %collective-permute-done.17.refs_3_ = bf16[64,128]{1,0:T(8,128)(2,1)S(1)} collective-permute-done((bf16[64,128]{1,0:T(8,128)(2,1)S(1)}, bf16[64,128]{1,0:T(8,128)(2,1)S(1)}, u32[]{:S(2)}, u32[]{:S(2)}) %collective-permute-start.17) | collective-permute-done | bytes 16416 | tf_op jit(solution)/shard_map/ppermute | solution.py:29
  58.8 0.3 shard_map.154
  59.1 0.6 collective-permute-start.21
  59.7 3.8 %collective-permute-done.21.arrived_ref = bf16[2,64,256]{2,1,0:T(8,128)(2,1)S(1)} collective-permute-done((bf16[2,64,256]{2,1,0:T(8,128)(2,1)S(1)}, bf16[2,64,256]{2,1,0:T(8,128)(2,1)S(1)}, u32[]{:S(2)}, u32[]{:S(2)}) %collective-permute-start.21) | collective-permute-done | bytes 65568 | tf_op jit(solution)/shard_map/ppermute | solution.py:29
  63.5 3.3 %collective-permute-start.22 = (bf16[2,64,256]{2,1,0:T(8,128)(2,1)S(1)}, bf16[2,64,256]{2,1,0:T(8,128)(2,1)S(1)}, u32[]{:S(2)}, u32[]{:S(2)}) collective-permute-start(bf16[2,64,256]{2,1,0:T(8,128)(2,1)S(1)} %shard_map.155.own_ref), channel_id=1, source_target_pairs={{0,16},{2,18},{4,20},{6,22},{8,24},{10,26},{12,28},{14,30},{16,0},... | collective-permute-start | bytes 196616 | tf_op jit(solution)/shard_map/ppermute | solution.py:29
  66.8 1.2 %collective-permute-done.23.arrived_ref = bf16[2,32,128]{2,1,0:T(8,128)(2,1)S(1)} collective-permute-done((bf16[2,32,128]{2,1,0:T(8,128)(2,1)S(1)}, bf16[2,32,128]{2,1,0:T(8,128)(2,1)S(1)}, u32[]{:S(2)}, u32[]{:S(2)}) %collective-permute-start.23) | collective-permute-done | bytes 16416 | tf_op jit(solution)/shard_map/ppermute | solution.py:29
  68.0 1.3 %collective-permute-done.22.arrived_ref = bf16[2,64,256]{2,1,0:T(8,128)(2,1)S(1)} collective-permute-done((bf16[2,64,256]{2,1,0:T(8,128)(2,1)S(1)}, bf16[2,64,256]{2,1,0:T(8,128)(2,1)S(1)}, u32[]{:S(2)}, u32[]{:S(2)}) %collective-permute-start.22) | collective-permute-done | bytes 65568 | tf_op jit(solution)/shard_map/ppermute | solution.py:29
  69.4 0.1 collective-permute-start.24
  69.5 3.9 %collective-permute-done.24 = bf16[2,64,128]{2,1,0:T(8,128)(2,1)S(1)} collective-permute-done((bf16[2,64,128]{2,1,0:T(8,128)(2,1)S(1)}, bf16[2,64,128]{2,1,0:T(8,128)(2,1)S(1)}, u32[]{:S(2)}, u32[]{:S(2)}) %collective-permute-start.24) | collective-permute-done | bytes 32800 | tf_op jit(solution)/shard_map/ppermute | solution.py:29
  73.4 1.5 %collective-permute-start.27 = (bf16[2,2,64,128]{3,2,1,0:T(8,128)(2,1)S(1)}, bf16[2,2,64,128]{3,2,1,0:T(8,128)(2,1)S(1)}, u32[]{:S(2)}, u32[]{:S(2)}) collective-permute-start(bf16[2,2,64,128]{3,2,1,0:T(8,128)(2,1)S(1)} %pad_maximum_fusion.1.refs_0_), channel_id=1, source_target_pairs={{0,6},{2,4},{4,2},{6,0},{8,14},{10,12},{12,10},{14,8},{16,22},{18,... | collective-permute-start | bytes 196616 | tf_op jit(solution)/shard_map/ppermute | solution.py:29
  74.9 1.2 %collective-permute-start.25 = (bf16[2,2,64,128]{3,2,1,0:T(8,128)(2,1)S(1)}, bf16[2,2,64,128]{3,2,1,0:T(8,128)(2,1)S(1)}, u32[]{:S(2)}, u32[]{:S(2)}) collective-permute-start(bf16[2,2,64,128]{3,2,1,0:T(8,128)(2,1)S(1)} %pad_maximum_fusion.1.refs_0_), channel_id=1, source_target_pairs={{0,2},{2,0},{4,6},{6,4},{8,10},{10,8},{12,14},{14,12},{16,18},{18,... | collective-permute-start | bytes 196616 | tf_op jit(solution)/shard_map/ppermute | solution.py:29
  76.1 0.8 %collective-permute-start.26 = (bf16[2,2,64,128]{3,2,1,0:T(8,128)(2,1)S(1)}, bf16[2,2,64,128]{3,2,1,0:T(8,128)(2,1)S(1)}, u32[]{:S(2)}, u32[]{:S(2)}) collective-permute-start(bf16[2,2,64,128]{3,2,1,0:T(8,128)(2,1)S(1)} %pad_maximum_fusion.1.refs_0_), channel_id=1, source_target_pairs={{0,4},{2,6},{4,0},{6,2},{8,12},{10,14},{12,8},{14,10},{16,20},{18,... | collective-permute-start | bytes 196616 | tf_op jit(solution)/shard_map/ppermute | solution.py:29
  76.9 0.7 store.1
  77.7 1.0 %collective-permute-done.27.refs_1_ = bf16[2,2,64,128]{3,2,1,0:T(8,128)(2,1)S(1)} collective-permute-done((bf16[2,2,64,128]{3,2,1,0:T(8,128)(2,1)S(1)}, bf16[2,2,64,128]{3,2,1,0:T(8,128)(2,1)S(1)}, u32[]{:S(2)}, u32[]{:S(2)}) %collective-permute-start.27) | collective-permute-done | bytes 65568 | tf_op jit(solution)/shard_map/ppermute | solution.py:29
  78.6 0.7 settle.2.refs_2_
  79.3 1.0 %collective-permute-done.26.refs_1_ = bf16[2,2,64,128]{3,2,1,0:T(8,128)(2,1)S(1)} collective-permute-done((bf16[2,2,64,128]{3,2,1,0:T(8,128)(2,1)S(1)}, bf16[2,2,64,128]{3,2,1,0:T(8,128)(2,1)S(1)}, u32[]{:S(2)}, u32[]{:S(2)}) %collective-permute-start.26) | collective-permute-done | bytes 65568 | tf_op jit(solution)/shard_map/ppermute | solution.py:29
  80.4 0.7 settle.3
  (22 shorter events, 0.2 us)
Async XLA Ops:
  2.4 3.6 %collective-permute-start.1 = (bf16[128,2048]{1,0:T(8,128)(2,1)S(1)}, bf16[128,2048]{1,0:T(8,128)(2,1)S(1)}, u32[]{:S(2)}, u32[]{:S(2)}) collective-permute-start(bf16[128,2048]{1,0:T(8,128)(2,1)S(1)} %get-tuple-element.74.refs_0_), channel_id=1, source_target_pairs={{0,1},{1,0},{2,3},{3,2},{4,5},{5,4},{6,7},{7,6},{8,9},{9,8},{10,11... | collective-permute-start | bytes 1572872 | tf_op jit(solution)/shard_map/ppermute | solution.py:29
  3.0 3.1 %collective-permute-start.2 = (bf16[128,2048]{1,0:T(8,128)(2,1)S(1)}, bf16[128,2048]{1,0:T(8,128)(2,1)S(1)}, u32[]{:S(2)}, u32[]{:S(2)}) collective-permute-start(bf16[128,2048]{1,0:T(8,128)(2,1)S(1)} %get-tuple-element.75.refs_1_), channel_id=1, source_target_pairs={{0,1},{1,0},{2,3},{3,2},{4,5},{5,4},{6,7},{7,6},{8,9},{9,8},{10,11... | collective-permute-start | bytes 1572872 | tf_op jit(solution)/shard_map/ppermute | solution.py:29
  3.1 2.3 %collective-permute-start = (f32[32,512]{1,0:T(8,128)S(1)}, f32[32,512]{1,0:T(8,128)S(1)}, u32[]{:S(2)}, u32[]{:S(2)}) collective-permute-start(f32[32,512]{1,0:T(8,128)S(1)} %get-tuple-element.72), channel_id=1, source_target_pairs={{0,1},{1,0},{2,3},{3,2},{4,5},{5,4},{6,7},{7,6},{8,9},{9,8},{10,11... | collective-permute-start | bytes 196616 | tf_op jit(solution)/shard_map/ppermute | solution.py:29
  3.5 1.9 %copy-start = (f32[2,2,32,512]{3,2,1,0:T(8,128)S(1)}, f32[2,2,32,512]{3,2,1,0:T(8,128)}, u32[]{:S(2)}) copy-start(f32[2,2,32,512]{3,2,1,0:T(8,128)} %refs_4_.5) | copy-start | bytes 786436
  8.3 37.7 %collective-permute-start.10 = (bf16[2048,128]{1,0:T(8,128)(2,1)S(1)}, bf16[2048,128]{1,0:T(8,128)(2,1)S(1)}, u32[]{:S(2)}, u32[]{:S(2)}) collective-permute-start(bf16[2048,128]{1,0:T(8,128)(2,1)S(1)} %get-tuple-element.97.refs_2_), channel_id=1, source_target_pairs={{0,1},{1,0},{2,3},{3,2},{4,5},{5,4},{6,7},{7,6},{8,9},{9,8},{10,11... | collective-permute-start | bytes 1572872 | tf_op jit(solution)/shard_map/ppermute | solution.py:29
  8.7 6.8 %collective-permute-start.3 = (bf16[4,32,512]{2,1,0:T(8,128)(2,1)S(1)}, bf16[4,32,512]{2,1,0:T(8,128)(2,1)S(1)}, u32[]{:S(2)}, u32[]{:S(2)}) collective-permute-start(bf16[4,32,512]{2,1,0:T(8,128)(2,1)S(1)} %get-tuple-element.87), channel_id=1, source_target_pairs={{0,2},{2,0},{4,6},{6,4},{8,10},{10,8},{12,14},{14,12},{16,18},{18,... | collective-permute-start | bytes 393224 | tf_op jit(solution)/shard_map/ppermute | solution.py:29
  11.4 8.3 %collective-permute-start.4 = (bf16[4,32,512]{2,1,0:T(8,128)(2,1)S(1)}, bf16[4,32,512]{2,1,0:T(8,128)(2,1)S(1)}, u32[]{:S(2)}, u32[]{:S(2)}) collective-permute-start(bf16[4,32,512]{2,1,0:T(8,128)(2,1)S(1)} %get-tuple-element.88), channel_id=1, source_target_pairs={{0,4},{2,6},{4,0},{6,2},{8,12},{10,14},{12,8},{14,10},{16,20},{18,... | collective-permute-start | bytes 393224 | tf_op jit(solution)/shard_map/ppermute | solution.py:29
  12.9 6.8 %collective-permute-start.5 = (bf16[4,32,512]{2,1,0:T(8,128)(2,1)S(1)}, bf16[4,32,512]{2,1,0:T(8,128)(2,1)S(1)}, u32[]{:S(2)}, u32[]{:S(2)}) collective-permute-start(bf16[4,32,512]{2,1,0:T(8,128)(2,1)S(1)} %get-tuple-element.89), channel_id=1, source_target_pairs={{0,6},{2,4},{4,2},{6,0},{8,14},{10,12},{12,10},{14,8},{16,22},{18,... | collective-permute-start | bytes 393224 | tf_op jit(solution)/shard_map/ppermute | solution.py:29
  19.7 4.3 %collective-permute-start.6 = (bf16[2,32,512]{2,1,0:T(8,128)(2,1)S(1)}, bf16[2,32,512]{2,1,0:T(8,128)(2,1)S(1)}, u32[]{:S(2)}, u32[]{:S(2)}) collective-permute-start(bf16[2,32,512]{2,1,0:T(8,128)(2,1)S(1)} %get-tuple-element.91), channel_id=1, source_target_pairs={{0,8},{2,10},{4,12},{6,14},{8,0},{10,2},{12,4},{14,6},{16,24},{18,... | collective-permute-start | bytes 196616 | tf_op jit(solution)/shard_map/ppermute | solution.py:29
  24.1 5.3 %collective-permute-start.7 = (bf16[2,32,512]{2,1,0:T(8,128)(2,1)S(1)}, bf16[2,32,512]{2,1,0:T(8,128)(2,1)S(1)}, u32[]{:S(2)}, u32[]{:S(2)}) collective-permute-start(bf16[2,32,512]{2,1,0:T(8,128)(2,1)S(1)} %shard_map.146.own_ref), channel_id=1, source_target_pairs={{0,16},{2,18},{4,20},{6,22},{8,24},{10,26},{12,28},{14,30},{16,0},... | collective-permute-start | bytes 196616 | tf_op jit(solution)/shard_map/ppermute | solution.py:29
  29.4 2.9 %copy-start.1 = (f32[2,2048]{1,0:T(2,128)S(1)}, f32[2,2048]{1,0:T(2,128)}, u32[]{:S(2)}) copy-start(f32[2,2048]{1,0:T(2,128)} %refs_0_.9) | copy-start | bytes 49156
  29.4 4.0 %collective-permute-start.8 = (bf16[2,32,256]{2,1,0:T(8,128)(2,1)S(1)}, bf16[2,32,256]{2,1,0:T(8,128)(2,1)S(1)}, u32[]{:S(2)}, u32[]{:S(2)}) collective-permute-start(bf16[2,32,256]{2,1,0:T(8,128)(2,1)S(1)} %shard_map.147.own_ref), channel_id=1, source_target_pairs={{0,8},{2,10},{4,12},{6,14},{8,0},{10,2},{12,4},{14,6},{16,24},{18,... | collective-permute-start | bytes 98312 | tf_op jit(solution)/shard_map/ppermute | solution.py:29
  31.0 23.2 %collective-permute-start.18 = (bf16[128,1024]{1,0:T(8,128)(2,1)S(1)}, bf16[128,1024]{1,0:T(8,128)(2,1)S(1)}, u32[]{:S(2)}, u32[]{:S(2)}) collective-permute-start(bf16[128,1024]{1,0:T(8,128)(2,1)S(1)} %get-tuple-element.112), channel_id=1, source_target_pairs={{0,2},{2,0},{4,6},{6,4},{8,10},{10,8},{12,14},{14,12},{16,18},{18,... | collective-permute-start | bytes 786440 | tf_op jit(solution)/shard_map/ppermute | solution.py:29
  32.2 2.6 %collective-permute-start.9 = (f32[2,2048]{1,0:T(2,128)S(1)}, f32[2,2048]{1,0:T(2,128)S(1)}, u32[]{:S(2)}, u32[]{:S(2)}) collective-permute-start(f32[2,2048]{1,0:T(2,128)S(1)} %copy-done.1), channel_id=1, source_target_pairs={{0,1},{1,0},{2,3},{3,2},{4,5},{5,4},{6,7},{7,6},{8,9},{9,8},{10,11... | collective-permute-start | bytes 49160 | tf_op jit(solution)/shard_map/ppermute | solution.py:29
  32.2 23.4 %collective-permute-start.19 = (bf16[128,1024]{1,0:T(8,128)(2,1)S(1)}, bf16[128,1024]{1,0:T(8,128)(2,1)S(1)}, u32[]{:S(2)}, u32[]{:S(2)}) collective-permute-start(bf16[128,1024]{1,0:T(8,128)(2,1)S(1)} %get-tuple-element.113), channel_id=1, source_target_pairs={{0,4},{2,6},{4,0},{6,2},{8,12},{10,14},{12,8},{14,10},{16,20},{18,... | collective-permute-start | bytes 786440 | tf_op jit(solution)/shard_map/ppermute | solution.py:29
  33.4 22.2 %collective-permute-start.20 = (bf16[128,1024]{1,0:T(8,128)(2,1)S(1)}, bf16[128,1024]{1,0:T(8,128)(2,1)S(1)}, u32[]{:S(2)}, u32[]{:S(2)}) collective-permute-start(bf16[128,1024]{1,0:T(8,128)(2,1)S(1)} %get-tuple-element.114), channel_id=1, source_target_pairs={{0,6},{2,4},{4,2},{6,0},{8,14},{10,12},{12,10},{14,8},{16,22},{18,... | collective-permute-start | bytes 786440 | tf_op jit(solution)/shard_map/ppermute | solution.py:29
  34.9 10.6 %collective-permute-start.11 = (bf16[2,2,32,256]{3,2,1,0:T(8,128)(2,1)S(1)}, bf16[2,2,32,256]{3,2,1,0:T(8,128)(2,1)S(1)}, u32[]{:S(2)}, u32[]{:S(2)}) collective-permute-start(bf16[2,2,32,256]{3,2,1,0:T(8,128)(2,1)S(1)} %pad_maximum_fusion.piece), channel_id=1, source_target_pairs={{0,6},{2,4},{4,2},{6,0},{8,14},{10,12},{12,10},{14,8},{16,22},{18,... | collective-permute-start | bytes 196616 | tf_op jit(solution)/shard_map/ppermute | solution.py:29
  45.5 4.3 %collective-permute-start.12 = (bf16[2,2,32,256]{3,2,1,0:T(8,128)(2,1)S(1)}, bf16[2,2,32,256]{3,2,1,0:T(8,128)(2,1)S(1)}, u32[]{:S(2)}, u32[]{:S(2)}) collective-permute-start(bf16[2,2,32,256]{3,2,1,0:T(8,128)(2,1)S(1)} %pad_maximum_fusion.piece), channel_id=1, source_target_pairs={{0,4},{2,6},{4,0},{6,2},{8,12},{10,14},{12,8},{14,10},{16,20},{18,... | collective-permute-start | bytes 196616 | tf_op jit(solution)/shard_map/ppermute | solution.py:29
  46.0 4.3 %collective-permute-start.13 = (bf16[2,2,32,256]{3,2,1,0:T(8,128)(2,1)S(1)}, bf16[2,2,32,256]{3,2,1,0:T(8,128)(2,1)S(1)}, u32[]{:S(2)}, u32[]{:S(2)}) collective-permute-start(bf16[2,2,32,256]{3,2,1,0:T(8,128)(2,1)S(1)} %pad_maximum_fusion.piece), channel_id=1, source_target_pairs={{0,2},{2,0},{4,6},{6,4},{8,10},{10,8},{12,14},{14,12},{16,18},{18,... | collective-permute-start | bytes 196616 | tf_op jit(solution)/shard_map/ppermute | solution.py:29
  50.9 1.2 %collective-permute-start.14 = (bf16[1,32,128]{2,1,0:T(8,128)(2,1)S(1)}, bf16[1,32,128]{2,1,0:T(8,128)(2,1)S(1)}, u32[]{:S(2)}, u32[]{:S(2)}) collective-permute-start(bf16[1,32,128]{2,1,0:T(8,128)(2,1)S(1)} %bitcast.17), channel_id=1, source_target_pairs={{0,1},{1,0},{2,3},{3,2},{4,5},{5,4},{6,7},{7,6},{8,9},{9,8},{10,11... | collective-permute-start | bytes 24584 | tf_op jit(solution)/shard_map/ppermute | solution.py:29
  52.1 3.7 %collective-permute-start.15 = (bf16[64,128]{1,0:T(8,128)(2,1)S(1)}, bf16[64,128]{1,0:T(8,128)(2,1)S(1)}, u32[]{:S(2)}, u32[]{:S(2)}) collective-permute-start(bf16[64,128]{1,0:T(8,128)(2,1)S(1)} %bitcast.13), channel_id=1, source_target_pairs={{0,2},{2,0},{4,6},{6,4},{8,10},{10,8},{12,14},{14,12},{16,18},{18,... | collective-permute-start | bytes 49160 | tf_op jit(solution)/shard_map/ppermute | solution.py:29
  53.3 3.7 %collective-permute-start.16 = (bf16[64,128]{1,0:T(8,128)(2,1)S(1)}, bf16[64,128]{1,0:T(8,128)(2,1)S(1)}, u32[]{:S(2)}, u32[]{:S(2)}) collective-permute-start(bf16[64,128]{1,0:T(8,128)(2,1)S(1)} %bitcast.14), channel_id=1, source_target_pairs={{0,4},{2,6},{4,0},{6,2},{8,12},{10,14},{12,8},{14,10},{16,20},{18,... | collective-permute-start | bytes 49160 | tf_op jit(solution)/shard_map/ppermute | solution.py:29
  54.2 4.6 %collective-permute-start.17 = (bf16[64,128]{1,0:T(8,128)(2,1)S(1)}, bf16[64,128]{1,0:T(8,128)(2,1)S(1)}, u32[]{:S(2)}, u32[]{:S(2)}) collective-permute-start(bf16[64,128]{1,0:T(8,128)(2,1)S(1)} %bitcast.15), channel_id=1, source_target_pairs={{0,6},{2,4},{4,2},{6,0},{8,14},{10,12},{12,10},{14,8},{16,22},{18,... | collective-permute-start | bytes 49160 | tf_op jit(solution)/shard_map/ppermute | solution.py:29
  59.1 4.3 %collective-permute-start.21 = (bf16[2,64,256]{2,1,0:T(8,128)(2,1)S(1)}, bf16[2,64,256]{2,1,0:T(8,128)(2,1)S(1)}, u32[]{:S(2)}, u32[]{:S(2)}) collective-permute-start(bf16[2,64,256]{2,1,0:T(8,128)(2,1)S(1)} %get-tuple-element.116), channel_id=1, source_target_pairs={{0,8},{2,10},{4,12},{6,14},{8,0},{10,2},{12,4},{14,6},{16,24},{18,... | collective-permute-start | bytes 196616 | tf_op jit(solution)/shard_map/ppermute | solution.py:29
  63.5 5.9 %collective-permute-start.22 = (bf16[2,64,256]{2,1,0:T(8,128)(2,1)S(1)}, bf16[2,64,256]{2,1,0:T(8,128)(2,1)S(1)}, u32[]{:S(2)}, u32[]{:S(2)}) collective-permute-start(bf16[2,64,256]{2,1,0:T(8,128)(2,1)S(1)} %shard_map.155.own_ref), channel_id=1, source_target_pairs={{0,16},{2,18},{4,20},{6,22},{8,24},{10,26},{12,28},{14,30},{16,0},... | collective-permute-start | bytes 196616 | tf_op jit(solution)/shard_map/ppermute | solution.py:29
  66.8 1.2 %collective-permute-start.23 = (bf16[2,32,128]{2,1,0:T(8,128)(2,1)S(1)}, bf16[2,32,128]{2,1,0:T(8,128)(2,1)S(1)}, u32[]{:S(2)}, u32[]{:S(2)}) collective-permute-start(bf16[2,32,128]{2,1,0:T(8,128)(2,1)S(1)} %slice.4), channel_id=1, source_target_pairs={{0,1},{1,0},{2,3},{3,2},{4,5},{5,4},{6,7},{7,6},{8,9},{9,8},{10,11... | collective-permute-start | bytes 49160 | tf_op jit(solution)/shard_map/ppermute | solution.py:29
  69.4 4.0 %collective-permute-start.24 = (bf16[2,64,128]{2,1,0:T(8,128)(2,1)S(1)}, bf16[2,64,128]{2,1,0:T(8,128)(2,1)S(1)}, u32[]{:S(2)}, u32[]{:S(2)}) collective-permute-start(bf16[2,64,128]{2,1,0:T(8,128)(2,1)S(1)} %shard_map.157), channel_id=1, source_target_pairs={{0,8},{2,10},{4,12},{6,14},{8,0},{10,2},{12,4},{14,6},{16,24},{18,... | collective-permute-start | bytes 98312 | tf_op jit(solution)/shard_map/ppermute | solution.py:29
  73.4 5.2 %collective-permute-start.27 = (bf16[2,2,64,128]{3,2,1,0:T(8,128)(2,1)S(1)}, bf16[2,2,64,128]{3,2,1,0:T(8,128)(2,1)S(1)}, u32[]{:S(2)}, u32[]{:S(2)}) collective-permute-start(bf16[2,2,64,128]{3,2,1,0:T(8,128)(2,1)S(1)} %pad_maximum_fusion.1.refs_0_), channel_id=1, source_target_pairs={{0,6},{2,4},{4,2},{6,0},{8,14},{10,12},{12,10},{14,8},{16,22},{18,... | collective-permute-start | bytes 196616 | tf_op jit(solution)/shard_map/ppermute | solution.py:29
  74.9 4.4 %collective-permute-start.25 = (bf16[2,2,64,128]{3,2,1,0:T(8,128)(2,1)S(1)}, bf16[2,2,64,128]{3,2,1,0:T(8,128)(2,1)S(1)}, u32[]{:S(2)}, u32[]{:S(2)}) collective-permute-start(bf16[2,2,64,128]{3,2,1,0:T(8,128)(2,1)S(1)} %pad_maximum_fusion.1.refs_0_), channel_id=1, source_target_pairs={{0,2},{2,0},{4,6},{6,4},{8,10},{10,8},{12,14},{14,12},{16,18},{18,... | collective-permute-start | bytes 196616 | tf_op jit(solution)/shard_map/ppermute | solution.py:29
  76.1 4.3 %collective-permute-start.26 = (bf16[2,2,64,128]{3,2,1,0:T(8,128)(2,1)S(1)}, bf16[2,2,64,128]{3,2,1,0:T(8,128)(2,1)S(1)}, u32[]{:S(2)}, u32[]{:S(2)}) collective-permute-start(bf16[2,2,64,128]{3,2,1,0:T(8,128)(2,1)S(1)} %pad_maximum_fusion.1.refs_0_), channel_id=1, source_target_pairs={{0,4},{2,6},{4,0},{6,2},{8,12},{10,14},{12,8},{14,10},{16,20},{18,... | collective-permute-start | bytes 196616 | tf_op jit(solution)/shard_map/ppermute | solution.py:29
